TPU v7x, 32 devices: a whole 2x2x4 slice. The times are simulated.
32 devices in a mesh: ep: 32 (over z, y, x, core).
Axes of the slice: x: 2, y: 2, z: 4, core: 2. Of those that a mesh axis runs over, the one named last changes fastest.
Arguments:
- latest_embeddings: bfloat16 [512, 2048], P('ep'), may hold values from -6 to 6
- prior_memory_grids: float32 [512, 32, 4096], P('ep'), may hold values from -1.75 to 1.75
- earlier_rescale_gain: float32 [2048], replicated, may hold values from 0.1 to 1.9
- query_map: bfloat16 [2048, 2048], P(None, 'ep'), may hold values from -0.125 to 0.125
- lookup_map: bfloat16 [2048, 2048], P(None, 'ep'), may hold values from -0.125 to 0.125
- content_map: bfloat16 [2048, 2048], P(None, 'ep'), may hold values from -0.125 to 0.125
- forget_lower_map: bfloat16 [2048, 64], replicated, may hold values from -0.125 to 0.125
- forget_upper_map: bfloat16 [64, 2048], replicated, may hold values from -0.75 to 0.75
- forget_shift: float32 [2048], replicated, may hold values from -3 to 3
- adapt_lower_map: bfloat16 [2048, 64], replicated, may hold values from -0.125 to 0.125
- adapt_upper_map: bfloat16 [64, 2048], replicated, may hold values from -0.75 to 0.75
- adapt_shift: float32 [2048], replicated, may hold values from -2 to 2
- erase_lookup_gains: float32 [2048], replicated, may hold values from 0.1 to 1.9
- substitute_lookup_gains: float32 [2048], replicated, may hold values from 0.1 to 1.9
- present_extra_gains: float32 [2048], replicated, may hold values from -1.75 to 1.75
- attender_rescale_gain: float32 [2048], replicated, may hold values from 0.1 to 1.9
- result_map: bfloat16 [2048, 2048], P(None, 'ep'), may hold values from -0.125 to 0.125
- later_rescale_gain: float32 [2048], replicated, may hold values from 0.1 to 1.9
- specialist_switch_maps: bfloat16 [32, 2048, 512], P('ep'), may hold values from -0.125 to 0.125
- specialist_widen_maps: bfloat16 [32, 2048, 512], P('ep'), may hold values from -0.125 to 0.125
- specialist_shrink_maps: bfloat16 [32, 512, 2048], P('ep'), may hold values from -0.25 to 0.25
- picked_specialists: int32 [512, 6], P('ep'), may hold values from 0 to 31, as said below
- specialist_picked_shares: float32 [512, 6], P('ep'), may hold values from 0.02 to 0.5
Outputs:
- new_hidden: bfloat16 [512, 2048], P('ep')
- new_state: float32 [512, 32, 4096], P('ep')
Inputs may be any that keep to these rules, and one draw needn't show every extreme that they name: `picked_specialists`: each row names 6 different experts of one group; a group is a run of 8 consecutive expert numbers. The rows of one device use exactly two groups, one of them for half of the device's rows rounded up and the other for the rest. No expert is named by more than 6 rows of one device, and on every device some expert is named by exactly 6.
All inputs are finite; a program needn't handle non-finite values.
Results may differ from a plain program's by a relative error of at most 0.011.
Values may be sent and summed in bfloat16 or wider, within the bound.
No kernel may reach another device: no remote copies, remote signals or barrier semaphores. Data moves between devices by JAX's collectives and lax.ppermute only.
A program may use at most 256 MiB of HBM per device.

v0:
```python
import math

import jax
import jax.numpy as jnp
from jax import lax
from jax.sharding import PartitionSpec as P

GROUPS = 4


norm_eps = 1e-06
group_eps = 0.00064
unit_eps = 1e-06


def rms_norm(rows_in, gain):
    values = rows_in.astype(jnp.float32)
    scale = lax.rsqrt(jnp.mean(values * values, axis=-1, keepdims=True) + norm_eps)
    return (values * scale * gain).astype(jnp.bfloat16)


def memory_readout(
    query_signal,
    substitute_lookup,
    content_signals,
    forget_multiplier,
    adapt_speed,
    erase_signal,
    memory_grid,
    attender_rescale_gain,
    present_extra_gains,
):
    highest = lax.Precision.HIGHEST
    removed = jnp.einsum("bhij,bhj->bhi", memory_grid, erase_signal, precision=highest)
    memory_grid = (
        memory_grid * forget_multiplier[:, :, None, :]
        - removed[..., None] * (erase_signal * adapt_speed)[:, :, None, :]
        + content_signals[..., None] * substitute_lookup[:, :, None, :]
    )
    readout = jnp.einsum("bhij,bhj->bhi", memory_grid, query_signal, precision=highest)
    centered = readout - jnp.mean(readout, axis=-1, keepdims=True)
    variance = jnp.mean(centered * centered, axis=-1, keepdims=True)
    rescaled_result = centered * lax.rsqrt(variance + group_eps) * attender_rescale_gain
    present_extra = (
        jnp.sum(query_signal * substitute_lookup * present_extra_gains, axis=-1, keepdims=True)
        * content_signals
    )
    return (rescaled_result + present_extra, memory_grid)


def local(
    latest_embeddings,
    prior_memory_grids,
    earlier_rescale_gain,
    query_map,
    lookup_map,
    content_map,
    forget_lower_map,
    forget_upper_map,
    forget_shift,
    adapt_lower_map,
    adapt_upper_map,
    adapt_shift,
    erase_lookup_gains,
    substitute_lookup_gains,
    present_extra_gains,
    attender_rescale_gain,
    result_map,
    later_rescale_gain,
    specialist_switch_maps,
    specialist_widen_maps,
    specialist_shrink_maps,
    picked_specialists,
    specialist_picked_shares,
):
    seq_count, model_width = latest_embeddings.shape
    attender_count = prior_memory_grids.shape[1]
    channel_span = model_width // attender_count
    devices = lax.axis_size("ep")
    columns = query_map.shape[1]
    normed = rms_norm(latest_embeddings, earlier_rescale_gain)
    stacked = jnp.concatenate([query_map, lookup_map, content_map], axis=1)
    projected = jnp.dot(
        lax.all_gather(normed, "ep", axis=0, tiled=True),
        stacked,
        preferred_element_type=jnp.float32,
    ).astype(jnp.bfloat16)
    query_signal, key_rows, content_signals = (
        lax.all_to_all(projected[:, :columns], "ep", split_axis=0, concat_axis=1, tiled=True),
        lax.all_to_all(
            projected[:, columns : 2 * columns], "ep", split_axis=0, concat_axis=1, tiled=True
        ),
        lax.all_to_all(projected[:, 2 * columns :], "ep", split_axis=0, concat_axis=1, tiled=True),
    )
    decay_low = jnp.tanh(
        jnp.dot(normed, forget_lower_map, preferred_element_type=jnp.float32)
    ).astype(jnp.bfloat16)
    forget_multiplier = jnp.exp(
        -math.exp(-0.5)
        * jax.nn.sigmoid(
            forget_shift + jnp.dot(decay_low, forget_upper_map, preferred_element_type=jnp.float32)
        )
    )
    rate_low = jnp.dot(normed, adapt_lower_map, preferred_element_type=jnp.float32).astype(
        jnp.bfloat16
    )
    adapt_speed = jax.nn.sigmoid(
        adapt_shift + jnp.dot(rate_low, adapt_upper_map, preferred_element_type=jnp.float32)
    )
    key_float = key_rows.astype(jnp.float32)
    erase_signal = (key_float * erase_lookup_gains).reshape(seq_count, attender_count, channel_span)
    erase_signal = erase_signal * lax.rsqrt(
        jnp.sum(erase_signal * erase_signal, axis=-1, keepdims=True) + unit_eps
    )
    substitute_lookup = key_float * (1.0 + (adapt_speed - 1.0) * substitute_lookup_gains)
    head_shape = (seq_count, attender_count, channel_span)
    mixed_heads, memory_grid = memory_readout(
        query_signal.astype(jnp.float32).reshape(head_shape),
        substitute_lookup.reshape(head_shape),
        content_signals.astype(jnp.float32).reshape(head_shape),
        forget_multiplier.reshape(head_shape),
        adapt_speed.reshape(head_shape),
        erase_signal,
        prior_memory_grids.reshape(seq_count, attender_count, channel_span, channel_span),
        attender_rescale_gain.reshape(attender_count, channel_span),
        present_extra_gains.reshape(attender_count, channel_span),
    )
    mixed = mixed_heads.reshape(seq_count, model_width).astype(jnp.bfloat16)
    new_state = memory_grid.reshape(seq_count, attender_count, channel_span * channel_span)
    partial_rows = jnp.dot(
        lax.all_gather(mixed, "ep", axis=0, tiled=True),
        result_map,
        preferred_element_type=jnp.float32,
    ).astype(jnp.bfloat16)
    mixer_out = lax.all_to_all(partial_rows, "ep", split_axis=0, concat_axis=1, tiled=True)
    residual = (latest_embeddings.astype(jnp.float32) + mixer_out.astype(jnp.float32)).astype(
        jnp.bfloat16
    )
    second = rms_norm(residual, later_rescale_gain)
    top_count = picked_specialists.shape[1]
    expert_count = specialist_switch_maps.shape[0] * devices
    group_size = expert_count // GROUPS
    capacity = ((seq_count + 1) // 2 * top_count + group_size - 1) // group_size
    flat_ids = picked_specialists.reshape(-1)
    matches = (flat_ids[:, None] == jnp.arange(expert_count, dtype=jnp.int32)[None, :]).astype(
        jnp.int32
    )
    slot_rank = jnp.sum((jnp.cumsum(matches, axis=0) - matches) * matches, axis=1)
    slot_ids = flat_ids * capacity + slot_rank
    picks = (
        slot_ids[:, None] == jnp.arange(expert_count * capacity, dtype=jnp.int32)[None, :]
    ).astype(jnp.bfloat16)
    repeated = jnp.repeat(second, top_count, axis=0)
    send_rows = jnp.einsum("sk,sd->kd", picks, repeated, preferred_element_type=jnp.float32).astype(
        jnp.bfloat16
    )
    send_rows = send_rows.reshape(devices, expert_count // devices * capacity, model_width)
    received = lax.all_to_all(send_rows, "ep", split_axis=0, concat_axis=0, tiled=True)
    rows_in = received.reshape(-1, model_width)
    gate_proj = jnp.dot(rows_in, specialist_switch_maps[0], preferred_element_type=jnp.float32)
    up_proj = jnp.dot(rows_in, specialist_widen_maps[0], preferred_element_type=jnp.float32)
    hidden_act = (jax.nn.silu(gate_proj) * up_proj).astype(jnp.bfloat16)
    results = jnp.dot(
        hidden_act, specialist_shrink_maps[0], preferred_element_type=jnp.float32
    ).astype(jnp.bfloat16)
    returned = lax.all_to_all(
        results.reshape(received.shape), "ep", split_axis=0, concat_axis=0, tiled=True
    )
    collected = jnp.dot(
        picks, returned.reshape(-1, model_width), preferred_element_type=jnp.float32
    )
    expert_sum = jnp.sum(
        collected.reshape(seq_count, top_count, model_width) * specialist_picked_shares[:, :, None],
        axis=1,
    )
    new_hidden = (residual.astype(jnp.float32) + expert_sum).astype(jnp.bfloat16)
    return (new_hidden, new_state)


def solution(mesh):
    return jax.shard_map(
        local,
        mesh=mesh,
        in_specs=(
            P("ep", None),
            P("ep", None, None),
            P(),
            P(None, "ep"),
            P(None, "ep"),
            P(None, "ep"),
            P(),
            P(),
            P(),
            P(),
            P(),
            P(),
            P(),
            P(),
            P(),
            P(),
            P(None, "ep"),
            P(),
            P("ep", None, None),
            P("ep", None, None),
            P("ep", None, None),
            P("ep", None),
            P("ep", None),
        ),
        out_specs=(P("ep", None), P("ep", None, None)),
        check_vma=False,
    )
```

profile of v0, /device:TPU:0, one launch (start us, length us, event | category | flops | bytes accessed | tf_op | source)
XLA Modules:
  0.0 342.3 jit_solution(15131973935184943869)
XLA Ops:
  8.3 1.6 fusion.59
  12.2 58.1 %all-gather.3.cloned.1.call-done = bf16[512,2048]{1,0:T(8,128)(2,1)} async-done(((bf16[16,2048]{1,0:T(8,128)(2,1)}), bf16[512,2048]{1,0:T(8,128)(2,1)}) %all-gather.3.cloned.1.call-update) | async-done | bytes 2097168 | tf_op jit(solution)/shard_map/all_gather | solution.py:84
  70.4 2.6 convolution_convert_fusion.2
  73.9 3.5 %all-to-all-start = ((bf16[32,2,512]{2,1,0:T(2,128)(2,1)}), bf16[32,2,512]{2,1,0:T(2,128)(2,1)S(1)}, u32[]{:S(2)}, u32[]{:S(2)}) async-start(bf16[32,2,512]{2,1,0:T(2,128)(2,1)} %reshape.162), calls=%async_computation | async-start | bytes 131072 | tf_op jit(solution)/shard_map/all_to_all | solution.py:90
  77.3 1.5 fusion.15
  79.0 14.2 %reshape.147 = f32[16,32,64,64]{3,2,1,0:T(8,128)} reshape(f32[16,32,4096]{2,1,0:T(8,128)} %param.24) | data formatting | bytes 16777216 | tf_op jit(solution)/shard_map/reshape | solution.py:124
  95.0 5.8 %all-to-all-start.1 = ((bf16[32,2,512]{2,1,0:T(2,128)(2,1)}), bf16[32,2,512]{2,1,0:T(2,128)(2,1)S(1)}, u32[]{:S(2)}, u32[]{:S(2)}) async-start(bf16[32,2,512]{2,1,0:T(2,128)(2,1)} %reshape.164), calls=%async_computation.1 | async-start | bytes 131072 | tf_op jit(solution)/shard_map/all_to_all | solution.py:93
  101.4 1.4 add_multiply_fusion
  103.8 28.7 %fusion.51 = f32[16,32,1,64]{3,2,1,0:T(1,128)S(1)} fusion(f32[16,32,64,64]{3,2,1,0:T(8,128)} %reshape.147, f32[16,32,64,1]{2,0,1,3:T(8,128)S(1)} %get-tuple-element.7), kind=kOutput, calls=%fused_computation.61 | convolution fusion | flops 25165824 | bytes 8650752 | tf_op jit(solution)/shard_map/bhij,bhj->bhi/dot_general | solution.py:34
  133.6 5.8 %all-to-all-start.2 = ((bf16[32,2,512]{2,1,0:T(2,128)(2,1)}), bf16[32,2,512]{2,1,0:T(2,128)(2,1)S(1)}, u32[]{:S(2)}, u32[]{:S(2)}) async-start(bf16[32,2,512]{2,1,0:T(2,128)(2,1)} %reshape.166), calls=%async_computation.2 | async-start | bytes 131072 | tf_op jit(solution)/shard_map/all_to_all | solution.py:89
  140.7 6.2 %all-to-all-done.2 = bf16[32,2,512]{2,1,0:T(2,128)(2,1)S(1)} async-done(((bf16[32,2,512]{2,1,0:T(2,128)(2,1)}), bf16[32,2,512]{2,1,0:T(2,128)(2,1)S(1)}, u32[]{:S(2)}, u32[]{:S(2)}) %all-to-all-start.2) | async-done | bytes 65568 | tf_op jit(solution)/shard_map/all_to_all | solution.py:89
  147.1 20.5 %fusion.1 = f32[16,32,1,64]{3,2,1,0:T(1,128)S(1)} fusion(f32[16,32,64,64]{3,2,1,0:T(8,128)} %reshape.147, f32[16,32,64]{2,1,0:T(8,128)S(1)} %mul.216, f32[16,32,64]{2,1,0:T(8,128)S(1)} %copy.61, f32[16,32,64]{2,1,0:T(8,128)S(1)} %bitcast.81, f32[16,32,64]{2,1,0:T(8,128)S(1)} %mul.234, f32[16,32,64]{2,1,0:T(8,128)} %copy.63, ...), kind=kOutput, calls=%fused_computation.1 | convolution fusion | flops 35651584 | bytes 9240576 | tf_op jit(solution)/shard_map/bhij,bhj->bhi/dot_general | solution.py:40
  170.8 6.8 %mul.217 = f32[16,32,64,64]{3,2,1,0:T(8,128)} broadcast(f32[16,32,64]{2,1,0:T(8,128)S(1)} %mul.216), dimensions={0,1,3} | broadcast | bytes 8519680 | tf_op jit(solution)/shard_map/mul | solution.py:36
  177.6 14.8 %mul.263 = f32[16,32,4096]{2,1,0:T(8,128)} reshape(f32[16,32,64,64]{3,2,1,0:T(8,128)} %mul.217) | data formatting | bytes 16777216 | tf_op jit(solution)/shard_map/mul | solution.py:36
  192.4 30.7 %all-gather.5.cloned.1.call-done = bf16[512,2048]{1,0:T(8,128)(2,1)} async-done(((bf16[16,2048]{1,0:T(8,128)(2,1)}), bf16[512,2048]{1,0:T(8,128)(2,1)}) %all-gather.5.cloned.1.call-update) | async-done | bytes 2097168 | tf_op jit(solution)/shard_map/all_gather | solution.py:131
  223.1 2.3 convolution_convert_fusion.3
  226.4 3.5 %all-to-all-start.3 = ((bf16[32,2,512]{2,1,0:T(2,128)(2,1)}), bf16[32,2,512]{2,1,0:T(2,128)(2,1)S(1)}, u32[]{:S(2)}, u32[]{:S(2)}) async-start(bf16[32,2,512]{2,1,0:T(2,128)(2,1)} %reshape.168), calls=%async_computation.3 | async-start | bytes 131072 | tf_op jit(solution)/shard_map/all_to_all | solution.py:135
  229.8 7.4 %all-to-all-done.3 = bf16[32,2,512]{2,1,0:T(2,128)(2,1)S(1)} async-done(((bf16[32,2,512]{2,1,0:T(2,128)(2,1)}), bf16[32,2,512]{2,1,0:T(2,128)(2,1)S(1)}, u32[]{:S(2)}, u32[]{:S(2)}) %all-to-all-start.3) | async-done | bytes 65568 | tf_op jit(solution)/shard_map/all_to_all | solution.py:135
  238.8 1.5 convolution_convert_fusion.1
  240.3 1.2 reshape.150
  241.5 2.9 all-to-all-start.4
  244.4 9.3 %broadcast_multiply_fusion = f32[16,32,64,64]{3,2,1,0:T(8,128)} fusion(f32[16,32,64]{2,1,0:T(8,128)S(1)} %mul.234, f32[16,32,64]{2,1,0:T(8,128)} %copy.63), kind=kLoop, calls=%fused_computation.6 | loop fusion | flops 2097152 | bytes 8650752 | tf_op jit(solution)/shard_map/mul | solution.py:38
  253.7 14.8 %mul.266 = f32[16,32,4096]{2,1,0:T(8,128)} reshape(f32[16,32,64,64]{3,2,1,0:T(8,128)} %broadcast_multiply_fusion) | data formatting | bytes 16777216 | tf_op jit(solution)/shard_map/mul | solution.py:38
  268.5 9.3 %broadcast_multiply_fusion.1 = f32[16,32,64,64]{3,2,1,0:T(8,128)} fusion(f32[16,32,64]{2,1,0:T(8,128)} %copy-done.3, f32[16,32,64]{2,1,0:T(8,128)S(1)} %bitcast.82), kind=kLoop, calls=%fused_computation.7 | loop fusion | flops 2097152 | bytes 8650752 | tf_op jit(solution)/shard_map/mul | solution.py:37
  277.9 14.7 %mul.265 = f32[16,32,4096]{2,1,0:T(8,128)} reshape(f32[16,32,64,64]{3,2,1,0:T(8,128)} %broadcast_multiply_fusion.1) | data formatting | bytes 16777216 | tf_op jit(solution)/shard_map/mul | solution.py:37
  293.7 2.4 fusion.19
  296.2 3.0 convolution_convert_fusion
  299.1 1.2 reshape.152
  300.4 5.6 %all-to-all-start.5 = ((bf16[32,6,2048]{2,1,0:T(8,128)(2,1)}), bf16[32,6,2048]{2,1,0:T(8,128)(2,1)S(1)}, u32[]{:S(2)}, u32[]{:S(2)}) async-start(bf16[32,6,2048]{2,1,0:T(8,128)(2,1)} %reshape.152), calls=%async_computation.5 | async-start | bytes 2097152 | tf_op jit(solution)/shard_map/all_to_all | solution.py:166
  306.0 16.1 %subtract_add_fusion = f32[16,32,4096]{2,1,0:T(8,128)} fusion(f32[16,32,4096]{2,1,0:T(8,128)} %mul.266, f32[16,32,4096]{2,1,0:T(8,128)} %mul.265, f32[16,32,4096]{2,1,0:T(8,128)} %param.24, f32[16,32,4096]{2,1,0:T(8,128)} %mul.263), kind=kLoop, calls=%fused_computation.5 | loop fusion | flops 6291456 | bytes 41943040 | tf_op jit(solution)/shard_map/add | solution.py:36
  322.1 10.1 %all-to-all-done.5 = bf16[32,6,2048]{2,1,0:T(8,128)(2,1)S(1)} async-done(((bf16[32,6,2048]{2,1,0:T(8,128)(2,1)}), bf16[32,6,2048]{2,1,0:T(8,128)(2,1)S(1)}, u32[]{:S(2)}, u32[]{:S(2)}) %all-to-all-start.5) | async-done | bytes 786464 | tf_op jit(solution)/shard_map/all_to_all | solution.py:166
  333.3 1.5 fusion.21
  (90 shorter events, 18.8 us)
Async XLA Ops:
  7.2 289.0 %copy-start = (bf16[1,512,2048]{2,1,0:T(8,128)(2,1)S(1)}, bf16[1,512,2048]{2,1,0:T(8,128)(2,1)}, u32[]{:S(2)}) copy-start(bf16[1,512,2048]{2,1,0:T(8,128)(2,1)} %param.43) | copy-start | bytes 6291460
  7.2 63.2 %all-gather.3.cloned.1.call-start = ((), (), s32[]{:S(2)}) async-start(), calls=%async_computation.6 | async-start | bytes 2162688 | tf_op jit(solution)/shard_map/all_gather | solution.py:84
  73.9 21.1 %all-to-all-start = ((bf16[32,2,512]{2,1,0:T(2,128)(2,1)}), bf16[32,2,512]{2,1,0:T(2,128)(2,1)S(1)}, u32[]{:S(2)}, u32[]{:S(2)}) async-start(bf16[32,2,512]{2,1,0:T(2,128)(2,1)} %reshape.162), calls=%async_computation | async-start | bytes 131072 | tf_op jit(solution)/shard_map/all_to_all | solution.py:90
  78.9 22.4 %copy-start.6 = (bf16[16,2048]{1,0:T(8,128)(2,1)S(1)}, bf16[16,2048]{1,0:T(8,128)(2,1)}, u32[]{:S(2)}) copy-start(bf16[16,2048]{1,0:T(8,128)(2,1)} %fusion.59) | copy-start | bytes 196612
  79.0 22.4 %copy-start.9 = (bf16[64,2048]{1,0:T(8,128)(2,1)S(1)}, bf16[64,2048]{1,0:T(8,128)(2,1)}, u32[]{:S(2)}) copy-start(bf16[64,2048]{1,0:T(8,128)(2,1)} %param.33) | copy-start | bytes 786436
  79.0 22.4 %copy-start.10 = (f32[2048]{0:T(1024)S(1)}, f32[2048]{0:T(1024)}, u32[]{:S(2)}) copy-start(f32[2048]{0:T(1024)} %param.36) | copy-start | bytes 24580
  79.0 22.4 %copy-start.11 = (f32[2048]{0:T(1024)S(1)}, f32[2048]{0:T(1024)}, u32[]{:S(2)}) copy-start(f32[2048]{0:T(1024)} %param.34) | copy-start | bytes 24580
  95.0 38.6 %all-to-all-start.1 = ((bf16[32,2,512]{2,1,0:T(2,128)(2,1)}), bf16[32,2,512]{2,1,0:T(2,128)(2,1)S(1)}, u32[]{:S(2)}, u32[]{:S(2)}) async-start(bf16[32,2,512]{2,1,0:T(2,128)(2,1)} %reshape.164), calls=%async_computation.1 | async-start | bytes 131072 | tf_op jit(solution)/shard_map/all_to_all | solution.py:93
  132.5 35.1 %copy-start.1 = (f32[16,32,1,64]{3,2,1,0:T(1,128)}, f32[16,32,1,64]{3,2,1,0:T(1,128)S(1)}, u32[]{:S(2)}) copy-start(f32[16,32,1,64]{3,2,1,0:T(1,128)S(1)} %fusion.51) | copy-start | bytes 393220
  133.6 33.9 %copy-start.3 = (f32[16,32,64]{2,1,0:T(8,128)}, f32[16,32,64]{2,1,0:T(8,128)S(1)}, u32[]{:S(2)}) copy-start(f32[16,32,64]{2,1,0:T(8,128)S(1)} %copy.61) | copy-start | bytes 393220
  133.6 13.3 %all-to-all-start.2 = ((bf16[32,2,512]{2,1,0:T(2,128)(2,1)}), bf16[32,2,512]{2,1,0:T(2,128)(2,1)S(1)}, u32[]{:S(2)}, u32[]{:S(2)}) async-start(bf16[32,2,512]{2,1,0:T(2,128)(2,1)} %reshape.166), calls=%async_computation.2 | async-start | bytes 131072 | tf_op jit(solution)/shard_map/all_to_all | solution.py:89
  139.5 83.6 %all-gather.5.cloned.1.call-start = ((), (), s32[]{:S(2)}) async-start(), calls=%async_computation.7 | async-start | bytes 2162688 | tf_op jit(solution)/shard_map/all_gather | solution.py:131
  147.0 23.0 %copy-start.7 = (s32[16,6]{0,1:T(8,128)S(1)}, s32[16,6]{0,1:T(8,128)}, u32[]{:S(2)}) copy-start(s32[16,6]{0,1:T(8,128)} %param.44) | copy-start | bytes 1156
  177.6 45.5 %copy-start.5 = (bf16[2048,64]{0,1:T(8,128)(2,1)S(1)}, bf16[2048,64]{0,1:T(8,128)(2,1)}, u32[]{:S(2)}) copy-start(bf16[2048,64]{0,1:T(8,128)(2,1)} %param.39) | copy-start | bytes 786436
  177.6 60.0 %copy-start.4 = (bf16[16,2048]{1,0:T(8,128)(2,1)S(1)}, bf16[16,2048]{1,0:T(8,128)(2,1)}, u32[]{:S(2)}) copy-start(bf16[16,2048]{1,0:T(8,128)(2,1)} %param.23) | copy-start | bytes 196612
  177.6 60.2 %copy-start.8 = (f32[2048]{0:T(1024)S(1)}, f32[2048]{0:T(1024)}, u32[]{:S(2)}) copy-start(f32[2048]{0:T(1024)} %param.40) | copy-start | bytes 24580
  226.4 10.9 %all-to-all-start.3 = ((bf16[32,2,512]{2,1,0:T(2,128)(2,1)}), bf16[32,2,512]{2,1,0:T(2,128)(2,1)S(1)}, u32[]{:S(2)}, u32[]{:S(2)}) async-start(bf16[32,2,512]{2,1,0:T(2,128)(2,1)} %reshape.168), calls=%async_computation.3 | async-start | bytes 131072 | tf_op jit(solution)/shard_map/all_to_all | solution.py:135
  241.5 51.1 %all-to-all-start.4 = ((bf16[32,6,2048]{2,1,0:T(8,128)(2,1)}), bf16[32,6,2048]{2,1,0:T(8,128)(2,1)S(1)}, u32[]{:S(2)}, u32[]{:S(2)}) async-start(bf16[32,6,2048]{2,1,0:T(8,128)(2,1)} %reshape.150), calls=%async_computation.4 | async-start | bytes 2097152 | tf_op jit(solution)/shard_map/all_to_all | solution.py:158
  253.7 14.8 %copy-start.2 = (f32[16,32,1,64]{3,2,1,0:T(1,128)S(1)}, f32[16,32,1,64]{3,2,1,0:T(1,128)}, u32[]{:S(2)}) copy-start(f32[16,32,1,64]{3,2,1,0:T(1,128)} %copy-done.1) | copy-start | bytes 393220
  300.4 31.8 %all-to-all-start.5 = ((bf16[32,6,2048]{2,1,0:T(8,128)(2,1)}), bf16[32,6,2048]{2,1,0:T(8,128)(2,1)S(1)}, u32[]{:S(2)}, u32[]{:S(2)}) async-start(bf16[32,6,2048]{2,1,0:T(8,128)(2,1)} %reshape.152), calls=%async_computation.5 | async-start | bytes 2097152 | tf_op jit(solution)/shard_map/all_to_all | solution.py:166
  306.0 27.4 %copy-start.12 = (f32[16,6]{0,1:T(8,128)S(1)}, f32[16,6]{0,1:T(8,128)}, u32[]{:S(2)}) copy-start(f32[16,6]{0,1:T(8,128)} %param.45) | copy-start | bytes 1156
Sparse Core Ops, SparseCore 0:
  11.4 58.9 all-gather.2
  170.1 52.9 all-gather.4
where the time goes:
time: 345 us; the launch traced here: 342 us
  waiting for transfers between devices  113 us (33%)
  local copies, waits for them, and re-layouts  81.3 us (24%)
  matrix products  65.2 us (19%)
  other arithmetic  41.3 us (12%)
  starting transfers between devices  27.3 us (8%)
  between operations  14.5 us (4%)
    all_gather x1, waiting for transfers between devices, local(): lax.all_gather(normed, 'ep', axis=0, tiled=True)  58.1 us
    all_gather x1, waiting for transfers between devices, local(): lax.all_gather(mixed, 'ep', axis=0, tiled=True)  30.7 us
    dot_general x1, matrix products, memory_readout(): jnp.einsum('bhij,bhj->bhi', memory_grid, erase_signal, precision=highest)  28.7 us
    mul x3, local copies, waits for them, and re-layouts, memory_readout(): memory_grid * forget_multiplier[:, :, None, :]  21.8 us
    dot_general x1, matrix products, memory_readout(): jnp.einsum('bhij,bhj->bhi', memory_grid, query_signal, precision=highest)  20.5 us
    add x1, other arithmetic, memory_readout(): memory_grid * forget_multiplier[:, :, None, :]  16.1 us
    mul x2, local copies, waits for them, and re-layouts, memory_readout(): content_signals[..., None] * substitute_lookup[:, :, None, :]  14.9 us
    mul x1, local copies, waits for them, and re-layouts, memory_readout(): removed[..., None] * (erase_signal * adapt_speed)[:, :, None, :]  14.7 us
  transfers between devices with their start and end apart: 8, of which 5 were waited for; matrix products, arithmetic and copies ran while one was open for 41% of the time, Pallas kernels for 0%

commit v1 on v0

--- a/solution.py
+++ b/solution.py
@@ -1,8 +1,11 @@
+import functools
 import math
 
 import jax
 import jax.numpy as jnp
 from jax import lax
+from jax.experimental import pallas as pl
+from jax.experimental.pallas import tpu as pltpu
 from jax.sharding import PartitionSpec as P
 
 GROUPS = 4
@@ -11,6 +14,456 @@
 norm_eps = 1e-06
 group_eps = 0.00064
 unit_eps = 1e-06
+
+f32 = jnp.float32
+bf16 = jnp.bfloat16
+
+
+def full(shape):
+    return pl.BlockSpec(shape, lambda *_: (0,) * len(shape))
+
+
+def rms_rows(values, gain):
+    scale = lax.rsqrt(jnp.mean(values * values, axis=-1, keepdims=True) + norm_eps)
+    return (values * scale * gain).astype(bf16)
+
+
+def split_dot(values, selector):
+    high = values.astype(bf16)
+    low = (values - high.astype(f32)).astype(bf16)
+    return jnp.dot(high, selector, preferred_element_type=f32) + jnp.dot(
+        low, selector, preferred_element_type=f32
+    )
+
+
+def project_kernel(chips, where_ref, *refs):
+    rows_refs, gain_ref, weight_ref, out_ref = refs[:-3], refs[-3], refs[-2], refs[-1]
+    plane, place = where_ref[0], where_ref[1]
+    for kp, rows_ref in enumerate(rows_refs):
+        normed = rms_rows(rows_ref[...].astype(f32), gain_ref[...])
+        result = jnp.dot(normed, weight_ref[...], preferred_element_type=f32).astype(bf16)
+        seqs = result.shape[0] // GROUPS
+        for kz in range(GROUPS):
+            chip = (plane ^ kz) * chips + (place ^ kp)
+            out_ref[pl.ds(pl.multiple_of(chip * seqs, seqs), seqs), :] = result[
+                kz * seqs : (kz + 1) * seqs
+            ]
+
+
+def state_kernel(
+    channel,
+    key_ref,
+    query_ref,
+    value_ref,
+    decay_ref,
+    rate_ref,
+    erase_ref,
+    substitute_ref,
+    extra_ref,
+    attend_ref,
+    state_ref,
+    new_ref,
+    mixed_ref,
+    erase2,
+    write2,
+    replace2,
+    query2,
+    decay2,
+    readout,
+):
+    step = pl.program_id(0)
+    seqs, heads, width = state_ref.shape
+    rows = seqs * heads
+    span = 256
+
+    def flat(x):
+        return x.astype(f32).reshape(rows, channel)
+
+    def twice(x):
+        return jnp.concatenate([x, x], axis=-1)
+
+    @pl.when(step == 0)
+    def _():
+        key = flat(key_ref[...])
+        rate = flat(rate_ref[...])
+        erase = (key.reshape(seqs, heads, channel) * erase_ref[...][None]).reshape(rows, channel)
+        erase = erase * lax.rsqrt(jnp.sum(erase * erase, axis=-1, keepdims=True) + unit_eps)
+        gain = jnp.broadcast_to(substitute_ref[...][None], (seqs, heads, channel)).reshape(
+            rows, channel
+        )
+        replace = key * (1.0 + (rate - 1.0) * gain)
+        erase2[...] = twice(erase)
+        write2[...] = twice(erase * rate)
+        replace2[...] = twice(replace)
+        query2[...] = twice(flat(query_ref[...]))
+        decay2[...] = twice(flat(decay_ref[...]))
+        readout[...] = jnp.zeros_like(readout)
+
+    def wide(ref):
+        return jnp.concatenate([ref[...]] * (span // (2 * channel)), axis=-1)
+
+    across = lax.broadcasted_iota(jnp.int32, (span, span), 0) // channel
+    down = lax.broadcasted_iota(jnp.int32, (span, span), 1) // channel
+    block_ones = (across == down).astype(f32).astype(bf16)
+    value = value_ref[...].reshape(rows, channel)
+    for part in range(width // span):
+        lanes = slice(part * span, (part + 1) * span)
+        first = (step * width + part * span) // channel
+        spread = (
+            (
+                lax.broadcasted_iota(jnp.int32, (channel, span), 0)
+                == lax.broadcasted_iota(jnp.int32, (channel, span), 1) // channel + first
+            )
+            .astype(f32)
+            .astype(bf16)
+        )
+        collect = (
+            (
+                lax.broadcasted_iota(jnp.int32, (span, channel), 0) // channel + first
+                == lax.broadcasted_iota(jnp.int32, (span, channel), 1)
+            )
+            .astype(f32)
+            .astype(bf16)
+        )
+        memory = state_ref[:, :, lanes].reshape(rows, span)
+        removed = split_dot(memory * wide(erase2), block_ones)
+        value_wide = jnp.dot(value, spread, preferred_element_type=f32)
+        memory = (
+            memory * wide(decay2) - removed * wide(write2) + value_wide * wide(replace2)
+        )
+        new_ref[:, :, lanes] = memory.reshape(seqs, heads, span)
+        readout[...] += split_dot(memory * wide(query2), collect)
+
+    @pl.when(step == pl.num_programs(0) - 1)
+    def _():
+        result = readout[...]
+        centered = result - jnp.mean(result, axis=-1, keepdims=True)
+        variance = jnp.mean(centered * centered, axis=-1, keepdims=True)
+        gain = jnp.broadcast_to(attend_ref[...][None], (seqs, heads, channel)).reshape(
+            rows, channel
+        )
+        extra = jnp.broadcast_to(extra_ref[...][None], (seqs, heads, channel)).reshape(
+            rows, channel
+        )
+        bonus = jnp.sum(
+            query2[:, :channel] * replace2[:, :channel] * extra, axis=-1, keepdims=True
+        )
+        mixed = centered * lax.rsqrt(variance + group_eps) * gain + bonus * value.astype(f32)
+        mixed_ref[...] = mixed.astype(bf16).reshape(seqs, heads, channel)
+
+
+def output_kernel(where_ref, mixed_ref, own_ref, near_ref, far_ref, out_ref):
+    place, core = where_ref[1], where_ref[2]
+    depth, columns = own_ref.shape
+    half = depth // 2
+    mixed = mixed_ref[:, :depth]
+    near = mixed_ref[:, pl.ds(pl.multiple_of(core * half, half), half)]
+    far = mixed_ref[:, pl.ds(pl.multiple_of((1 - core) * half, half), half)]
+    for kp in range(near_ref.shape[0] + 1):
+        if kp == 0:
+            result = jnp.dot(mixed, own_ref[...], preferred_element_type=f32)
+        else:
+            result = jnp.dot(near, near_ref[kp - 1], preferred_element_type=f32) + jnp.dot(
+                far, far_ref[kp - 1], preferred_element_type=f32
+            )
+        at = pl.multiple_of((place ^ kp) * columns, columns)
+        out_ref[:, pl.ds(at, columns)] = result.astype(bf16)
+
+
+def residual_kernel(
+    where_ref, *refs
+):
+    parts, (rows_ref, tail_ref, gain_ref, pick_ref, chosen_ref, own_ref, held) = (
+        refs[:GROUPS],
+        refs[GROUPS:],
+    )
+    plane = where_ref[0]
+    seqs = rows_ref.shape[0] // GROUPS
+    width = rows_ref.shape[1]
+    columns = width // GROUPS
+    for k, part_ref in enumerate(parts):
+        at = pl.multiple_of((plane ^ k) * columns, columns)
+        for j in range(GROUPS):
+            mine = slice((k ^ j) * seqs, ((k ^ j) + 1) * seqs)
+            held[mine, pl.ds(at, columns)] = rows_ref[mine, pl.ds(at, columns)].astype(
+                f32
+            ) + part_ref[j * seqs : (j + 1) * seqs, :].astype(f32)
+    residual = held[...].astype(bf16)
+    own_ref[...] = residual[:seqs]
+    second = rms_rows(residual.astype(f32), gain_ref[...])
+    pick = pick_ref[...]
+    chosen_ref[:, :width] = jnp.dot(pick, second, preferred_element_type=f32).astype(bf16)
+    chosen_ref[:, width:] = jnp.dot(pick, tail_ref[...], preferred_element_type=f32).astype(bf16)
+
+
+def expert_kernel(
+    members, where_ref, own_ref, other_ref, switch_ref, widen_ref, shrink_ref, mine_ref, theirs_ref, total
+):
+    step = pl.program_id(0)
+    width = switch_ref.shape[0]
+    count = own_ref.shape[0]
+
+    @pl.when(step == 0)
+    def _():
+        total[...] = jnp.zeros_like(total)
+
+    rows = jnp.concatenate([own_ref[:, :width], other_ref[:, :width]], axis=0)
+    gate = jnp.dot(rows, switch_ref[...], preferred_element_type=f32)
+    up = jnp.dot(rows, widen_ref[...], preferred_element_type=f32)
+    hidden = (gate * jax.nn.sigmoid(gate) * up).astype(bf16)
+    total[...] += jnp.dot(hidden, shrink_ref[...], preferred_element_type=f32)
+
+    @pl.when(step == pl.num_programs(0) - 1)
+    def _():
+        member = where_ref[3]
+        for ref, out_ref, start in ((own_ref, mine_ref, 0), (other_ref, theirs_ref, count)):
+            tail = ref[:, width:].astype(f32)
+            lane = lax.broadcasted_iota(jnp.int32, tail.shape, 1)
+            share = jnp.sum(
+                jnp.where((lane == member) | (lane == member + members), tail, 0.0),
+                axis=-1,
+                keepdims=True,
+            )
+            out_ref[...] = (total[start : start + count, :] * share).astype(bf16)
+
+
+def swap(rows, mask):
+    count = lax.axis_size("ep")
+    return lax.ppermute(rows, "ep", [(i, i ^ mask) for i in range(count)])
+
+
+def layered(
+    latest_embeddings,
+    prior_memory_grids,
+    earlier_rescale_gain,
+    query_map,
+    lookup_map,
+    content_map,
+    forget_lower_map,
+    forget_upper_map,
+    forget_shift,
+    adapt_lower_map,
+    adapt_upper_map,
+    adapt_shift,
+    erase_lookup_gains,
+    substitute_lookup_gains,
+    present_extra_gains,
+    attender_rescale_gain,
+    result_map,
+    later_rescale_gain,
+    specialist_switch_maps,
+    specialist_widen_maps,
+    specialist_shrink_maps,
+    picked_specialists,
+    specialist_picked_shares,
+):
+    seqs, width = latest_embeddings.shape
+    heads = prior_memory_grids.shape[1]
+    channel = width // heads
+    devices = lax.axis_size("ep")
+    members = devices // GROUPS
+    chips = members // 2
+    columns = query_map.shape[1]
+    me = lax.axis_index("ep").astype(jnp.int32)
+    core, place, plane = me % 2, (me // 2) % chips, me // members
+    where = jnp.stack([plane, place, core, me % members])
+    smem = pl.BlockSpec(memory_space=pltpu.SMEM)
+    vmem = pl.BlockSpec(memory_space=pltpu.VMEM)
+    same_core = [[2 * i + c for i in range(devices // 2)] for c in range(2)]
+    same_plane = [
+        [members * z + 2 * i + c for i in range(chips)] for z in range(GROUPS) for c in range(2)
+    ]
+
+    line = [latest_embeddings] + [swap(latest_embeddings, members * k) for k in range(1, GROUPS)]
+    line_rows = jnp.concatenate(line, axis=0)
+    gathered = [line_rows] + [swap(line_rows, 2 * k) for k in range(1, chips)]
+
+    stacked = jnp.concatenate([query_map, lookup_map, content_map, result_map], axis=1)
+    paired = swap(stacked, 1)
+    lower = jnp.where(core == 0, stacked, paired)
+    upper = jnp.where(core == 0, paired, stacked)
+    chip_maps = jnp.stack(
+        [lower.reshape(width, 4, columns), upper.reshape(width, 4, columns)], axis=2
+    ).reshape(width, 4 * 2 * columns)
+    project_maps = chip_maps[:, : 3 * 2 * columns]
+    output_map = chip_maps[:, 3 * 2 * columns :]
+
+    normed = rms_rows(latest_embeddings.astype(f32), earlier_rescale_gain)
+    decay_low = jnp.tanh(
+        jnp.dot(normed, forget_lower_map, preferred_element_type=f32)
+    ).astype(bf16)
+    decay = jnp.exp(
+        -math.exp(-0.5)
+        * jax.nn.sigmoid(
+            forget_shift + jnp.dot(decay_low, forget_upper_map, preferred_element_type=f32)
+        )
+    ).reshape(seqs, heads, channel)
+    rate_low = jnp.dot(normed, adapt_lower_map, preferred_element_type=f32).astype(bf16)
+    rate = jax.nn.sigmoid(
+        adapt_shift + jnp.dot(rate_low, adapt_upper_map, preferred_element_type=f32)
+    ).reshape(seqs, heads, channel)
+
+    top_count = picked_specialists.shape[1]
+    group = picked_specialists[:, 0] // members
+    share_at = (
+        picked_specialists[:, :, None] % members == jnp.arange(members, dtype=jnp.int32)
+    ).astype(f32)
+    shares = jnp.sum(share_at * specialist_picked_shares[:, :, None], axis=1)
+    share_high = shares.astype(bf16)
+    share_low = (shares - share_high.astype(f32)).astype(bf16)
+    tail_width = -(-(2 * members + 1) // 128) * 128
+    tail = jnp.concatenate(
+        [
+            share_high,
+            share_low,
+            group[:, None].astype(bf16),
+            jnp.zeros((seqs, tail_width - 2 * members - 1), bf16),
+        ],
+        axis=1,
+    )
+
+    all_rows = seqs * GROUPS * chips
+    projected = pl.pallas_call(
+        functools.partial(project_kernel, chips),
+        out_shape=jax.ShapeDtypeStruct((all_rows, 6 * columns), bf16),
+        in_specs=[smem] + [vmem] * (chips + 2),
+        out_specs=vmem,
+        name="project",
+    )(where, *gathered, earlier_rescale_gain.reshape(1, width), project_maps)
+    arrived = lax.all_to_all(
+        projected, "ep", split_axis=0, concat_axis=0, tiled=True, axis_index_groups=same_core
+    )
+    signals = (
+        arrived.reshape(devices // 2, seqs, 3, heads * 2 // devices, channel)
+        .transpose(2, 1, 0, 3, 4)
+        .reshape(3, seqs, heads, channel)
+    )
+
+    half = lax.dynamic_slice_in_dim(output_map, core * (width // 2), width // 2, axis=0)
+    half, projected_done = lax.optimization_barrier((half, projected))
+    near = jnp.stack([swap(half, 2 * k) for k in range(1, chips)])
+    far = swap(near, 1)
+
+    lanes = 512
+    small = pl.BlockSpec((seqs, heads, channel), lambda i: (0, 0, 0))
+    gains = pl.BlockSpec((heads, channel), lambda i: (0, 0))
+    block = pl.BlockSpec((seqs, heads, lanes), lambda i: (0, 0, i))
+    tile = pltpu.VMEM((seqs * heads, 2 * channel), f32)
+    new_state, mixed = pl.pallas_call(
+        functools.partial(state_kernel, channel),
+        grid=(channel * channel // lanes,),
+        out_shape=[
+            jax.ShapeDtypeStruct(prior_memory_grids.shape, f32),
+            jax.ShapeDtypeStruct((seqs, heads, channel), bf16),
+        ],
+        in_specs=[small] * 5 + [gains] * 4 + [block],
+        out_specs=[block, small],
+        scratch_shapes=[tile] * 5 + [pltpu.VMEM((seqs * heads, channel), f32)],
+        compiler_params=pltpu.CompilerParams(
+            dimension_semantics=("arbitrary",), vmem_limit_bytes=48 * 2**20
+        ),
+        name="state",
+    )(
+        signals[1],
+        signals[0],
+        signals[2],
+        decay,
+        rate,
+        erase_lookup_gains.reshape(heads, channel),
+        substitute_lookup_gains.reshape(heads, channel),
+        present_extra_gains.reshape(heads, channel),
+        attender_rescale_gain.reshape(heads, channel),
+        prior_memory_grids,
+    )
+
+    mixed_rows = jnp.concatenate([mixed.reshape(seqs, width), tail], axis=1)
+    mixed_line = jnp.concatenate(
+        [mixed_rows] + [swap(mixed_rows, members * k) for k in range(1, GROUPS)], axis=0
+    )
+    line_columns = pl.pallas_call(
+        output_kernel,
+        out_shape=jax.ShapeDtypeStruct((GROUPS * seqs, width // GROUPS), bf16),
+        in_specs=[smem] + [vmem] * 4,
+        out_specs=vmem,
+        name="output",
+    )(where, mixed_line, output_map, near, far)
+    parts = [line_columns] + [swap(line_columns, members * k) for k in range(1, GROUPS)]
+
+    room = (seqs + 1) // 2
+    line_tail = mixed_line[:, width:]
+    line_group = line_tail[:, 2 * members].reshape(GROUPS, seqs)
+    wanted = (line_group == plane.astype(bf16)).astype(jnp.int32)
+    rank = jnp.cumsum(wanted, axis=1) - wanted
+    pick = (
+        (wanted[:, None, :] == 1)
+        & (rank[:, None, :] == jnp.arange(room, dtype=jnp.int32)[None, :, None])
+    ).astype(bf16)
+    pick = (
+        pick[:, :, None, :] * jnp.eye(GROUPS, dtype=bf16)[:, None, :, None]
+    ).reshape(GROUPS * room, GROUPS * seqs)
+    chosen, residual = pl.pallas_call(
+        residual_kernel,
+        out_shape=[
+            jax.ShapeDtypeStruct((GROUPS * room, width + tail_width), bf16),
+            jax.ShapeDtypeStruct((seqs, width), bf16),
+        ],
+        in_specs=[smem] + [vmem] * (GROUPS + 4),
+        out_specs=[vmem] * 2,
+        scratch_shapes=[pltpu.VMEM((GROUPS * seqs, width), f32)],
+        name="residual",
+    )(where, *parts, line_rows, line_tail, later_rescale_gain.reshape(1, width), pick)
+
+    own_rows = lax.all_gather(chosen, "ep", axis=0, tiled=True, axis_index_groups=same_plane)
+    other_rows = swap(own_rows, 1)
+    hidden = specialist_switch_maps.shape[2]
+    piece = hidden // 2
+    count = own_rows.shape[0]
+    mine, theirs = pl.pallas_call(
+        functools.partial(expert_kernel, members),
+        grid=(hidden // piece,),
+        out_shape=[jax.ShapeDtypeStruct((count, width), bf16)] * 2,
+        in_specs=[
+            smem,
+            full(own_rows.shape),
+            full(own_rows.shape),
+            pl.BlockSpec((None, width, piece), lambda i: (0, 0, i)),
+            pl.BlockSpec((None, width, piece), lambda i: (0, 0, i)),
+            pl.BlockSpec((None, piece, width), lambda i: (0, i, 0)),
+        ],
+        out_specs=[full((count, width))] * 2,
+        scratch_shapes=[pltpu.VMEM((2 * count, width), f32)],
+        compiler_params=pltpu.CompilerParams(
+            dimension_semantics=("arbitrary",), vmem_limit_bytes=48 * 2**20
+        ),
+        name="expert",
+    )(
+        where,
+        own_rows,
+        other_rows,
+        specialist_switch_maps,
+        specialist_widen_maps,
+        specialist_shrink_maps,
+    )
+
+    both = (mine.astype(f32) + swap(theirs, 1).astype(f32)).astype(bf16)
+    spread = lax.all_to_all(
+        both, "ep", split_axis=0, concat_axis=0, tiled=True, axis_index_groups=same_plane
+    )
+    summed = jnp.sum(
+        spread.reshape(chips, GROUPS, room, width).astype(f32), axis=0
+    ).astype(bf16)
+    home = jnp.concatenate(
+        [summed[0]] + [swap(summed[k], members * k) for k in range(1, GROUPS)], axis=0
+    )
+    own_rank = jnp.sum(
+        (group[None, :] == group[:, None]) & (jnp.arange(seqs)[None, :] < jnp.arange(seqs)[:, None]),
+        axis=1,
+    ).astype(jnp.int32)
+    slot = (group ^ plane) * room + own_rank
+    fetch = (slot[:, None] == jnp.arange(GROUPS * room, dtype=jnp.int32)[None, :]).astype(bf16)
+    expert_sum = jnp.dot(fetch, home, preferred_element_type=f32)
+    new_hidden = (residual.astype(f32) + expert_sum).astype(bf16)
+    return (new_hidden, new_state)
 
 
 def rms_norm(rows_in, gain):
@@ -177,9 +630,16 @@
     return (new_hidden, new_state)
 
 
+def step(*args):
+    devices, columns = lax.axis_size("ep"), args[3].shape[1]
+    if devices % (2 * GROUPS) == 0 and (2 * columns) % 128 == 0 and args[18].shape[0] == 1:
+        return layered(*args)
+    return local(*args)
+
+
 def solution(mesh):
     return jax.shard_map(
-        local,
+        step,
         mesh=mesh,
         in_specs=(
             P("ep", None),

time: 345 us -> 128 us (0.37)
  waiting for transfers between devices: 113 us -> 21.4 us
  local copies, waits for them, and re-layouts: 81.3 us -> 16.3 us
  matrix products: 65.2 us -> 4.12 us
  other arithmetic: 41.3 us -> 3.82 us
  Pallas kernels: 0 us -> 26.1 us
  blocking collectives: 0 us -> 21.7 us
  between operations: 14.5 us -> 1.19 us
  starting transfers between devices: 27.3 us -> 32.8 us
    all_gather x2 -> x0, waiting for transfers between devices: 88.8 us -> none  [the longest x1 58.1 us: local(): lax.all_gather(normed, 'ep', axis=0, tiled=True)]
    dot_general x10 -> x3, matrix products: 65.2 us -> 4.12 us  [the longest x1 2.17 us: layered(): jnp.dot(decay_low, forget_upper_map, preferred_element_type=f32)]
    mul x10 -> x1, local copies, waits for them, and re-layouts: 54.7 us -> 0.68 us  [layered(): pick[:, :, None, :] * jnp.eye(GROUPS, dtype=bf16)[:, None, :, None]]
    ppermute x0 -> x22, starting transfers between devices: none -> 26.5 us  [swap(): return lax.ppermute(rows, 'ep', [(i, i ^ mask) for i in range(count)])]
    pallas_call x0 -> x5, Pallas kernels: none -> 26.1 us  [the longest x1 13.4 us: layered(): pl.pallas_call(functools.partial(state_kernel, channel), grid=(channel *...]
    all_to_all x6 -> x1, waiting for transfers between devices: 23.8 us -> 2.43 us  [layered(): lax.all_to_all(projected, 'ep', split_axis=0, concat_axis=0, tiled=True,...]
    all_to_all x6 -> x1, starting transfers between devices: 27.1 us -> 6.34 us  [layered(): lax.all_to_all(projected, 'ep', split_axis=0, concat_axis=0, tiled=True,...]
    mul x4 -> x1, other arithmetic: 20.6 us -> 0.08 us  [layered(): pick[:, :, None, :] * jnp.eye(GROUPS, dtype=bf16)[:, None, :, None]]
  transfers between devices with their start and end apart: 8 -> 23, of which waited for: 5 -> 12; matrix products, arithmetic and copies ran while one was open for 41% -> 17% of each run, Pallas kernels for 0% -> 11%
where the time goes in v1:
time: 128 us; the launch traced here: 127 us
  starting transfers between devices  32.8 us (26%)
  Pallas kernels  26.1 us (20%)
  blocking collectives  21.7 us (17%)
  waiting for transfers between devices  21.4 us (17%)
  local copies, waits for them, and re-layouts  16.3 us (13%)
  matrix products  4.12 us (3%)
  other arithmetic  3.82 us (3%)
    ppermute x22, starting transfers between devices, swap(): return lax.ppermute(rows, 'ep', [(i, i ^ mask) for i in range(count)])  26.5 us
    ppermute x22, waiting for transfers between devices, swap(): return lax.ppermute(rows, 'ep', [(i, i ^ mask) for i in range(count)])  18.9 us
    pallas_call x1, Pallas kernels, layered(): pl.pallas_call(functools.partial(state_kernel, channel), grid=(channel *...  13.4 us
    all_to_all x1, blocking collectives, layered(): lax.all_to_all(both, 'ep', split_axis=0, concat_axis=0, tiled=True, axis_...  11.5 us
    all_gather x1, blocking collectives, layered(): lax.all_gather(chosen, 'ep', axis=0, tiled=True, axis_index_groups=same_p...  10.2 us
    unnamed x57, local copies, waits for them, and re-layouts  7.35 us
    all_to_all x1, starting transfers between devices, layered(): lax.all_to_all(projected, 'ep', split_axis=0, concat_axis=0, tiled=True,...  6.34 us
    pallas_call x1, Pallas kernels, layered(): pl.pallas_call(functools.partial(expert_kernel, members), grid=(hidden //...  4.15 us
  transfers between devices with their start and end apart: 23, of which 12 were waited for; matrix products, arithmetic and copies ran while one was open for 17% of the time, Pallas kernels for 11%

profile of v1, /device:TPU:0, one launch (start us, length us, event | category | flops | bytes accessed | tf_op | source)
XLA Modules:
  0.0 127.4 jit_solution(3985953366638851085)
XLA Ops:
  0.7 5.1 %collective-permute-start.2 = (bf16[16,2048]{1,0:T(8,128)(2,1)}, bf16[16,2048]{1,0:T(8,128)(2,1)S(1)}, u32[]{:S(2)}, u32[]{:S(2)}) collective-permute-start(bf16[16,2048]{1,0:T(8,128)(2,1)} %param.23), channel_id=1, source_target_pairs={{0,24},{1,25},{2,26},{3,27},{4,28},{5,29},{6,30},{7,31},{8,16},{9,... | collective-permute-start | bytes 196616 | tf_op jit(solution)/shard_map/ppermute | solution.py:232
  11.4 1.1 fusion.3
  12.7 2.2 %fusion.9 = f32[16,2048]{1,0:T(8,128)} fusion(bf16[64,2048]{1,0:T(8,128)(2,1)} %param.30, bf16[2048,64]{0,1:T(8,128)(2,1)} %param.29, f32[2048]{0:T(1024)S(1)} %copy-done.23, bf16[16,2048]{1,0:T(8,128)(2,1)S(1)} %copy-done.9, f32[2048]{0:T(1024)S(1)} %copy-done.13, f32[16]{0:T(128)S(1)} %add_rsqrt_fusion), kind=kOutput, calls=%fused_computation.11 | convolution fusion | flops 8684544 | bytes 737344 | tf_op jit(solution)/shard_map/dot_general | solution.py:298
  15.6 2.7 %collective-permute-start.5 = (bf16[64,2048]{1,0:T(8,128)(2,1)S(1)}, bf16[64,2048]{1,0:T(8,128)(2,1)S(1)}, u32[]{:S(2)}, u32[]{:S(2)}) collective-permute-start(bf16[64,2048]{1,0:T(8,128)(2,1)S(1)} %constant_dynamic-update-slice_fusion.refs_0_.refs_4_), channel_id=1, source_target_pairs={{0,6},{1,7},{2,4},{3,5},{4,2},{5,3},{6,0},{7,1},{8,14},{9,15},{10,... | collective-permute-start | bytes 786440 | tf_op jit(solution)/shard_map/ppermute | solution.py:232
  19.5 1.2 slice.56
  20.7 2.6 %copy.59.refs_5_ = bf16[2048,384]{1,0:T(8,128)(2,1)} copy(bf16[2048,384]{0,1:T(8,128)(2,1)} %slice.56) | data formatting | bytes 3145728
  23.4 2.4 %collective-permute-done.5.refs_3_ = bf16[64,2048]{1,0:T(8,128)(2,1)S(1)} collective-permute-done((bf16[64,2048]{1,0:T(8,128)(2,1)S(1)}, bf16[64,2048]{1,0:T(8,128)(2,1)S(1)}, u32[]{:S(2)}, u32[]{:S(2)}) %collective-permute-start.5) | collective-permute-done | bytes 262176 | tf_op jit(solution)/shard_map/ppermute | solution.py:232
  25.8 5.1 %collective-permute-done.4.refs_2_ = bf16[64,2048]{1,0:T(8,128)(2,1)S(1)} collective-permute-done((bf16[64,2048]{1,0:T(8,128)(2,1)S(1)}, bf16[64,2048]{1,0:T(8,128)(2,1)S(1)}, u32[]{:S(2)}, u32[]{:S(2)}) %collective-permute-start.4) | collective-permute-done | bytes 262176 | tf_op jit(solution)/shard_map/ppermute | solution.py:232
  31.8 3.7 %project.1 = bf16[256,384]{1,0:T(8,128)(2,1)} custom-call(s32[4]{0:T(128)} %pad_add_fusion.where_ref, bf16[64,2048]{1,0:T(8,128)(2,1)} %copy-done.5, bf16[64,2048]{1,0:T(8,128)(2,1)} %copy-done.8, bf16[64,2048]{1,0:T(8,128)(2,1)} %copy-done.7, bf16[64,2048]{1,0:T(8,128)(2,1)} %copy-done.6, f32[1,2048]{1,0:T(1,128)} %bitcast.44, bf16[2048,384]{1,0:T(8,128)(2,1)} %copy.59.refs_5_), custom_call_target="tpu_custom_call" | custom-call | tf_op jit(solution)/shard_map/project/pallas_call | solution.py:326
  35.5 6.3 %all-to-all-start = ((bf16[16,16,384]{2,1,0:T(8,128)(2,1)}), bf16[16,16,384]{2,1,0:T(8,128)(2,1)}, u32[]{:S(2)}, u32[]{:S(2)}) async-start(bf16[16,16,384]{2,1,0:T(8,128)(2,1)} %bitcast.40), calls=%async_computation | async-start | bytes 393216 | tf_op jit(solution)/shard_map/all_to_all | solution.py:333
  42.2 2.8 %collective-permute-start.12 = (bf16[1024,128]{1,0:T(8,128)(2,1)S(1)}, bf16[1024,128]{1,0:T(8,128)(2,1)S(1)}, u32[]{:S(2)}, u32[]{:S(2)}) collective-permute-start(bf16[1024,128]{1,0:T(8,128)(2,1)S(1)} %constant_dynamic-slice_fusion), channel_id=1, source_target_pairs={{0,6},{1,7},{2,4},{3,5},{4,2},{5,3},{6,0},{7,1},{8,14},{9,15},{10,... | collective-permute-start | bytes 786440 | tf_op jit(solution)/shard_map/ppermute | solution.py:232
  48.1 2.4 %all-to-all-done = bf16[16,16,384]{2,1,0:T(8,128)(2,1)} async-done(((bf16[16,16,384]{2,1,0:T(8,128)(2,1)}), bf16[16,16,384]{2,1,0:T(8,128)(2,1)}, u32[]{:S(2)}, u32[]{:S(2)}) %all-to-all-start) | async-done | bytes 196640 | tf_op jit(solution)/shard_map/all_to_all | solution.py:333
  50.6 1.2 reshape.155
  52.3 13.4 %state.1 = (f32[16,32,4096]{2,1,0:T(8,128)}, bf16[16,32,64]{2,1,0:T(8,128)(2,1)S(1)}) custom-call(bf16[16,32,64]{2,1,0:T(8,128)(2,1)S(1)} %bitcast.33, bf16[16,32,64]{2,1,0:T(8,128)(2,1)S(1)} %bitcast.32, bf16[16,32,64]{2,1,0:T(8,128)(2,1)S(1)} %bitcast.31, f32[16,32,64]{2,1,0:T(8,128)S(1)} %reshape.156.decay_ref, f32[16,32,64]{2,1,0:T(8,128)S(1)} %reshape.157.rate_ref, ...), custom_call_target="tpu_custom_call" | custom-call | tf_op jit(solution)/shard_map/state/pallas_call | solution.py:352
  66.0 1.7 %collective-permute-start.9 = (bf16[16,2176]{1,0:T(8,128)(2,1)S(1)}, bf16[16,2176]{1,0:T(8,128)(2,1)S(1)}, u32[]{:S(2)}, u32[]{:S(2)}) collective-permute-start(bf16[16,2176]{1,0:T(8,128)(2,1)S(1)} %concatenate.17), channel_id=1, source_target_pairs={{0,24},{1,25},{2,26},{3,27},{4,28},{5,29},{6,30},{7,31},{8,16},{9,... | collective-permute-start | bytes 208904 | tf_op jit(solution)/shard_map/ppermute | solution.py:232
  68.4 2.0 %collective-permute-start.7 = (bf16[16,2176]{1,0:T(8,128)(2,1)S(1)}, bf16[16,2176]{1,0:T(8,128)(2,1)S(1)}, u32[]{:S(2)}, u32[]{:S(2)}) collective-permute-start(bf16[16,2176]{1,0:T(8,128)(2,1)S(1)} %concatenate.17), channel_id=1, source_target_pairs={{0,8},{1,9},{2,10},{3,11},{4,12},{5,13},{6,14},{7,15},{8,0},{9,1},... | collective-permute-start | bytes 208904 | tf_op jit(solution)/shard_map/ppermute | solution.py:232
  70.7 2.3 %collective-permute-done.9 = bf16[16,2176]{1,0:T(8,128)(2,1)S(1)} collective-permute-done((bf16[16,2176]{1,0:T(8,128)(2,1)S(1)}, bf16[16,2176]{1,0:T(8,128)(2,1)S(1)}, u32[]{:S(2)}, u32[]{:S(2)}) %collective-permute-start.9) | collective-permute-done | bytes 69664 | tf_op jit(solution)/shard_map/ppermute | solution.py:232
  73.0 1.0 collective-permute-done.8
  76.0 2.7 %output.1.refs_0_ = bf16[64,512]{1,0:T(8,128)(2,1)} custom-call(s32[4]{0:T(128)} %pad_add_fusion.where_ref, bf16[64,2176]{1,0:T(8,128)(2,1)} %pad_maximum_fusion.2.mixed_ref, bf16[2048,128]{1,0:T(8,128)(2,1)} %copy-done.3, bf16[3,1024,128]{2,1,0:T(8,128)(2,1)} %copy-done.4, bf16[3,1024,128]{2,1,0:T(8,128)(2,1)} %collective-permute-done.13.far_ref), custom_call_target="tpu_custom_call" | custom-call | tf_op jit(solution)/shard_map/output/pallas_call | solution.py:383
  78.7 2.2 %collective-permute-start.16 = (bf16[64,512]{1,0:T(8,128)(2,1)}, bf16[64,512]{1,0:T(8,128)(2,1)S(1)}, u32[]{:S(2)}, u32[]{:S(2)}) collective-permute-start(bf16[64,512]{1,0:T(8,128)(2,1)} %output.1.refs_0_), channel_id=1, source_target_pairs={{0,24},{1,25},{2,26},{3,27},{4,28},{5,29},{6,30},{7,31},{8,16},{9,... | collective-permute-start | bytes 196616 | tf_op jit(solution)/shard_map/ppermute | solution.py:232
  80.9 2.2 %collective-permute-start.14 = (bf16[64,512]{1,0:T(8,128)(2,1)}, bf16[64,512]{1,0:T(8,128)(2,1)S(1)}, u32[]{:S(2)}, u32[]{:S(2)}) collective-permute-start(bf16[64,512]{1,0:T(8,128)(2,1)} %output.1.refs_0_), channel_id=1, source_target_pairs={{0,8},{1,9},{2,10},{3,11},{4,12},{5,13},{6,14},{7,15},{8,0},{9,1},... | collective-permute-start | bytes 196616 | tf_op jit(solution)/shard_map/ppermute | solution.py:232
  83.2 1.3 %slice.61.refs_5_ = bf16[64,128]{1,0:T(8,128)(2,1)} slice(bf16[64,2176]{1,0:T(8,128)(2,1)} %pad_maximum_fusion.2.mixed_ref), slice={[0:64], [2048:2176]} | slice | bytes 32768 | tf_op jit(solution)/shard_map/slice | solution.py:393
  85.7 1.3 %collective-permute-done.15.refs_2_ = bf16[64,512]{1,0:T(8,128)(2,1)S(1)} collective-permute-done((bf16[64,512]{1,0:T(8,128)(2,1)}, bf16[64,512]{1,0:T(8,128)(2,1)S(1)}, u32[]{:S(2)}, u32[]{:S(2)}) %collective-permute-start.15) | collective-permute-done | bytes 65568 | tf_op jit(solution)/shard_map/ppermute | solution.py:232
  87.7 2.1 %residual.1 = (bf16[32,2176]{1,0:T(8,128)(2,1)}, bf16[16,2048]{1,0:T(8,128)(2,1)}) custom-call(s32[4]{0:T(128)} %pad_add_fusion.where_ref, bf16[64,512]{1,0:T(8,128)(2,1)} %output.1.refs_0_, bf16[64,512]{1,0:T(8,128)(2,1)} %copy-done.12, bf16[64,512]{1,0:T(8,128)(2,1)} %copy-done.11, bf16[64,512]{1,0:T(8,128)(2,1)} %copy-done.10, ...), custom_call_target="tpu_custom_call" | custom-call | tf_op jit(solution)/shard_map/residual/pallas_call | solution.py:404
  89.8 10.2 %all_gather.3.own_ref = bf16[128,2176]{1,0:T(8,128)(2,1)S(1)} all-gather(bf16[32,2176]{1,0:T(8,128)(2,1)} %get-tuple-element.12), channel_id=1, replica_groups={{0,2,4,6},{1,3,5,7},{8,10,12,14},{9,11,13,15},{16,18,20,22},{17,19,21,2..., dimensions={0}, use_global_device_ids=true | all-gather | bytes 696320 | tf_op jit(solution)/shard_map/all_gather | solution.py:416
  100.0 2.0 %collective-permute-done.17.other_ref = bf16[128,2176]{1,0:T(8,128)(2,1)S(1)} collective-permute-done((bf16[128,2176]{1,0:T(8,128)(2,1)S(1)}, bf16[128,2176]{1,0:T(8,128)(2,1)S(1)}, u32[]{:S(2)}, u32[]{:S(2)}) %collective-permute-start.17) | collective-permute-done | bytes 557088 | tf_op jit(solution)/shard_map/ppermute | solution.py:232
  102.0 4.1 %expert.1 = (bf16[128,2048]{1,0:T(8,128)(2,1)S(1)}, bf16[128,2048]{1,0:T(8,128)(2,1)S(1)}) custom-call(s32[4]{0:T(128)S(1)} %copy-done.2, bf16[128,2176]{1,0:T(8,128)(2,1)S(1)} %all_gather.3.own_ref, bf16[128,2176]{1,0:T(8,128)(2,1)S(1)} %collective-permute-done.17.other_ref, bf16[1,2048,512]{2,1,0:T(8,128)(2,1)S(1)} %copy-done.1, ...), custom_call_target="tpu_custom_call" | custom-call | tf_op jit(solution)/shard_map/expert/pallas_call | solution.py:421
  106.3 1.8 %collective-permute-done.18 = bf16[128,2048]{1,0:T(8,128)(2,1)S(1)} collective-permute-done((bf16[128,2048]{1,0:T(8,128)(2,1)S(1)}, bf16[128,2048]{1,0:T(8,128)(2,1)S(1)}, u32[]{:S(2)}, u32[]{:S(2)}) %collective-permute-start.18) | collective-permute-done | bytes 524320 | tf_op jit(solution)/shard_map/ppermute | solution.py:232
  108.3 11.5 %all_to_all.18 = bf16[4,32,2048]{2,1,0:T(8,128)(2,1)S(1)} all-to-all(bf16[4,32,2048]{2,1,0:T(8,128)(2,1)S(1)} %bitcast.38), channel_id=1, replica_groups={{0,2,4,6},{1,3,5,7},{8,10,12,14},{9,11,13,15},{16,18,20,22},{17,19,21,2..., dimensions={0} | all-to-all | bytes 1048576 | tf_op jit(solution)/shard_map/all_to_all | solution.py:449
  119.9 1.8 %collective-permute-start.21 = (bf16[8,2048]{1,0:T(8,128)(2,1)S(1)}, bf16[8,2048]{1,0:T(8,128)(2,1)S(1)}, u32[]{:S(2)}, u32[]{:S(2)}) collective-permute-start(bf16[8,2048]{1,0:T(8,128)(2,1)S(1)} %get-tuple-element.22), channel_id=1, source_target_pairs={{0,24},{1,25},{2,26},{3,27},{4,28},{5,29},{6,30},{7,31},{8,16},{9,... | collective-permute-start | bytes 98312 | tf_op jit(solution)/shard_map/ppermute | solution.py:232
  122.0 2.4 %collective-permute-start.19 = (bf16[8,2048]{1,0:T(8,128)(2,1)S(1)}, bf16[8,2048]{1,0:T(8,128)(2,1)S(1)}, u32[]{:S(2)}, u32[]{:S(2)}) collective-permute-start(bf16[8,2048]{1,0:T(8,128)(2,1)S(1)} %get-tuple-element.24), channel_id=1, source_target_pairs={{0,8},{1,9},{2,10},{3,11},{4,12},{5,13},{6,14},{7,15},{8,0},{9,1},... | collective-permute-start | bytes 98312 | tf_op jit(solution)/shard_map/ppermute | solution.py:232
  124.3 1.3 %collective-permute-done.21 = bf16[8,2048]{1,0:T(8,128)(2,1)S(1)} collective-permute-done((bf16[8,2048]{1,0:T(8,128)(2,1)S(1)}, bf16[8,2048]{1,0:T(8,128)(2,1)S(1)}, u32[]{:S(2)}, u32[]{:S(2)}) %collective-permute-start.21) | collective-permute-done | bytes 32800 | tf_op jit(solution)/shard_map/ppermute | solution.py:232
  (133 shorter events, 19.9 us)
Async XLA Ops:
  0.6 10.7 %copy-start = (bf16[64,2048]{1,0:T(8,128)(2,1)S(1)}, bf16[64,2048]{1,0:T(8,128)(2,1)}, u32[]{:S(2)}) copy-start(bf16[64,2048]{1,0:T(8,128)(2,1)} %param.33) | copy-start | bytes 786436
  0.7 10.6 %copy-start.13 = (f32[2048]{0:T(1024)S(1)}, f32[2048]{0:T(1024)}, u32[]{:S(2)}) copy-start(f32[2048]{0:T(1024)} %param.25) | copy-start | bytes 24580
  0.7 10.6 %copy-start.22 = (f32[2048]{0:T(1024)S(1)}, f32[2048]{0:T(1024)}, u32[]{:S(2)}) copy-start(f32[2048]{0:T(1024)} %param.34) | copy-start | bytes 24580
  0.7 11.8 %copy-start.18 = (f32[16,6]{0,1:T(8,128)S(1)}, f32[16,6]{0,1:T(8,128)}, u32[]{:S(2)}) copy-start(f32[16,6]{0,1:T(8,128)} %param.45) | copy-start | bytes 1156
  0.7 12.0 %copy-start.23 = (f32[2048]{0:T(1024)S(1)}, f32[2048]{0:T(1024)}, u32[]{:S(2)}) copy-start(f32[2048]{0:T(1024)} %param.31) | copy-start | bytes 24580
  0.7 14.8 %collective-permute-start.2 = (bf16[16,2048]{1,0:T(8,128)(2,1)}, bf16[16,2048]{1,0:T(8,128)(2,1)S(1)}, u32[]{:S(2)}, u32[]{:S(2)}) collective-permute-start(bf16[16,2048]{1,0:T(8,128)(2,1)} %param.23), channel_id=1, source_target_pairs={{0,24},{1,25},{2,26},{3,27},{4,28},{5,29},{6,30},{7,31},{8,16},{9,... | collective-permute-start | bytes 196616 | tf_op jit(solution)/shard_map/ppermute | solution.py:232
  5.9 9.6 %collective-permute-start.1 = (bf16[16,2048]{1,0:T(8,128)(2,1)}, bf16[16,2048]{1,0:T(8,128)(2,1)S(1)}, u32[]{:S(2)}, u32[]{:S(2)}) collective-permute-start(bf16[16,2048]{1,0:T(8,128)(2,1)} %param.23), channel_id=1, source_target_pairs={{0,16},{1,17},{2,18},{3,19},{4,20},{5,21},{6,22},{7,23},{8,24},{9,... | collective-permute-start | bytes 196616 | tf_op jit(solution)/shard_map/ppermute | solution.py:232
  5.9 9.6 %collective-permute-start = (bf16[16,2048]{1,0:T(8,128)(2,1)}, bf16[16,2048]{1,0:T(8,128)(2,1)S(1)}, u32[]{:S(2)}, u32[]{:S(2)}) collective-permute-start(bf16[16,2048]{1,0:T(8,128)(2,1)} %param.23), channel_id=1, source_target_pairs={{0,8},{1,9},{2,10},{3,11},{4,12},{5,13},{6,14},{7,15},{8,0},{9,1},... | collective-permute-start | bytes 196616 | tf_op jit(solution)/shard_map/ppermute | solution.py:232
  10.4 8.7 %collective-permute-start.6 = (bf16[2048,256]{0,1:T(8,128)(2,1)S(1)}, bf16[2048,256]{0,1:T(8,128)(2,1)S(1)}, u32[]{:S(2)}, u32[]{:S(2)}) collective-permute-start(bf16[2048,256]{0,1:T(8,128)(2,1)S(1)} %constant_dynamic-update-slice_fusion.4), channel_id=1, source_target_pairs={{0,1},{1,0},{2,3},{3,2},{4,5},{5,4},{6,7},{7,6},{8,9},{9,8},{10,11... | collective-permute-start | bytes 3145736 | tf_op jit(solution)/shard_map/ppermute | solution.py:232
  15.6 10.2 %collective-permute-start.5 = (bf16[64,2048]{1,0:T(8,128)(2,1)S(1)}, bf16[64,2048]{1,0:T(8,128)(2,1)S(1)}, u32[]{:S(2)}, u32[]{:S(2)}) collective-permute-start(bf16[64,2048]{1,0:T(8,128)(2,1)S(1)} %constant_dynamic-update-slice_fusion.refs_0_.refs_4_), channel_id=1, source_target_pairs={{0,6},{1,7},{2,4},{3,5},{4,2},{5,3},{6,0},{7,1},{8,14},{9,15},{10,... | collective-permute-start | bytes 786440 | tf_op jit(solution)/shard_map/ppermute | solution.py:232
  18.2 12.6 %collective-permute-start.4 = (bf16[64,2048]{1,0:T(8,128)(2,1)S(1)}, bf16[64,2048]{1,0:T(8,128)(2,1)S(1)}, u32[]{:S(2)}, u32[]{:S(2)}) collective-permute-start(bf16[64,2048]{1,0:T(8,128)(2,1)S(1)} %constant_dynamic-update-slice_fusion.refs_0_.refs_4_), channel_id=1, source_target_pairs={{0,4},{1,5},{2,6},{3,7},{4,0},{5,1},{6,2},{7,3},{8,12},{9,13},{10,... | collective-permute-start | bytes 786440 | tf_op jit(solution)/shard_map/ppermute | solution.py:232
  18.7 12.4 %collective-permute-start.3 = (bf16[64,2048]{1,0:T(8,128)(2,1)S(1)}, bf16[64,2048]{1,0:T(8,128)(2,1)S(1)}, u32[]{:S(2)}, u32[]{:S(2)}) collective-permute-start(bf16[64,2048]{1,0:T(8,128)(2,1)S(1)} %constant_dynamic-update-slice_fusion.refs_0_.refs_4_), channel_id=1, source_target_pairs={{0,2},{1,3},{2,0},{3,1},{4,6},{5,7},{6,4},{7,5},{8,10},{9,11},{10,... | collective-permute-start | bytes 786440 | tf_op jit(solution)/shard_map/ppermute | solution.py:232
  35.5 15.1 %all-to-all-start = ((bf16[16,16,384]{2,1,0:T(8,128)(2,1)}), bf16[16,16,384]{2,1,0:T(8,128)(2,1)}, u32[]{:S(2)}, u32[]{:S(2)}) async-start(bf16[16,16,384]{2,1,0:T(8,128)(2,1)} %bitcast.40), calls=%async_computation | async-start | bytes 393216 | tf_op jit(solution)/shard_map/all_to_all | solution.py:333
  42.2 23.6 %copy-start.3 = (bf16[2048,128]{1,0:T(8,128)(2,1)}, bf16[2048,128]{1,0:T(8,128)(2,1)S(1)}, u32[]{:S(2)}) copy-start(bf16[2048,128]{1,0:T(8,128)(2,1)S(1)} %copy.61.own_ref) | copy-start | bytes 1572868
  42.2 26.2 %collective-permute-start.12 = (bf16[1024,128]{1,0:T(8,128)(2,1)S(1)}, bf16[1024,128]{1,0:T(8,128)(2,1)S(1)}, u32[]{:S(2)}, u32[]{:S(2)}) collective-permute-start(bf16[1024,128]{1,0:T(8,128)(2,1)S(1)} %constant_dynamic-slice_fusion), channel_id=1, source_target_pairs={{0,6},{1,7},{2,4},{3,5},{4,2},{5,3},{6,0},{7,1},{8,14},{9,15},{10,... | collective-permute-start | bytes 786440 | tf_op jit(solution)/shard_map/ppermute | solution.py:232
  45.1 25.4 %collective-permute-start.11 = (bf16[1024,128]{1,0:T(8,128)(2,1)S(1)}, bf16[1024,128]{1,0:T(8,128)(2,1)S(1)}, u32[]{:S(2)}, u32[]{:S(2)}) collective-permute-start(bf16[1024,128]{1,0:T(8,128)(2,1)S(1)} %constant_dynamic-slice_fusion), channel_id=1, source_target_pairs={{0,4},{1,5},{2,6},{3,7},{4,0},{5,1},{6,2},{7,3},{8,12},{9,13},{10,... | collective-permute-start | bytes 786440 | tf_op jit(solution)/shard_map/ppermute | solution.py:232
  45.6 24.8 %collective-permute-start.10 = (bf16[1024,128]{1,0:T(8,128)(2,1)S(1)}, bf16[1024,128]{1,0:T(8,128)(2,1)S(1)}, u32[]{:S(2)}, u32[]{:S(2)}) collective-permute-start(bf16[1024,128]{1,0:T(8,128)(2,1)S(1)} %constant_dynamic-slice_fusion), channel_id=1, source_target_pairs={{0,2},{1,3},{2,0},{3,1},{4,6},{5,7},{6,4},{7,5},{8,10},{9,11},{10,... | collective-permute-start | bytes 786440 | tf_op jit(solution)/shard_map/ppermute | solution.py:232
  66.0 7.0 %collective-permute-start.9 = (bf16[16,2176]{1,0:T(8,128)(2,1)S(1)}, bf16[16,2176]{1,0:T(8,128)(2,1)S(1)}, u32[]{:S(2)}, u32[]{:S(2)}) collective-permute-start(bf16[16,2176]{1,0:T(8,128)(2,1)S(1)} %concatenate.17), channel_id=1, source_target_pairs={{0,24},{1,25},{2,26},{3,27},{4,28},{5,29},{6,30},{7,31},{8,16},{9,... | collective-permute-start | bytes 208904 | tf_op jit(solution)/shard_map/ppermute | solution.py:232
  67.7 6.3 %collective-permute-start.8 = (bf16[16,2176]{1,0:T(8,128)(2,1)S(1)}, bf16[16,2176]{1,0:T(8,128)(2,1)S(1)}, u32[]{:S(2)}, u32[]{:S(2)}) collective-permute-start(bf16[16,2176]{1,0:T(8,128)(2,1)S(1)} %concatenate.17), channel_id=1, source_target_pairs={{0,16},{1,17},{2,18},{3,19},{4,20},{5,21},{6,22},{7,23},{8,24},{9,... | collective-permute-start | bytes 208904 | tf_op jit(solution)/shard_map/ppermute | solution.py:232
  68.4 5.6 %collective-permute-start.7 = (bf16[16,2176]{1,0:T(8,128)(2,1)S(1)}, bf16[16,2176]{1,0:T(8,128)(2,1)S(1)}, u32[]{:S(2)}, u32[]{:S(2)}) collective-permute-start(bf16[16,2176]{1,0:T(8,128)(2,1)S(1)} %concatenate.17), channel_id=1, source_target_pairs={{0,8},{1,9},{2,10},{3,11},{4,12},{5,13},{6,14},{7,15},{8,0},{9,1},... | collective-permute-start | bytes 208904 | tf_op jit(solution)/shard_map/ppermute | solution.py:232
  70.5 31.4 %copy-start.1 = (bf16[1,2048,512]{2,1,0:T(8,128)(2,1)S(1)}, bf16[1,2048,512]{2,1,0:T(8,128)(2,1)}, u32[]{:S(2)}) copy-start(bf16[1,2048,512]{2,1,0:T(8,128)(2,1)} %switch_ref.1) | copy-start | bytes 6291460
  70.6 31.4 %copy-start.2 = (s32[4]{0:T(128)S(1)}, s32[4]{0:T(128)}, u32[]{:S(2)}) copy-start(s32[4]{0:T(128)} %pad_add_fusion.where_ref) | copy-start | bytes 52
  70.6 5.4 %collective-permute-start.13 = (bf16[3,1024,128]{2,1,0:T(8,128)(2,1)S(1)}, bf16[3,1024,128]{2,1,0:T(8,128)(2,1)}, u32[]{:S(2)}, u32[]{:S(2)}) collective-permute-start(bf16[3,1024,128]{2,1,0:T(8,128)(2,1)S(1)} %pad_maximum_fusion.1.near_ref), channel_id=1, source_target_pairs={{0,1},{1,0},{2,3},{3,2},{4,5},{5,4},{6,7},{7,6},{8,9},{9,8},{10,11... | collective-permute-start | bytes 2359304 | tf_op jit(solution)/shard_map/ppermute | solution.py:232
  78.7 7.0 %collective-permute-start.16 = (bf16[64,512]{1,0:T(8,128)(2,1)}, bf16[64,512]{1,0:T(8,128)(2,1)S(1)}, u32[]{:S(2)}, u32[]{:S(2)}) collective-permute-start(bf16[64,512]{1,0:T(8,128)(2,1)} %output.1.refs_0_), channel_id=1, source_target_pairs={{0,24},{1,25},{2,26},{3,27},{4,28},{5,29},{6,30},{7,31},{8,16},{9,... | collective-permute-start | bytes 196616 | tf_op jit(solution)/shard_map/ppermute | solution.py:232
  80.9 6.1 %collective-permute-start.15 = (bf16[64,512]{1,0:T(8,128)(2,1)}, bf16[64,512]{1,0:T(8,128)(2,1)S(1)}, u32[]{:S(2)}, u32[]{:S(2)}) collective-permute-start(bf16[64,512]{1,0:T(8,128)(2,1)} %output.1.refs_0_), channel_id=1, source_target_pairs={{0,16},{1,17},{2,18},{3,19},{4,20},{5,21},{6,22},{7,23},{8,24},{9,... | collective-permute-start | bytes 196616 | tf_op jit(solution)/shard_map/ppermute | solution.py:232
  80.9 6.1 %collective-permute-start.14 = (bf16[64,512]{1,0:T(8,128)(2,1)}, bf16[64,512]{1,0:T(8,128)(2,1)S(1)}, u32[]{:S(2)}, u32[]{:S(2)}) collective-permute-start(bf16[64,512]{1,0:T(8,128)(2,1)} %output.1.refs_0_), channel_id=1, source_target_pairs={{0,8},{1,9},{2,10},{3,11},{4,12},{5,13},{6,14},{7,15},{8,0},{9,1},... | collective-permute-start | bytes 196616 | tf_op jit(solution)/shard_map/ppermute | solution.py:232
  100.0 2.0 %collective-permute-start.17 = (bf16[128,2176]{1,0:T(8,128)(2,1)S(1)}, bf16[128,2176]{1,0:T(8,128)(2,1)S(1)}, u32[]{:S(2)}, u32[]{:S(2)}) collective-permute-start(bf16[128,2176]{1,0:T(8,128)(2,1)S(1)} %all_gather.3.own_ref), channel_id=1, source_target_pairs={{0,1},{1,0},{2,3},{3,2},{4,5},{5,4},{6,7},{7,6},{8,9},{9,8},{10,11... | collective-permute-start | bytes 1671176 | tf_op jit(solution)/shard_map/ppermute | solution.py:232
  106.1 20.4 %copy-start.21 = (bf16[16,2048]{1,0:T(8,128)(2,1)S(1)}, bf16[16,2048]{1,0:T(8,128)(2,1)}, u32[]{:S(2)}) copy-start(bf16[16,2048]{1,0:T(8,128)(2,1)} %get-tuple-element.11) | copy-start | bytes 196612
  106.2 2.0 %collective-permute-start.18 = (bf16[128,2048]{1,0:T(8,128)(2,1)S(1)}, bf16[128,2048]{1,0:T(8,128)(2,1)S(1)}, u32[]{:S(2)}, u32[]{:S(2)}) collective-permute-start(bf16[128,2048]{1,0:T(8,128)(2,1)S(1)} %get-tuple-element.14), channel_id=1, source_target_pairs={{0,1},{1,0},{2,3},{3,2},{4,5},{5,4},{6,7},{7,6},{8,9},{9,8},{10,11... | collective-permute-start | bytes 1572872 | tf_op jit(solution)/shard_map/ppermute | solution.py:232
  119.9 5.8 %collective-permute-start.21 = (bf16[8,2048]{1,0:T(8,128)(2,1)S(1)}, bf16[8,2048]{1,0:T(8,128)(2,1)S(1)}, u32[]{:S(2)}, u32[]{:S(2)}) collective-permute-start(bf16[8,2048]{1,0:T(8,128)(2,1)S(1)} %get-tuple-element.22), channel_id=1, source_target_pairs={{0,24},{1,25},{2,26},{3,27},{4,28},{5,29},{6,30},{7,31},{8,16},{9,... | collective-permute-start | bytes 98312 | tf_op jit(solution)/shard_map/ppermute | solution.py:232
  121.6 4.9 %collective-permute-start.20 = (bf16[8,2048]{1,0:T(8,128)(2,1)S(1)}, bf16[8,2048]{1,0:T(8,128)(2,1)S(1)}, u32[]{:S(2)}, u32[]{:S(2)}) collective-permute-start(bf16[8,2048]{1,0:T(8,128)(2,1)S(1)} %get-tuple-element.23), channel_id=1, source_target_pairs={{0,16},{1,17},{2,18},{3,19},{4,20},{5,21},{6,22},{7,23},{8,24},{9,... | collective-permute-start | bytes 98312 | tf_op jit(solution)/shard_map/ppermute | solution.py:232
  122.0 4.6 %collective-permute-start.19 = (bf16[8,2048]{1,0:T(8,128)(2,1)S(1)}, bf16[8,2048]{1,0:T(8,128)(2,1)S(1)}, u32[]{:S(2)}, u32[]{:S(2)}) collective-permute-start(bf16[8,2048]{1,0:T(8,128)(2,1)S(1)} %get-tuple-element.24), channel_id=1, source_target_pairs={{0,8},{1,9},{2,10},{3,11},{4,12},{5,13},{6,14},{7,15},{8,0},{9,1},... | collective-permute-start | bytes 98312 | tf_op jit(solution)/shard_map/ppermute | solution.py:232
  (16 other events, 100.7 us)

commit v2 on v1

--- a/solution.py
+++ b/solution.py
@@ -36,17 +36,34 @@
     )
 
 
+def turned_dot(rows, columns):
+    return lax.dot_general(rows, columns, (((1,), (1,)), ((), ())), preferred_element_type=f32)
+
+
 def project_kernel(chips, where_ref, *refs):
-    rows_refs, gain_ref, weight_ref, out_ref = refs[:-3], refs[-3], refs[-2], refs[-1]
-    plane, place = where_ref[0], where_ref[1]
-    for kp, rows_ref in enumerate(rows_refs):
-        normed = rms_rows(rows_ref[...].astype(f32), gain_ref[...])
-        result = jnp.dot(normed, weight_ref[...], preferred_element_type=f32).astype(bf16)
-        seqs = result.shape[0] // GROUPS
+    rows_refs, (gain_ref, *map_refs, out_ref, maps) = refs[:chips], refs[chips:]
+    plane, place, core = where_ref[0], where_ref[1], where_ref[2]
+    own_refs, pair_refs = map_refs[:3], map_refs[3:]
+    columns = own_refs[0].shape[0]
+
+    def lay(lower_refs, upper_refs):
+        for m in range(3):
+            maps[2 * m * columns : (2 * m + 1) * columns, :] = lower_refs[m][...]
+            maps[(2 * m + 1) * columns : (2 * m + 2) * columns, :] = upper_refs[m][...]
+
+    pl.when(core == 0)(lambda: lay(own_refs, pair_refs))
+    pl.when(core != 0)(lambda: lay(pair_refs, own_refs))
+    normed = jnp.concatenate(
+        [rms_rows(ref[...].astype(f32), gain_ref[...]) for ref in rows_refs], axis=0
+    )
+    result = turned_dot(normed, maps[...]).astype(bf16)
+    seqs = result.shape[0] // (GROUPS * chips)
+    for kp in range(chips):
         for kz in range(GROUPS):
             chip = (plane ^ kz) * chips + (place ^ kp)
+            block = (kp * GROUPS + kz) * seqs
             out_ref[pl.ds(pl.multiple_of(chip * seqs, seqs), seqs), :] = result[
-                kz * seqs : (kz + 1) * seqs
+                block : block + seqs
             ]
 
 
@@ -126,7 +143,9 @@
             .astype(bf16)
         )
         memory = state_ref[:, :, lanes].reshape(rows, span)
-        removed = split_dot(memory * wide(erase2), block_ones)
+        removed = jnp.dot(
+            (memory * wide(erase2)).astype(bf16), block_ones, preferred_element_type=f32
+        )
         value_wide = jnp.dot(value, spread, preferred_element_type=f32)
         memory = (
             memory * wide(decay2) - removed * wide(write2) + value_wide * wide(replace2)
@@ -152,79 +171,92 @@
         mixed_ref[...] = mixed.astype(bf16).reshape(seqs, heads, channel)
 
 
-def output_kernel(where_ref, mixed_ref, own_ref, near_ref, far_ref, out_ref):
-    place, core = where_ref[1], where_ref[2]
-    depth, columns = own_ref.shape
+def output_kernel(room, members, where_ref, *refs):
+    mixed_refs, (own_ref, near_ref, far_ref) = refs[:GROUPS], refs[GROUPS : GROUPS + 3]
+    part_refs, (pick_ref, tail_ref, mixed, result) = refs[GROUPS + 3 : 2 * GROUPS + 3], refs[2 * GROUPS + 3 :]
+    plane, place, core = where_ref[0], where_ref[1], where_ref[2]
+    columns, depth = own_ref.shape
     half = depth // 2
-    mixed = mixed_ref[:, :depth]
-    near = mixed_ref[:, pl.ds(pl.multiple_of(core * half, half), half)]
-    far = mixed_ref[:, pl.ds(pl.multiple_of((1 - core) * half, half), half)]
+    seqs = mixed_refs[0].shape[0]
+    rows = GROUPS * seqs
+    for k, ref in enumerate(mixed_refs):
+        mixed[k * seqs : (k + 1) * seqs, :] = ref[...]
+    near = mixed[:, pl.ds(pl.multiple_of(core * half, half), half)]
+    far = mixed[:, pl.ds(pl.multiple_of((1 - core) * half, half), half)]
     for kp in range(near_ref.shape[0] + 1):
         if kp == 0:
-            result = jnp.dot(mixed, own_ref[...], preferred_element_type=f32)
+            block = turned_dot(mixed[:, :depth], own_ref[...])
         else:
-            result = jnp.dot(near, near_ref[kp - 1], preferred_element_type=f32) + jnp.dot(
-                far, far_ref[kp - 1], preferred_element_type=f32
-            )
+            block = turned_dot(near, near_ref[kp - 1]) + turned_dot(far, far_ref[kp - 1])
         at = pl.multiple_of((place ^ kp) * columns, columns)
-        out_ref[:, pl.ds(at, columns)] = result.astype(bf16)
-
-
-def residual_kernel(
-    where_ref, *refs
-):
-    parts, (rows_ref, tail_ref, gain_ref, pick_ref, chosen_ref, own_ref, held) = (
+        result[:, pl.ds(at, columns)] = block.astype(bf16)
+
+    def iota(shape, axis):
+        return lax.broadcasted_iota(jnp.int32, shape, axis)
+
+    tail = mixed[:, depth:]
+    at = iota(tail.shape, 1) == 2 * members
+    group = jnp.sum(jnp.where(at, tail.astype(f32), 0.0), axis=1, keepdims=True)
+    above, along = iota((rows, rows), 0), iota((rows, rows), 1)
+    group_row = jnp.sum(jnp.where(above == along, group, 0.0), axis=0, keepdims=True)
+    earlier = (above // seqs == along // seqs) & (above < along) & (group == group_row)
+    rank = jnp.sum(earlier.astype(f32), axis=0, keepdims=True)
+    slot, lane = iota((GROUPS * room, rows), 0), iota((GROUPS * room, rows), 1)
+    for k, part_ref in enumerate(part_refs):
+        pick = (
+            (lane // seqs == ((slot // room) ^ k))
+            & (group_row == (plane ^ k).astype(f32))
+            & (rank == (slot % room).astype(f32))
+        )
+        pick = pick.astype(f32).astype(bf16)
+        part_ref[...] = jnp.dot(pick, result[...], preferred_element_type=f32).astype(bf16)
+        if k == 0:
+            pick_ref[...] = pick
+            tail_ref[...] = jnp.dot(pick, tail, preferred_element_type=f32).astype(bf16)
+
+
+def residual_kernel(where_ref, *refs):
+    parts, (rows_ref, tail_ref, gain_ref, chosen_ref, residual_ref, held) = (
         refs[:GROUPS],
         refs[GROUPS:],
     )
     plane = where_ref[0]
-    seqs = rows_ref.shape[0] // GROUPS
     width = rows_ref.shape[1]
     columns = width // GROUPS
     for k, part_ref in enumerate(parts):
         at = pl.multiple_of((plane ^ k) * columns, columns)
-        for j in range(GROUPS):
-            mine = slice((k ^ j) * seqs, ((k ^ j) + 1) * seqs)
-            held[mine, pl.ds(at, columns)] = rows_ref[mine, pl.ds(at, columns)].astype(
-                f32
-            ) + part_ref[j * seqs : (j + 1) * seqs, :].astype(f32)
+        held[:, pl.ds(at, columns)] = rows_ref[:, pl.ds(at, columns)].astype(f32) + part_ref[
+            ...
+        ].astype(f32)
     residual = held[...].astype(bf16)
-    own_ref[...] = residual[:seqs]
-    second = rms_rows(residual.astype(f32), gain_ref[...])
-    pick = pick_ref[...]
-    chosen_ref[:, :width] = jnp.dot(pick, second, preferred_element_type=f32).astype(bf16)
-    chosen_ref[:, width:] = jnp.dot(pick, tail_ref[...], preferred_element_type=f32).astype(bf16)
-
-
-def expert_kernel(
-    members, where_ref, own_ref, other_ref, switch_ref, widen_ref, shrink_ref, mine_ref, theirs_ref, total
-):
-    step = pl.program_id(0)
-    width = switch_ref.shape[0]
-    count = own_ref.shape[0]
-
-    @pl.when(step == 0)
-    def _():
-        total[...] = jnp.zeros_like(total)
-
-    rows = jnp.concatenate([own_ref[:, :width], other_ref[:, :width]], axis=0)
-    gate = jnp.dot(rows, switch_ref[...], preferred_element_type=f32)
-    up = jnp.dot(rows, widen_ref[...], preferred_element_type=f32)
+    residual_ref[...] = residual
+    chosen_ref[:, :width] = rms_rows(residual.astype(f32), gain_ref[...])
+    chosen_ref[:, width:] = tail_ref[...]
+
+
+def expert_kernel(members, where_ref, *refs):
+    blocks, (switch_ref, widen_ref, shrink_ref, mine_ref, theirs_ref, rows) = (
+        refs[:members],
+        refs[members:],
+    )
+    width = switch_ref.shape[1]
+    size = blocks[0].shape[0]
+    for i, ref in enumerate(blocks):
+        rows[i * size : (i + 1) * size, :] = ref[...]
+    tokens = rows[:, :width]
+    gate = jnp.dot(tokens, switch_ref[0], preferred_element_type=f32)
+    up = jnp.dot(tokens, widen_ref[0], preferred_element_type=f32)
     hidden = (gate * jax.nn.sigmoid(gate) * up).astype(bf16)
-    total[...] += jnp.dot(hidden, shrink_ref[...], preferred_element_type=f32)
-
-    @pl.when(step == pl.num_programs(0) - 1)
-    def _():
-        member = where_ref[3]
-        for ref, out_ref, start in ((own_ref, mine_ref, 0), (other_ref, theirs_ref, count)):
-            tail = ref[:, width:].astype(f32)
-            lane = lax.broadcasted_iota(jnp.int32, tail.shape, 1)
-            share = jnp.sum(
-                jnp.where((lane == member) | (lane == member + members), tail, 0.0),
-                axis=-1,
-                keepdims=True,
-            )
-            out_ref[...] = (total[start : start + count, :] * share).astype(bf16)
+    tail = rows[:, width:].astype(f32)
+    lane = lax.broadcasted_iota(jnp.int32, tail.shape, 1)
+    member = where_ref[3]
+    share = jnp.sum(
+        jnp.where((lane == member) | (lane == member + members), tail, 0.0), axis=-1, keepdims=True
+    )
+    result = jnp.dot(hidden, shrink_ref[0], preferred_element_type=f32) * share
+    half = result.shape[0] // 2
+    mine_ref[...] = result[:half].astype(bf16)
+    theirs_ref[...] = result[half:].astype(bf16)
 
 
 def swap(rows, mask):
@@ -270,25 +302,18 @@
     smem = pl.BlockSpec(memory_space=pltpu.SMEM)
     vmem = pl.BlockSpec(memory_space=pltpu.VMEM)
     same_core = [[2 * i + c for i in range(devices // 2)] for c in range(2)]
-    same_plane = [
-        [members * z + 2 * i + c for i in range(chips)] for z in range(GROUPS) for c in range(2)
-    ]
+
+    def limit(mib):
+        return pltpu.CompilerParams(vmem_limit_bytes=mib * 2**20)
 
     line = [latest_embeddings] + [swap(latest_embeddings, members * k) for k in range(1, GROUPS)]
     line_rows = jnp.concatenate(line, axis=0)
     gathered = [line_rows] + [swap(line_rows, 2 * k) for k in range(1, chips)]
 
-    stacked = jnp.concatenate([query_map, lookup_map, content_map, result_map], axis=1)
-    paired = swap(stacked, 1)
-    lower = jnp.where(core == 0, stacked, paired)
-    upper = jnp.where(core == 0, paired, stacked)
-    chip_maps = jnp.stack(
-        [lower.reshape(width, 4, columns), upper.reshape(width, 4, columns)], axis=2
-    ).reshape(width, 4 * 2 * columns)
-    project_maps = chip_maps[:, : 3 * 2 * columns]
-    output_map = chip_maps[:, 3 * 2 * columns :]
-
-    normed = rms_rows(latest_embeddings.astype(f32), earlier_rescale_gain)
+    own_maps = [m.T for m in (query_map, lookup_map, content_map, result_map)]
+    pair_maps = [swap(m, 1) for m in own_maps]
+
+    normed = rms_rows(line_rows[:seqs].astype(f32), earlier_rescale_gain)
     decay_low = jnp.tanh(
         jnp.dot(normed, forget_lower_map, preferred_element_type=f32)
     ).astype(bf16)
@@ -326,10 +351,12 @@
     projected = pl.pallas_call(
         functools.partial(project_kernel, chips),
         out_shape=jax.ShapeDtypeStruct((all_rows, 6 * columns), bf16),
-        in_specs=[smem] + [vmem] * (chips + 2),
+        in_specs=[smem] + [vmem] * (chips + 7),
         out_specs=vmem,
+        scratch_shapes=[pltpu.VMEM((6 * columns, width), bf16)],
+        compiler_params=limit(16),
         name="project",
-    )(where, *gathered, earlier_rescale_gain.reshape(1, width), project_maps)
+    )(where, *gathered, earlier_rescale_gain.reshape(1, width), *own_maps[:3], *pair_maps[:3])
     arrived = lax.all_to_all(
         projected, "ep", split_axis=0, concat_axis=0, tiled=True, axis_index_groups=same_core
     )
@@ -339,12 +366,17 @@
         .reshape(3, seqs, heads, channel)
     )
 
-    half = lax.dynamic_slice_in_dim(output_map, core * (width // 2), width // 2, axis=0)
-    half, projected_done = lax.optimization_barrier((half, projected))
+    chip_map = jnp.where(
+        core == 0,
+        jnp.concatenate([own_maps[3], pair_maps[3]], axis=0),
+        jnp.concatenate([pair_maps[3], own_maps[3]], axis=0),
+    )
+    half = lax.dynamic_slice_in_dim(chip_map, core * (width // 2), width // 2, axis=1)
+    half, _ = lax.optimization_barrier((half, projected))
     near = jnp.stack([swap(half, 2 * k) for k in range(1, chips)])
     far = swap(near, 1)
 
-    lanes = 512
+    lanes = 1024
     small = pl.BlockSpec((seqs, heads, channel), lambda i: (0, 0, 0))
     gains = pl.BlockSpec((heads, channel), lambda i: (0, 0))
     block = pl.BlockSpec((seqs, heads, lanes), lambda i: (0, 0, i))
@@ -359,9 +391,7 @@
         in_specs=[small] * 5 + [gains] * 4 + [block],
         out_specs=[block, small],
         scratch_shapes=[tile] * 5 + [pltpu.VMEM((seqs * heads, channel), f32)],
-        compiler_params=pltpu.CompilerParams(
-            dimension_semantics=("arbitrary",), vmem_limit_bytes=48 * 2**20
-        ),
+        compiler_params=limit(32),
         name="state",
     )(
         signals[1],
@@ -377,92 +407,75 @@
     )
 
     mixed_rows = jnp.concatenate([mixed.reshape(seqs, width), tail], axis=1)
-    mixed_line = jnp.concatenate(
-        [mixed_rows] + [swap(mixed_rows, members * k) for k in range(1, GROUPS)], axis=0
-    )
-    line_columns = pl.pallas_call(
-        output_kernel,
-        out_shape=jax.ShapeDtypeStruct((GROUPS * seqs, width // GROUPS), bf16),
-        in_specs=[smem] + [vmem] * 4,
-        out_specs=vmem,
+    mixed_line = [mixed_rows] + [swap(mixed_rows, members * k) for k in range(1, GROUPS)]
+    room = (seqs + 1) // 2
+    count = GROUPS * room
+    *parts, pick, chosen_tail = pl.pallas_call(
+        functools.partial(output_kernel, room, members),
+        out_shape=[jax.ShapeDtypeStruct((count, width // GROUPS), bf16)] * GROUPS
+        + [
+            jax.ShapeDtypeStruct((count, GROUPS * seqs), bf16),
+            jax.ShapeDtypeStruct((count, tail_width), bf16),
+        ],
+        in_specs=[smem] + [vmem] * (GROUPS + 3),
+        out_specs=[vmem] * (GROUPS + 2),
+        scratch_shapes=[
+            pltpu.VMEM((GROUPS * seqs, width + tail_width), bf16),
+            pltpu.VMEM((GROUPS * seqs, width // GROUPS), bf16),
+        ],
+        compiler_params=limit(16),
         name="output",
-    )(where, mixed_line, output_map, near, far)
-    parts = [line_columns] + [swap(line_columns, members * k) for k in range(1, GROUPS)]
-
-    room = (seqs + 1) // 2
-    line_tail = mixed_line[:, width:]
-    line_group = line_tail[:, 2 * members].reshape(GROUPS, seqs)
-    wanted = (line_group == plane.astype(bf16)).astype(jnp.int32)
-    rank = jnp.cumsum(wanted, axis=1) - wanted
-    pick = (
-        (wanted[:, None, :] == 1)
-        & (rank[:, None, :] == jnp.arange(room, dtype=jnp.int32)[None, :, None])
-    ).astype(bf16)
-    pick = (
-        pick[:, :, None, :] * jnp.eye(GROUPS, dtype=bf16)[:, None, :, None]
-    ).reshape(GROUPS * room, GROUPS * seqs)
+    )(where, *mixed_line, chip_map, near, far)
+    parts = [parts[0]] + [swap(parts[k], members * k) for k in range(1, GROUPS)]
+    chosen_rows = jnp.dot(pick, line_rows, preferred_element_type=f32).astype(bf16)
     chosen, residual = pl.pallas_call(
         residual_kernel,
         out_shape=[
-            jax.ShapeDtypeStruct((GROUPS * room, width + tail_width), bf16),
-            jax.ShapeDtypeStruct((seqs, width), bf16),
+            jax.ShapeDtypeStruct((count, width + tail_width), bf16),
+            jax.ShapeDtypeStruct((count, width), bf16),
         ],
-        in_specs=[smem] + [vmem] * (GROUPS + 4),
+        in_specs=[smem] + [vmem] * (GROUPS + 3),
         out_specs=[vmem] * 2,
-        scratch_shapes=[pltpu.VMEM((GROUPS * seqs, width), f32)],
+        scratch_shapes=[pltpu.VMEM((count, width), f32)],
+        compiler_params=limit(8),
         name="residual",
-    )(where, *parts, line_rows, line_tail, later_rescale_gain.reshape(1, width), pick)
-
-    own_rows = lax.all_gather(chosen, "ep", axis=0, tiled=True, axis_index_groups=same_plane)
-    other_rows = swap(own_rows, 1)
-    hidden = specialist_switch_maps.shape[2]
-    piece = hidden // 2
-    count = own_rows.shape[0]
+    )(where, *parts, chosen_rows, chosen_tail, later_rescale_gain.reshape(1, width))
+
+    own_rows = [chosen] + [swap(chosen, 2 * k) for k in range(1, chips)]
+    other_rows = [swap(rows, 1) for rows in own_rows]
     mine, theirs = pl.pallas_call(
         functools.partial(expert_kernel, members),
-        grid=(hidden // piece,),
-        out_shape=[jax.ShapeDtypeStruct((count, width), bf16)] * 2,
-        in_specs=[
-            smem,
-            full(own_rows.shape),
-            full(own_rows.shape),
-            pl.BlockSpec((None, width, piece), lambda i: (0, 0, i)),
-            pl.BlockSpec((None, width, piece), lambda i: (0, 0, i)),
-            pl.BlockSpec((None, piece, width), lambda i: (0, i, 0)),
-        ],
-        out_specs=[full((count, width))] * 2,
-        scratch_shapes=[pltpu.VMEM((2 * count, width), f32)],
-        compiler_params=pltpu.CompilerParams(
-            dimension_semantics=("arbitrary",), vmem_limit_bytes=48 * 2**20
-        ),
+        out_shape=[jax.ShapeDtypeStruct((chips * count, width), bf16)] * 2,
+        in_specs=[smem] + [vmem] * (members + 3),
+        out_specs=[vmem] * 2,
+        scratch_shapes=[pltpu.VMEM((members * count, width + tail_width), bf16)],
+        compiler_params=limit(24),
         name="expert",
     )(
         where,
-        own_rows,
-        other_rows,
+        *own_rows,
+        *other_rows,
         specialist_switch_maps,
         specialist_widen_maps,
         specialist_shrink_maps,
     )
 
     both = (mine.astype(f32) + swap(theirs, 1).astype(f32)).astype(bf16)
-    spread = lax.all_to_all(
-        both, "ep", split_axis=0, concat_axis=0, tiled=True, axis_index_groups=same_plane
-    )
-    summed = jnp.sum(
-        spread.reshape(chips, GROUPS, room, width).astype(f32), axis=0
-    ).astype(bf16)
+    pieces = [both[k * count : (k + 1) * count] for k in range(chips)]
+    pieces = [pieces[0]] + [swap(pieces[k], 2 * k) for k in range(1, chips)]
+    finished = residual.astype(f32)
+    for piece in pieces:
+        finished = finished + piece.astype(f32)
+    finished = finished.astype(bf16).reshape(GROUPS, room, width)
     home = jnp.concatenate(
-        [summed[0]] + [swap(summed[k], members * k) for k in range(1, GROUPS)], axis=0
-    )
-    own_rank = jnp.sum(
-        (group[None, :] == group[:, None]) & (jnp.arange(seqs)[None, :] < jnp.arange(seqs)[:, None]),
-        axis=1,
-    ).astype(jnp.int32)
-    slot = (group ^ plane) * room + own_rank
-    fetch = (slot[:, None] == jnp.arange(GROUPS * room, dtype=jnp.int32)[None, :]).astype(bf16)
-    expert_sum = jnp.dot(fetch, home, preferred_element_type=f32)
-    new_hidden = (residual.astype(f32) + expert_sum).astype(bf16)
+        [finished[0]] + [swap(finished[k], members * k) for k in range(1, GROUPS)], axis=0
+    )
+    earlier = (group[None, :] == group[:, None]) & (
+        jnp.arange(seqs)[None, :] < jnp.arange(seqs)[:, None]
+    )
+    slot = (group ^ plane) * room + jnp.sum(earlier, axis=1).astype(jnp.int32)
+    fetch = (slot[:, None] == jnp.arange(count, dtype=jnp.int32)[None, :]).astype(bf16)
+    new_hidden = jnp.dot(fetch, home, preferred_element_type=f32).astype(bf16)
     return (new_hidden, new_state)
 
 

time: 128 us -> 129 us (level)
  waiting for transfers between devices: 21.4 us -> 50.5 us
  blocking collectives: 21.7 us -> 0 us
  Pallas kernels: 26.1 us -> 15.2 us
  starting transfers between devices: 32.8 us -> 41.8 us
  local copies, waits for them, and re-layouts: 16.3 us -> 11.9 us
    ppermute x22 -> x34, waiting for transfers between devices: 18.9 us -> 41.7 us  [swap(): return lax.ppermute(rows, 'ep', [(i, i ^ mask) for i in range(count)])]
    all_to_all x1 -> x0, blocking collectives: 11.5 us -> none  [layered(): lax.all_to_all(both, 'ep', split_axis=0, concat_axis=0, tiled=True, axis_...]
    all_gather x1 -> x0, blocking collectives: 10.2 us -> none  [layered(): lax.all_gather(chosen, 'ep', axis=0, tiled=True, axis_index_groups=same_p...]
    ppermute x22 -> x34, starting transfers between devices: 26.5 us -> 35.9 us  [swap(): return lax.ppermute(rows, 'ep', [(i, i ^ mask) for i in range(count)])]
    all_to_all x1, waiting for transfers between devices: 2.43 us -> 8.81 us  [layered(): lax.all_to_all(projected, 'ep', split_axis=0, concat_axis=0, tiled=True,...]
    pallas_call x1, Pallas kernels: 13.4 us -> 8.21 us  [layered(): pl.pallas_call(functools.partial(state_kernel, channel), grid=(channel *...]
    pallas_call x3, Pallas kernels: 9.01 us -> 4.7 us  [the longest x1 2.43 us: layered(): pl.pallas_call(functools.partial(expert_kernel, members), out_shape=[jax....]
    slice x4 -> x2, local copies, waits for them, and re-layouts: 2.62 us -> 0.04 us  [the longest x1 0.03 us: layered(): pieces = [both[k * count:(k + 1) * count] for k in range(chips)]]
  transfers between devices with their start and end apart: 23 -> 35, of which waited for: 12 -> 19; matrix products, arithmetic and copies ran while one was open for 17% -> 10% of each run, Pallas kernels for 11% -> 6%
where the time goes in v2:
time: 129 us
  waiting for transfers between devices  50.5 us (39%)
  starting transfers between devices  41.8 us (32%)
  Pallas kernels  15.2 us (12%)
  local copies, waits for them, and re-layouts  11.9 us (9%)
  other arithmetic  4.38 us (3%)
  matrix products  3.98 us (3%)
    ppermute x34, waiting for transfers between devices, swap(): return lax.ppermute(rows, 'ep', [(i, i ^ mask) for i in range(count)])  41.7 us
    ppermute x34, starting transfers between devices, swap(): return lax.ppermute(rows, 'ep', [(i, i ^ mask) for i in range(count)])  35.9 us
    all_to_all x1, waiting for transfers between devices, layered(): lax.all_to_all(projected, 'ep', split_axis=0, concat_axis=0, tiled=True,...  8.81 us
    pallas_call x1, Pallas kernels, layered(): pl.pallas_call(functools.partial(state_kernel, channel), grid=(channel *...  8.21 us
    unnamed x38, local copies, waits for them, and re-layouts  7.57 us
    all_to_all x1, starting transfers between devices, layered(): lax.all_to_all(projected, 'ep', split_axis=0, concat_axis=0, tiled=True,...  5.87 us
  transfers between devices with their start and end apart: 35, of which 19 were waited for; matrix products, arithmetic and copies ran while one was open for 10% of the time, Pallas kernels for 6%

profile of v2, /device:TPU:0, one launch (start us, length us, event | category | flops | bytes accessed | tf_op | source)
XLA Modules:
  0.0 128.7 jit_solution(635180991555499489)
XLA Ops:
  0.7 3.1 %collective-permute-start = (bf16[16,2048]{1,0:T(8,128)(2,1)}, bf16[16,2048]{1,0:T(8,128)(2,1)S(1)}, u32[]{:S(2)}, u32[]{:S(2)}) collective-permute-start(bf16[16,2048]{1,0:T(8,128)(2,1)} %param.23), channel_id=1, source_target_pairs={{0,8},{1,9},{2,10},{3,11},{4,12},{5,13},{6,14},{7,15},{8,0},{9,1},... | collective-permute-start | bytes 196616 | tf_op jit(solution)/shard_map/ppermute | solution.py:264
  3.8 2.6 %collective-permute-start.1 = (bf16[16,2048]{1,0:T(8,128)(2,1)}, bf16[16,2048]{1,0:T(8,128)(2,1)S(1)}, u32[]{:S(2)}, u32[]{:S(2)}) collective-permute-start(bf16[16,2048]{1,0:T(8,128)(2,1)} %param.23), channel_id=1, source_target_pairs={{0,16},{1,17},{2,18},{3,19},{4,20},{5,21},{6,22},{7,23},{8,24},{9,... | collective-permute-start | bytes 196616 | tf_op jit(solution)/shard_map/ppermute | solution.py:264
  13.3 1.8 %collective-permute-start.3 = (bf16[64,2048]{1,0:T(8,128)(2,1)S(1)}, bf16[64,2048]{1,0:T(8,128)(2,1)S(1)}, u32[]{:S(2)}, u32[]{:S(2)}) collective-permute-start(bf16[64,2048]{1,0:T(8,128)(2,1)S(1)} %constant_dynamic-update-slice_fusion.refs_0_), channel_id=1, source_target_pairs={{0,2},{1,3},{2,0},{3,1},{4,6},{5,7},{6,4},{7,5},{8,10},{9,11},{10,... | collective-permute-start | bytes 786440 | tf_op jit(solution)/shard_map/ppermute | solution.py:264
  15.1 1.5 %collective-permute-start.4 = (bf16[64,2048]{1,0:T(8,128)(2,1)S(1)}, bf16[64,2048]{1,0:T(8,128)(2,1)S(1)}, u32[]{:S(2)}, u32[]{:S(2)}) collective-permute-start(bf16[64,2048]{1,0:T(8,128)(2,1)S(1)} %constant_dynamic-update-slice_fusion.refs_0_), channel_id=1, source_target_pairs={{0,4},{1,5},{2,6},{3,7},{4,0},{5,1},{6,2},{7,3},{8,12},{9,13},{10,... | collective-permute-start | bytes 786440 | tf_op jit(solution)/shard_map/ppermute | solution.py:264
  18.7 3.8 %collective-permute-done.3.refs_1_ = bf16[64,2048]{1,0:T(8,128)(2,1)S(1)} collective-permute-done((bf16[64,2048]{1,0:T(8,128)(2,1)S(1)}, bf16[64,2048]{1,0:T(8,128)(2,1)S(1)}, u32[]{:S(2)}, u32[]{:S(2)}) %collective-permute-start.3) | collective-permute-done | bytes 262176 | tf_op jit(solution)/shard_map/ppermute | solution.py:264
  22.5 6.1 %collective-permute-done.4.refs_2_ = bf16[64,2048]{1,0:T(8,128)(2,1)S(1)} collective-permute-done((bf16[64,2048]{1,0:T(8,128)(2,1)S(1)}, bf16[64,2048]{1,0:T(8,128)(2,1)S(1)}, u32[]{:S(2)}, u32[]{:S(2)}) %collective-permute-start.4) | collective-permute-done | bytes 262176 | tf_op jit(solution)/shard_map/ppermute | solution.py:264
  28.7 2.3 %project.1 = bf16[256,384]{1,0:T(8,128)(2,1)} custom-call(s32[4]{0:T(128)S(1)} %pad_add_fusion.where_ref, bf16[64,2048]{1,0:T(8,128)(2,1)S(1)} %constant_dynamic-update-slice_fusion.refs_0_, bf16[64,2048]{1,0:T(8,128)(2,1)S(1)} %collective-permute-done.3.refs_1_, bf16[64,2048]{1,0:T(8,128)(2,1)S(1)} %collective-permute-done.4.refs_2_, ...), custom_call_target="tpu_custom_call" | custom-call | tf_op jit(solution)/shard_map/project/pallas_call | solution.py:351
  31.0 1.6 %collective-permute-start.15 = (bf16[128,1024]{1,0:T(8,128)(2,1)S(1)}, bf16[128,1024]{1,0:T(8,128)(2,1)S(1)}, u32[]{:S(2)}, u32[]{:S(2)}) collective-permute-start(bf16[128,1024]{1,0:T(8,128)(2,1)S(1)} %constant_dynamic-slice_fusion), channel_id=1, source_target_pairs={{0,6},{1,7},{2,4},{3,5},{4,2},{5,3},{6,0},{7,1},{8,14},{9,15},{10,... | collective-permute-start | bytes 786440 | tf_op jit(solution)/shard_map/ppermute | solution.py:264
  36.2 4.9 %collective-permute-done.15 = bf16[128,1024]{1,0:T(8,128)(2,1)S(1)} collective-permute-done((bf16[128,1024]{1,0:T(8,128)(2,1)S(1)}, bf16[128,1024]{1,0:T(8,128)(2,1)S(1)}, u32[]{:S(2)}, u32[]{:S(2)}) %collective-permute-start.15) | collective-permute-done | bytes 262176 | tf_op jit(solution)/shard_map/ppermute | solution.py:264
  41.1 3.6 %collective-permute-done.14 = bf16[128,1024]{1,0:T(8,128)(2,1)S(1)} collective-permute-done((bf16[128,1024]{1,0:T(8,128)(2,1)S(1)}, bf16[128,1024]{1,0:T(8,128)(2,1)S(1)}, u32[]{:S(2)}, u32[]{:S(2)}) %collective-permute-start.14) | collective-permute-done | bytes 262176 | tf_op jit(solution)/shard_map/ppermute | solution.py:264
  45.7 5.9 %all-to-all-start = ((bf16[16,16,384]{2,1,0:T(8,128)(2,1)}), bf16[16,16,384]{2,1,0:T(8,128)(2,1)S(1)}, u32[]{:S(2)}, u32[]{:S(2)}) async-start(bf16[16,16,384]{2,1,0:T(8,128)(2,1)} %bitcast.9), calls=%async_computation | async-start | bytes 393216 | tf_op jit(solution)/shard_map/all_to_all | solution.py:360
  51.7 8.8 %all-to-all-done = bf16[16,16,384]{2,1,0:T(8,128)(2,1)S(1)} async-done(((bf16[16,16,384]{2,1,0:T(8,128)(2,1)}), bf16[16,16,384]{2,1,0:T(8,128)(2,1)S(1)}, u32[]{:S(2)}, u32[]{:S(2)}) %all-to-all-start) | async-done | bytes 196640 | tf_op jit(solution)/shard_map/all_to_all | solution.py:360
  63.1 3.4 %copy-done.1 = f32[16,32,4096]{2,1,0:T(8,128)S(1)} copy-done((f32[16,32,4096]{2,1,0:T(8,128)S(1)}, f32[16,32,4096]{2,1,0:T(8,128)}, u32[]{:S(2)}) %copy-start.1) | copy-done | bytes 8388632
  66.5 8.2 %state.1 = (f32[16,32,4096]{2,1,0:T(8,128)}, bf16[16,32,64]{2,1,0:T(8,128)(2,1)S(1)}) custom-call(bf16[16,32,64]{2,1,0:T(8,128)(2,1)S(1)} %bitcast.33, bf16[16,32,64]{2,1,0:T(8,128)(2,1)S(1)} %bitcast.34, bf16[16,32,64]{2,1,0:T(8,128)(2,1)S(1)} %bitcast.35, f32[16,32,64]{2,1,0:T(8,128)S(1)} %reshape.104.decay_ref, f32[16,32,64]{2,1,0:T(8,128)S(1)} %reshape.105.rate_ref, ...), custom_call_target="tpu_custom_call" | custom-call | tf_op jit(solution)/shard_map/state/pallas_call | solution.py:384
  77.6 1.8 %collective-permute-start.11 = (bf16[16,2176]{1,0:T(8,128)(2,1)S(1)}, bf16[16,2176]{1,0:T(8,128)(2,1)S(1)}, u32[]{:S(2)}, u32[]{:S(2)}) collective-permute-start(bf16[16,2176]{1,0:T(8,128)(2,1)S(1)} %concatenate.16.refs_0_), channel_id=1, source_target_pairs={{0,24},{1,25},{2,26},{3,27},{4,28},{5,29},{6,30},{7,31},{8,16},{9,... | collective-permute-start | bytes 208904 | tf_op jit(solution)/shard_map/ppermute | solution.py:264
  79.5 3.6 %collective-permute-done.10.refs_2_ = bf16[16,2176]{1,0:T(8,128)(2,1)S(1)} collective-permute-done((bf16[16,2176]{1,0:T(8,128)(2,1)S(1)}, bf16[16,2176]{1,0:T(8,128)(2,1)S(1)}, u32[]{:S(2)}, u32[]{:S(2)}) %collective-permute-start.10) | collective-permute-done | bytes 69664 | tf_op jit(solution)/shard_map/ppermute | solution.py:264
  83.9 1.6 %output.1 = (bf16[32,512]{1,0:T(8,128)(2,1)S(1)}, bf16[32,512]{1,0:T(8,128)(2,1)S(1)}, bf16[32,512]{1,0:T(8,128)(2,1)S(1)}, bf16[32,512]{1,0:T(8,128)(2,1)S(1)},...) custom-call(s32[4]{0:T(128)S(1)} %pad_add_fusion.where_ref, bf16[16,2176]{1,0:T(8,128)(2,1)S(1)} %concatenate.16.refs_0_, ...), custom_call_target="tpu_custom_call" | custom-call | tf_op jit(solution)/shard_map/output/pallas_call | solution.py:413
  87.9 2.0 %collective-permute-start.19 = (bf16[32,512]{1,0:T(8,128)(2,1)S(1)}, bf16[32,512]{1,0:T(8,128)(2,1)S(1)}, u32[]{:S(2)}, u32[]{:S(2)}) collective-permute-start(bf16[32,512]{1,0:T(8,128)(2,1)S(1)} %get-tuple-element.20), channel_id=1, source_target_pairs={{0,24},{1,25},{2,26},{3,27},{4,28},{5,29},{6,30},{7,31},{8,16},{9,... | collective-permute-start | bytes 98312 | tf_op jit(solution)/shard_map/ppermute | solution.py:264
  90.1 1.9 %collective-permute-done.18.refs_2_ = bf16[32,512]{1,0:T(8,128)(2,1)S(1)} collective-permute-done((bf16[32,512]{1,0:T(8,128)(2,1)S(1)}, bf16[32,512]{1,0:T(8,128)(2,1)S(1)}, u32[]{:S(2)}, u32[]{:S(2)}) %collective-permute-start.18) | collective-permute-done | bytes 32800 | tf_op jit(solution)/shard_map/ppermute | solution.py:264
  91.9 1.7 %collective-permute-done.19.refs_3_ = bf16[32,512]{1,0:T(8,128)(2,1)S(1)} collective-permute-done((bf16[32,512]{1,0:T(8,128)(2,1)S(1)}, bf16[32,512]{1,0:T(8,128)(2,1)S(1)}, u32[]{:S(2)}, u32[]{:S(2)}) %collective-permute-start.19) | collective-permute-done | bytes 32800 | tf_op jit(solution)/shard_map/ppermute | solution.py:264
  96.1 1.8 %collective-permute-start.22 = (bf16[32,2176]{1,0:T(8,128)(2,1)S(1)}, bf16[32,2176]{1,0:T(8,128)(2,1)S(1)}, u32[]{:S(2)}, u32[]{:S(2)}) collective-permute-start(bf16[32,2176]{1,0:T(8,128)(2,1)S(1)} %get-tuple-element.24.refs_0_), channel_id=1, source_target_pairs={{0,6},{1,7},{2,4},{3,5},{4,2},{5,3},{6,0},{7,1},{8,14},{9,15},{10,... | collective-permute-start | bytes 417800 | tf_op jit(solution)/shard_map/ppermute | solution.py:264
  97.8 1.6 %collective-permute-done.20.refs_1_ = bf16[32,2176]{1,0:T(8,128)(2,1)S(1)} collective-permute-done((bf16[32,2176]{1,0:T(8,128)(2,1)S(1)}, bf16[32,2176]{1,0:T(8,128)(2,1)S(1)}, u32[]{:S(2)}, u32[]{:S(2)}) %collective-permute-start.20) | collective-permute-done | bytes 139296 | tf_op jit(solution)/shard_map/ppermute | solution.py:264
  99.4 2.7 %collective-permute-done.21.refs_2_ = bf16[32,2176]{1,0:T(8,128)(2,1)S(1)} collective-permute-done((bf16[32,2176]{1,0:T(8,128)(2,1)S(1)}, bf16[32,2176]{1,0:T(8,128)(2,1)S(1)}, u32[]{:S(2)}, u32[]{:S(2)}) %collective-permute-start.21) | collective-permute-done | bytes 139296 | tf_op jit(solution)/shard_map/ppermute | solution.py:264
  103.7 1.6 %copy-done.3 = bf16[1,2048,512]{2,1,0:T(8,128)(2,1)S(1)} copy-done((bf16[1,2048,512]{2,1,0:T(8,128)(2,1)S(1)}, bf16[1,2048,512]{2,1,0:T(8,128)(2,1)}, u32[]{:S(2)}) %copy-start.3) | copy-done | bytes 2097176
  105.3 1.6 %copy-done.4 = bf16[1,512,2048]{2,1,0:T(8,128)(2,1)S(1)} copy-done((bf16[1,512,2048]{2,1,0:T(8,128)(2,1)S(1)}, bf16[1,512,2048]{2,1,0:T(8,128)(2,1)}, u32[]{:S(2)}) %copy-start.4) | copy-done | bytes 2097176
  106.9 2.4 %expert.1 = (bf16[128,2048]{1,0:T(8,128)(2,1)S(1)}, bf16[128,2048]{1,0:T(8,128)(2,1)S(1)}) custom-call(s32[4]{0:T(128)S(1)} %pad_add_fusion.where_ref, bf16[32,2176]{1,0:T(8,128)(2,1)S(1)} %get-tuple-element.24.refs_0_, bf16[32,2176]{1,0:T(8,128)(2,1)S(1)} %collective-permute-done.20.refs_1_, bf16[32,2176]{1,0:T(8,128)(2,1)S(1)} %collective-permute-done.21.refs_2_, ...), custom_call_target="tpu_custom_call" | custom-call | tf_op jit(solution)/shard_map/expert/pallas_call | solution.py:446
  109.7 1.6 %collective-permute-done.27 = bf16[128,2048]{1,0:T(8,128)(2,1)S(1)} collective-permute-done((bf16[128,2048]{1,0:T(8,128)(2,1)S(1)}, bf16[128,2048]{1,0:T(8,128)(2,1)S(1)}, u32[]{:S(2)}, u32[]{:S(2)}) %collective-permute-start.27) | collective-permute-done | bytes 524320 | tf_op jit(solution)/shard_map/ppermute | solution.py:264
  111.5 1.5 %collective-permute-start.30 = (bf16[32,2048]{1,0:T(8,128)(2,1)S(1)}, bf16[32,2048]{1,0:T(8,128)(2,1)S(1)}, u32[]{:S(2)}, u32[]{:S(2)}) collective-permute-start(bf16[32,2048]{1,0:T(8,128)(2,1)S(1)} %get-tuple-element.29), channel_id=1, source_target_pairs={{0,6},{1,7},{2,4},{3,5},{4,2},{5,3},{6,0},{7,1},{8,14},{9,15},{10,... | collective-permute-start | bytes 393224 | tf_op jit(solution)/shard_map/ppermute | solution.py:264
  115.0 3.8 %collective-permute-done.30 = bf16[32,2048]{1,0:T(8,128)(2,1)S(1)} collective-permute-done((bf16[32,2048]{1,0:T(8,128)(2,1)S(1)}, bf16[32,2048]{1,0:T(8,128)(2,1)S(1)}, u32[]{:S(2)}, u32[]{:S(2)}) %collective-permute-start.30) | collective-permute-done | bytes 131104 | tf_op jit(solution)/shard_map/ppermute | solution.py:264
  118.9 2.1 %collective-permute-done.29 = bf16[32,2048]{1,0:T(8,128)(2,1)S(1)} collective-permute-done((bf16[32,2048]{1,0:T(8,128)(2,1)S(1)}, bf16[32,2048]{1,0:T(8,128)(2,1)S(1)}, u32[]{:S(2)}, u32[]{:S(2)}) %collective-permute-start.29) | collective-permute-done | bytes 131104 | tf_op jit(solution)/shard_map/ppermute | solution.py:264
  121.1 1.7 %collective-permute-start.33 = (bf16[8,2048]{1,0:T(8,128)(2,1)S(1)}, bf16[8,2048]{1,0:T(8,128)(2,1)S(1)}, u32[]{:S(2)}, u32[]{:S(2)}) collective-permute-start(bf16[8,2048]{1,0:T(8,128)(2,1)S(1)} %get-tuple-element.35), channel_id=1, source_target_pairs={{0,24},{1,25},{2,26},{3,27},{4,28},{5,29},{6,30},{7,31},{8,16},{9,... | collective-permute-start | bytes 98312 | tf_op jit(solution)/shard_map/ppermute | solution.py:264
  122.8 2.7 %collective-permute-start.31 = (bf16[8,2048]{1,0:T(8,128)(2,1)S(1)}, bf16[8,2048]{1,0:T(8,128)(2,1)S(1)}, u32[]{:S(2)}, u32[]{:S(2)}) collective-permute-start(bf16[8,2048]{1,0:T(8,128)(2,1)S(1)} %get-tuple-element.37), channel_id=1, source_target_pairs={{0,8},{1,9},{2,10},{3,11},{4,12},{5,13},{6,14},{7,15},{8,0},{9,1},... | collective-permute-start | bytes 98312 | tf_op jit(solution)/shard_map/ppermute | solution.py:264
  (122 shorter events, 32.4 us)
Async XLA Ops:
  0.7 11.9 %collective-permute-start = (bf16[16,2048]{1,0:T(8,128)(2,1)}, bf16[16,2048]{1,0:T(8,128)(2,1)S(1)}, u32[]{:S(2)}, u32[]{:S(2)}) collective-permute-start(bf16[16,2048]{1,0:T(8,128)(2,1)} %param.23), channel_id=1, source_target_pairs={{0,8},{1,9},{2,10},{3,11},{4,12},{5,13},{6,14},{7,15},{8,0},{9,1},... | collective-permute-start | bytes 196616 | tf_op jit(solution)/shard_map/ppermute | solution.py:264
  3.8 8.9 %collective-permute-start.1 = (bf16[16,2048]{1,0:T(8,128)(2,1)}, bf16[16,2048]{1,0:T(8,128)(2,1)S(1)}, u32[]{:S(2)}, u32[]{:S(2)}) collective-permute-start(bf16[16,2048]{1,0:T(8,128)(2,1)} %param.23), channel_id=1, source_target_pairs={{0,16},{1,17},{2,18},{3,19},{4,20},{5,21},{6,22},{7,23},{8,24},{9,... | collective-permute-start | bytes 196616 | tf_op jit(solution)/shard_map/ppermute | solution.py:264
  6.4 6.8 %collective-permute-start.2 = (bf16[16,2048]{1,0:T(8,128)(2,1)}, bf16[16,2048]{1,0:T(8,128)(2,1)S(1)}, u32[]{:S(2)}, u32[]{:S(2)}) collective-permute-start(bf16[16,2048]{1,0:T(8,128)(2,1)} %param.23), channel_id=1, source_target_pairs={{0,24},{1,25},{2,26},{3,27},{4,28},{5,29},{6,30},{7,31},{8,16},{9,... | collective-permute-start | bytes 196616 | tf_op jit(solution)/shard_map/ppermute | solution.py:264
  6.4 8.7 %collective-permute-start.6 = (bf16[64,2048]{1,0:T(8,128)(2,1)}, bf16[64,2048]{1,0:T(8,128)(2,1)S(1)}, u32[]{:S(2)}, u32[]{:S(2)}) collective-permute-start(bf16[64,2048]{1,0:T(8,128)(2,1)} %bitcast.36), channel_id=1, source_target_pairs={{0,1},{1,0},{2,3},{3,2},{4,5},{5,4},{6,7},{7,6},{8,9},{9,8},{10,11... | collective-permute-start | bytes 786440 | tf_op jit(solution)/shard_map/ppermute | solution.py:264
  6.4 12.3 %collective-permute-start.7 = (bf16[64,2048]{1,0:T(8,128)(2,1)}, bf16[64,2048]{1,0:T(8,128)(2,1)S(1)}, u32[]{:S(2)}, u32[]{:S(2)}) collective-permute-start(bf16[64,2048]{1,0:T(8,128)(2,1)} %bitcast.38), channel_id=1, source_target_pairs={{0,1},{1,0},{2,3},{3,2},{4,5},{5,4},{6,7},{7,6},{8,9},{9,8},{10,11... | collective-permute-start | bytes 786440 | tf_op jit(solution)/shard_map/ppermute | solution.py:264
  12.6 6.0 %collective-permute-start.8 = (bf16[64,2048]{1,0:T(8,128)(2,1)}, bf16[64,2048]{1,0:T(8,128)(2,1)S(1)}, u32[]{:S(2)}, u32[]{:S(2)}) collective-permute-start(bf16[64,2048]{1,0:T(8,128)(2,1)} %bitcast.40), channel_id=1, source_target_pairs={{0,1},{1,0},{2,3},{3,2},{4,5},{5,4},{6,7},{7,6},{8,9},{9,8},{10,11... | collective-permute-start | bytes 786440 | tf_op jit(solution)/shard_map/ppermute | solution.py:264
  12.7 3.9 %collective-permute-start.12 = (bf16[64,2048]{1,0:T(8,128)(2,1)}, bf16[64,2048]{1,0:T(8,128)(2,1)S(1)}, u32[]{:S(2)}, u32[]{:S(2)}) collective-permute-start(bf16[64,2048]{1,0:T(8,128)(2,1)} %bitcast.45), channel_id=1, source_target_pairs={{0,1},{1,0},{2,3},{3,2},{4,5},{5,4},{6,7},{7,6},{8,9},{9,8},{10,11... | collective-permute-start | bytes 786440 | tf_op jit(solution)/shard_map/ppermute | solution.py:264
  13.3 9.2 %collective-permute-start.3 = (bf16[64,2048]{1,0:T(8,128)(2,1)S(1)}, bf16[64,2048]{1,0:T(8,128)(2,1)S(1)}, u32[]{:S(2)}, u32[]{:S(2)}) collective-permute-start(bf16[64,2048]{1,0:T(8,128)(2,1)S(1)} %constant_dynamic-update-slice_fusion.refs_0_), channel_id=1, source_target_pairs={{0,2},{1,3},{2,0},{3,1},{4,6},{5,7},{6,4},{7,5},{8,10},{9,11},{10,... | collective-permute-start | bytes 786440 | tf_op jit(solution)/shard_map/ppermute | solution.py:264
  15.1 13.6 %collective-permute-start.4 = (bf16[64,2048]{1,0:T(8,128)(2,1)S(1)}, bf16[64,2048]{1,0:T(8,128)(2,1)S(1)}, u32[]{:S(2)}, u32[]{:S(2)}) collective-permute-start(bf16[64,2048]{1,0:T(8,128)(2,1)S(1)} %constant_dynamic-update-slice_fusion.refs_0_), channel_id=1, source_target_pairs={{0,4},{1,5},{2,6},{3,7},{4,0},{5,1},{6,2},{7,3},{8,12},{9,13},{10,... | collective-permute-start | bytes 786440 | tf_op jit(solution)/shard_map/ppermute | solution.py:264
  16.6 12.1 %collective-permute-start.5 = (bf16[64,2048]{1,0:T(8,128)(2,1)S(1)}, bf16[64,2048]{1,0:T(8,128)(2,1)S(1)}, u32[]{:S(2)}, u32[]{:S(2)}) collective-permute-start(bf16[64,2048]{1,0:T(8,128)(2,1)S(1)} %constant_dynamic-update-slice_fusion.refs_0_), channel_id=1, source_target_pairs={{0,6},{1,7},{2,4},{3,5},{4,2},{5,3},{6,0},{7,1},{8,14},{9,15},{10,... | collective-permute-start | bytes 786440 | tf_op jit(solution)/shard_map/ppermute | solution.py:264
  31.0 10.2 %collective-permute-start.15 = (bf16[128,1024]{1,0:T(8,128)(2,1)S(1)}, bf16[128,1024]{1,0:T(8,128)(2,1)S(1)}, u32[]{:S(2)}, u32[]{:S(2)}) collective-permute-start(bf16[128,1024]{1,0:T(8,128)(2,1)S(1)} %constant_dynamic-slice_fusion), channel_id=1, source_target_pairs={{0,6},{1,7},{2,4},{3,5},{4,2},{5,3},{6,0},{7,1},{8,14},{9,15},{10,... | collective-permute-start | bytes 786440 | tf_op jit(solution)/shard_map/ppermute | solution.py:264
  32.5 12.2 %collective-permute-start.14 = (bf16[128,1024]{1,0:T(8,128)(2,1)S(1)}, bf16[128,1024]{1,0:T(8,128)(2,1)S(1)}, u32[]{:S(2)}, u32[]{:S(2)}) collective-permute-start(bf16[128,1024]{1,0:T(8,128)(2,1)S(1)} %constant_dynamic-slice_fusion), channel_id=1, source_target_pairs={{0,4},{1,5},{2,6},{3,7},{4,0},{5,1},{6,2},{7,3},{8,12},{9,13},{10,... | collective-permute-start | bytes 786440 | tf_op jit(solution)/shard_map/ppermute | solution.py:264
  33.7 11.0 %collective-permute-start.13 = (bf16[128,1024]{1,0:T(8,128)(2,1)S(1)}, bf16[128,1024]{1,0:T(8,128)(2,1)S(1)}, u32[]{:S(2)}, u32[]{:S(2)}) collective-permute-start(bf16[128,1024]{1,0:T(8,128)(2,1)S(1)} %constant_dynamic-slice_fusion), channel_id=1, source_target_pairs={{0,2},{1,3},{2,0},{3,1},{4,6},{5,7},{6,4},{7,5},{8,10},{9,11},{10,... | collective-permute-start | bytes 786440 | tf_op jit(solution)/shard_map/ppermute | solution.py:264
  44.9 39.0 %collective-permute-start.16 = (bf16[3,128,1024]{2,1,0:T(8,128)(2,1)S(1)}, bf16[3,128,1024]{2,1,0:T(8,128)(2,1)S(1)}, u32[]{:S(2)}, u32[]{:S(2)}) collective-permute-start(bf16[3,128,1024]{2,1,0:T(8,128)(2,1)S(1)} %pad_maximum_fusion.refs_5_), channel_id=1, source_target_pairs={{0,1},{1,0},{2,3},{3,2},{4,5},{5,4},{6,7},{7,6},{8,9},{9,8},{10,11... | collective-permute-start | bytes 2359304 | tf_op jit(solution)/shard_map/ppermute | solution.py:264
  45.7 14.8 %all-to-all-start = ((bf16[16,16,384]{2,1,0:T(8,128)(2,1)}), bf16[16,16,384]{2,1,0:T(8,128)(2,1)S(1)}, u32[]{:S(2)}, u32[]{:S(2)}) async-start(bf16[16,16,384]{2,1,0:T(8,128)(2,1)} %bitcast.9), calls=%async_computation | async-start | bytes 393216 | tf_op jit(solution)/shard_map/all_to_all | solution.py:360
  75.0 4.4 %collective-permute-start.9 = (bf16[16,2176]{1,0:T(8,128)(2,1)S(1)}, bf16[16,2176]{1,0:T(8,128)(2,1)S(1)}, u32[]{:S(2)}, u32[]{:S(2)}) collective-permute-start(bf16[16,2176]{1,0:T(8,128)(2,1)S(1)} %concatenate.16.refs_0_), channel_id=1, source_target_pairs={{0,8},{1,9},{2,10},{3,11},{4,12},{5,13},{6,14},{7,15},{8,0},{9,1},... | collective-permute-start | bytes 208904 | tf_op jit(solution)/shard_map/ppermute | solution.py:264
  76.4 6.7 %collective-permute-start.10 = (bf16[16,2176]{1,0:T(8,128)(2,1)S(1)}, bf16[16,2176]{1,0:T(8,128)(2,1)S(1)}, u32[]{:S(2)}, u32[]{:S(2)}) collective-permute-start(bf16[16,2176]{1,0:T(8,128)(2,1)S(1)} %concatenate.16.refs_0_), channel_id=1, source_target_pairs={{0,16},{1,17},{2,18},{3,19},{4,20},{5,21},{6,22},{7,23},{8,24},{9,... | collective-permute-start | bytes 208904 | tf_op jit(solution)/shard_map/ppermute | solution.py:264
  77.6 6.2 %collective-permute-start.11 = (bf16[16,2176]{1,0:T(8,128)(2,1)S(1)}, bf16[16,2176]{1,0:T(8,128)(2,1)S(1)}, u32[]{:S(2)}, u32[]{:S(2)}) collective-permute-start(bf16[16,2176]{1,0:T(8,128)(2,1)S(1)} %concatenate.16.refs_0_), channel_id=1, source_target_pairs={{0,24},{1,25},{2,26},{3,27},{4,28},{5,29},{6,30},{7,31},{8,16},{9,... | collective-permute-start | bytes 208904 | tf_op jit(solution)/shard_map/ppermute | solution.py:264
  85.4 4.6 %collective-permute-start.17 = (bf16[32,512]{1,0:T(8,128)(2,1)S(1)}, bf16[32,512]{1,0:T(8,128)(2,1)S(1)}, u32[]{:S(2)}, u32[]{:S(2)}) collective-permute-start(bf16[32,512]{1,0:T(8,128)(2,1)S(1)} %get-tuple-element.18), channel_id=1, source_target_pairs={{0,8},{1,9},{2,10},{3,11},{4,12},{5,13},{6,14},{7,15},{8,0},{9,1},... | collective-permute-start | bytes 98312 | tf_op jit(solution)/shard_map/ppermute | solution.py:264
  86.8 5.2 %collective-permute-start.18 = (bf16[32,512]{1,0:T(8,128)(2,1)S(1)}, bf16[32,512]{1,0:T(8,128)(2,1)S(1)}, u32[]{:S(2)}, u32[]{:S(2)}) collective-permute-start(bf16[32,512]{1,0:T(8,128)(2,1)S(1)} %get-tuple-element.19), channel_id=1, source_target_pairs={{0,16},{1,17},{2,18},{3,19},{4,20},{5,21},{6,22},{7,23},{8,24},{9,... | collective-permute-start | bytes 98312 | tf_op jit(solution)/shard_map/ppermute | solution.py:264
  87.9 5.7 %collective-permute-start.19 = (bf16[32,512]{1,0:T(8,128)(2,1)S(1)}, bf16[32,512]{1,0:T(8,128)(2,1)S(1)}, u32[]{:S(2)}, u32[]{:S(2)}) collective-permute-start(bf16[32,512]{1,0:T(8,128)(2,1)S(1)} %get-tuple-element.20), channel_id=1, source_target_pairs={{0,24},{1,25},{2,26},{3,27},{4,28},{5,29},{6,30},{7,31},{8,16},{9,... | collective-permute-start | bytes 98312 | tf_op jit(solution)/shard_map/ppermute | solution.py:264
  94.3 5.1 %collective-permute-start.20 = (bf16[32,2176]{1,0:T(8,128)(2,1)S(1)}, bf16[32,2176]{1,0:T(8,128)(2,1)S(1)}, u32[]{:S(2)}, u32[]{:S(2)}) collective-permute-start(bf16[32,2176]{1,0:T(8,128)(2,1)S(1)} %get-tuple-element.24.refs_0_), channel_id=1, source_target_pairs={{0,2},{1,3},{2,0},{3,1},{4,6},{5,7},{6,4},{7,5},{8,10},{9,11},{10,... | collective-permute-start | bytes 417800 | tf_op jit(solution)/shard_map/ppermute | solution.py:264
  95.6 6.5 %collective-permute-start.21 = (bf16[32,2176]{1,0:T(8,128)(2,1)S(1)}, bf16[32,2176]{1,0:T(8,128)(2,1)S(1)}, u32[]{:S(2)}, u32[]{:S(2)}) collective-permute-start(bf16[32,2176]{1,0:T(8,128)(2,1)S(1)} %get-tuple-element.24.refs_0_), channel_id=1, source_target_pairs={{0,4},{1,5},{2,6},{3,7},{4,0},{5,1},{6,2},{7,3},{8,12},{9,13},{10,... | collective-permute-start | bytes 417800 | tf_op jit(solution)/shard_map/ppermute | solution.py:264
  96.1 6.1 %collective-permute-start.22 = (bf16[32,2176]{1,0:T(8,128)(2,1)S(1)}, bf16[32,2176]{1,0:T(8,128)(2,1)S(1)}, u32[]{:S(2)}, u32[]{:S(2)}) collective-permute-start(bf16[32,2176]{1,0:T(8,128)(2,1)S(1)} %get-tuple-element.24.refs_0_), channel_id=1, source_target_pairs={{0,6},{1,7},{2,4},{3,5},{4,2},{5,3},{6,0},{7,1},{8,14},{9,15},{10,... | collective-permute-start | bytes 417800 | tf_op jit(solution)/shard_map/ppermute | solution.py:264
  97.8 4.8 %collective-permute-start.23 = (bf16[32,2176]{1,0:T(8,128)(2,1)S(1)}, bf16[32,2176]{1,0:T(8,128)(2,1)S(1)}, u32[]{:S(2)}, u32[]{:S(2)}) collective-permute-start(bf16[32,2176]{1,0:T(8,128)(2,1)S(1)} %get-tuple-element.24.refs_0_), channel_id=1, source_target_pairs={{0,1},{1,0},{2,3},{3,2},{4,5},{5,4},{6,7},{7,6},{8,9},{9,8},{10,11... | collective-permute-start | bytes 417800 | tf_op jit(solution)/shard_map/ppermute | solution.py:264
  99.4 3.3 %collective-permute-start.24 = (bf16[32,2176]{1,0:T(8,128)(2,1)S(1)}, bf16[32,2176]{1,0:T(8,128)(2,1)S(1)}, u32[]{:S(2)}, u32[]{:S(2)}) collective-permute-start(bf16[32,2176]{1,0:T(8,128)(2,1)S(1)} %collective-permute-done.20.refs_1_), channel_id=1, source_target_pairs={{0,1},{1,0},{2,3},{3,2},{4,5},{5,4},{6,7},{7,6},{8,9},{9,8},{10,11... | collective-permute-start | bytes 417800 | tf_op jit(solution)/shard_map/ppermute | solution.py:264
  111.5 7.4 %collective-permute-start.30 = (bf16[32,2048]{1,0:T(8,128)(2,1)S(1)}, bf16[32,2048]{1,0:T(8,128)(2,1)S(1)}, u32[]{:S(2)}, u32[]{:S(2)}) collective-permute-start(bf16[32,2048]{1,0:T(8,128)(2,1)S(1)} %get-tuple-element.29), channel_id=1, source_target_pairs={{0,6},{1,7},{2,4},{3,5},{4,2},{5,3},{6,0},{7,1},{8,14},{9,15},{10,... | collective-permute-start | bytes 393224 | tf_op jit(solution)/shard_map/ppermute | solution.py:264
  113.0 8.0 %collective-permute-start.29 = (bf16[32,2048]{1,0:T(8,128)(2,1)S(1)}, bf16[32,2048]{1,0:T(8,128)(2,1)S(1)}, u32[]{:S(2)}, u32[]{:S(2)}) collective-permute-start(bf16[32,2048]{1,0:T(8,128)(2,1)S(1)} %get-tuple-element.30), channel_id=1, source_target_pairs={{0,4},{1,5},{2,6},{3,7},{4,0},{5,1},{6,2},{7,3},{8,12},{9,13},{10,... | collective-permute-start | bytes 393224 | tf_op jit(solution)/shard_map/ppermute | solution.py:264
  114.2 6.8 %collective-permute-start.28 = (bf16[32,2048]{1,0:T(8,128)(2,1)S(1)}, bf16[32,2048]{1,0:T(8,128)(2,1)S(1)}, u32[]{:S(2)}, u32[]{:S(2)}) collective-permute-start(bf16[32,2048]{1,0:T(8,128)(2,1)S(1)} %get-tuple-element.28), channel_id=1, source_target_pairs={{0,2},{1,3},{2,0},{3,1},{4,6},{5,7},{6,4},{7,5},{8,10},{9,11},{10,... | collective-permute-start | bytes 393224 | tf_op jit(solution)/shard_map/ppermute | solution.py:264
  121.1 5.8 %collective-permute-start.33 = (bf16[8,2048]{1,0:T(8,128)(2,1)S(1)}, bf16[8,2048]{1,0:T(8,128)(2,1)S(1)}, u32[]{:S(2)}, u32[]{:S(2)}) collective-permute-start(bf16[8,2048]{1,0:T(8,128)(2,1)S(1)} %get-tuple-element.35), channel_id=1, source_target_pairs={{0,24},{1,25},{2,26},{3,27},{4,28},{5,29},{6,30},{7,31},{8,16},{9,... | collective-permute-start | bytes 98312 | tf_op jit(solution)/shard_map/ppermute | solution.py:264
  122.8 4.9 %collective-permute-start.32 = (bf16[8,2048]{1,0:T(8,128)(2,1)S(1)}, bf16[8,2048]{1,0:T(8,128)(2,1)S(1)}, u32[]{:S(2)}, u32[]{:S(2)}) collective-permute-start(bf16[8,2048]{1,0:T(8,128)(2,1)S(1)} %get-tuple-element.36), channel_id=1, source_target_pairs={{0,16},{1,17},{2,18},{3,19},{4,20},{5,21},{6,22},{7,23},{8,24},{9,... | collective-permute-start | bytes 98312 | tf_op jit(solution)/shard_map/ppermute | solution.py:264
  122.8 5.1 %collective-permute-start.31 = (bf16[8,2048]{1,0:T(8,128)(2,1)S(1)}, bf16[8,2048]{1,0:T(8,128)(2,1)S(1)}, u32[]{:S(2)}, u32[]{:S(2)}) collective-permute-start(bf16[8,2048]{1,0:T(8,128)(2,1)S(1)} %get-tuple-element.37), channel_id=1, source_target_pairs={{0,8},{1,9},{2,10},{3,11},{4,12},{5,13},{6,14},{7,15},{8,0},{9,1},... | collective-permute-start | bytes 98312 | tf_op jit(solution)/shard_map/ppermute | solution.py:264
  (20 other events, 298.2 us)

commit v3 on v2

--- a/solution.py
+++ b/solution.py
@@ -8,6 +8,7 @@
 from jax.experimental.pallas import tpu as pltpu
 from jax.sharding import PartitionSpec as P
 
+
 GROUPS = 4
 
 
@@ -17,10 +18,6 @@
 
 f32 = jnp.float32
 bf16 = jnp.bfloat16
-
-
-def full(shape):
-    return pl.BlockSpec(shape, lambda *_: (0,) * len(shape))
 
 
 def rms_rows(values, gain):
@@ -69,11 +66,11 @@
 
 def state_kernel(
     channel,
-    key_ref,
-    query_ref,
-    value_ref,
+    lanes,
+    arrived_ref,
     decay_ref,
     rate_ref,
+    tail_ref,
     erase_ref,
     substitute_ref,
     extra_ref,
@@ -81,99 +78,125 @@
     state_ref,
     new_ref,
     mixed_ref,
+    memory,
     erase2,
     write2,
     replace2,
     query2,
     decay2,
+    value2,
+    spare,
+    values,
     readout,
+    in_sems,
+    out_sems,
 ):
-    step = pl.program_id(0)
-    seqs, heads, width = state_ref.shape
+    seqs, heads, width = memory.shape
     rows = seqs * heads
     span = 256
-
-    def flat(x):
-        return x.astype(f32).reshape(rows, channel)
-
-    def twice(x):
-        return jnp.concatenate([x, x], axis=-1)
-
-    @pl.when(step == 0)
-    def _():
-        key = flat(key_ref[...])
-        rate = flat(rate_ref[...])
-        erase = (key.reshape(seqs, heads, channel) * erase_ref[...][None]).reshape(rows, channel)
-        erase = erase * lax.rsqrt(jnp.sum(erase * erase, axis=-1, keepdims=True) + unit_eps)
-        gain = jnp.broadcast_to(substitute_ref[...][None], (seqs, heads, channel)).reshape(
-            rows, channel
-        )
-        replace = key * (1.0 + (rate - 1.0) * gain)
-        erase2[...] = twice(erase)
-        write2[...] = twice(erase * rate)
-        replace2[...] = twice(replace)
-        query2[...] = twice(flat(query_ref[...]))
-        decay2[...] = twice(flat(decay_ref[...]))
-        readout[...] = jnp.zeros_like(readout)
+    tile = 2 * channel
+    chunks = width // lanes
+    parts = lanes // span
+
+    def copy_in(c):
+        at = pl.ds(pl.multiple_of(c * lanes, lanes), lanes)
+        return pltpu.make_async_copy(state_ref.at[:, :, at], memory.at[:, :, at], in_sems.at[c])
+
+    def copy_out(c):
+        at = pl.ds(pl.multiple_of(c * lanes, lanes), lanes)
+        return pltpu.make_async_copy(memory.at[:, :, at], new_ref.at[:, :, at], out_sems.at[c])
+
+    for c in range(chunks):
+        copy_in(c).start()
+
+    lower = lax.broadcasted_iota(jnp.int32, (seqs, tile), 1) < channel
+
+    def lay(target, block, pair):
+        turned = pltpu.roll(block, channel, 1)
+        target[pl.ds(2 * pair, seqs, stride=heads), :] = jnp.where(lower, block, turned)
+        target[pl.ds(2 * pair + 1, seqs, stride=heads), :] = jnp.where(lower, turned, block)
+
+    for pair in range(heads // 2):
+        block = arrived_ref[pair * seqs : (pair + 1) * seqs, :].astype(f32)
+        for m, target in enumerate((query2, replace2, value2)):
+            lay(target, block[:, m * tile : (m + 1) * tile], pair)
+        lay(decay2, decay_ref[:, pair * tile : (pair + 1) * tile], pair)
+        lay(spare, rate_ref[:, pair * tile : (pair + 1) * tile], pair)
+
+    def over_rows(ref):
+        return jnp.broadcast_to(ref[...][None], (seqs, heads, tile)).reshape(rows, tile)
+
+    def head_sum(x):
+        return 0.5 * jnp.sum(x, axis=-1, keepdims=True)
+
+    key, rate = replace2[...], spare[...]
+    erase = key * over_rows(erase_ref)
+    erase = erase * lax.rsqrt(head_sum(erase * erase) + unit_eps)
+    erase2[...] = erase
+    write2[...] = erase * rate
+    replace = key * (1.0 + (rate - 1.0) * over_rows(substitute_ref))
+    replace2[...] = replace
+    spare[...] = head_sum(query2[...] * replace * over_rows(extra_ref)) * value2[...]
+    values[...] = value2[:, :channel].astype(bf16)
+    readout[...] = jnp.zeros_like(readout)
 
     def wide(ref):
-        return jnp.concatenate([ref[...]] * (span // (2 * channel)), axis=-1)
-
-    across = lax.broadcasted_iota(jnp.int32, (span, span), 0) // channel
-    down = lax.broadcasted_iota(jnp.int32, (span, span), 1) // channel
-    block_ones = (across == down).astype(f32).astype(bf16)
-    value = value_ref[...].reshape(rows, channel)
-    for part in range(width // span):
-        lanes = slice(part * span, (part + 1) * span)
-        first = (step * width + part * span) // channel
-        spread = (
-            (
-                lax.broadcasted_iota(jnp.int32, (channel, span), 0)
-                == lax.broadcasted_iota(jnp.int32, (channel, span), 1) // channel + first
+        return jnp.concatenate([ref[...]] * (span // tile), axis=-1)
+
+    def iota(shape, axis):
+        return lax.broadcasted_iota(jnp.int32, shape, axis)
+
+    def mask(chosen):
+        return chosen.astype(f32).astype(bf16)
+
+    block_ones = mask(iota((span, span), 0) // channel == iota((span, span), 1) // channel)
+
+    def chunk(c, carry):
+        copy_in(c).wait()
+        for part in range(parts):
+            at = pl.multiple_of(c * lanes + part * span, span)
+            first = at // channel
+            spread = mask(
+                iota((channel, span), 0) == iota((channel, span), 1) // channel + first
             )
-            .astype(f32)
-            .astype(bf16)
-        )
-        collect = (
-            (
-                lax.broadcasted_iota(jnp.int32, (span, channel), 0) // channel + first
-                == lax.broadcasted_iota(jnp.int32, (span, channel), 1)
+            collect = mask(
+                iota((span, channel), 0) // channel + first == iota((span, channel), 1)
             )
-            .astype(f32)
-            .astype(bf16)
-        )
-        memory = state_ref[:, :, lanes].reshape(rows, span)
-        removed = jnp.dot(
-            (memory * wide(erase2)).astype(bf16), block_ones, preferred_element_type=f32
-        )
-        value_wide = jnp.dot(value, spread, preferred_element_type=f32)
-        memory = (
-            memory * wide(decay2) - removed * wide(write2) + value_wide * wide(replace2)
-        )
-        new_ref[:, :, lanes] = memory.reshape(seqs, heads, span)
-        readout[...] += split_dot(memory * wide(query2), collect)
-
-    @pl.when(step == pl.num_programs(0) - 1)
-    def _():
-        result = readout[...]
-        centered = result - jnp.mean(result, axis=-1, keepdims=True)
-        variance = jnp.mean(centered * centered, axis=-1, keepdims=True)
-        gain = jnp.broadcast_to(attend_ref[...][None], (seqs, heads, channel)).reshape(
-            rows, channel
-        )
-        extra = jnp.broadcast_to(extra_ref[...][None], (seqs, heads, channel)).reshape(
-            rows, channel
-        )
-        bonus = jnp.sum(
-            query2[:, :channel] * replace2[:, :channel] * extra, axis=-1, keepdims=True
-        )
-        mixed = centered * lax.rsqrt(variance + group_eps) * gain + bonus * value.astype(f32)
-        mixed_ref[...] = mixed.astype(bf16).reshape(seqs, heads, channel)
-
-
-def output_kernel(room, members, where_ref, *refs):
-    mixed_refs, (own_ref, near_ref, far_ref) = refs[:GROUPS], refs[GROUPS : GROUPS + 3]
-    part_refs, (pick_ref, tail_ref, mixed, result) = refs[GROUPS + 3 : 2 * GROUPS + 3], refs[2 * GROUPS + 3 :]
+            grid = memory[:, :, pl.ds(at, span)].reshape(rows, span)
+            removed = jnp.dot(
+                (grid * wide(erase2)).astype(bf16), block_ones, preferred_element_type=f32
+            )
+            value_wide = jnp.dot(values[...], spread, preferred_element_type=f32)
+            grid = grid * wide(decay2) - removed * wide(write2) + value_wide * wide(replace2)
+            memory[:, :, pl.ds(at, span)] = grid.reshape(seqs, heads, span)
+            readout[...] += split_dot(grid * wide(query2), collect)
+        copy_out(c).start()
+        return carry
+
+    lax.fori_loop(0, chunks, chunk, 0)
+
+    result = readout[...]
+    centered = result - jnp.mean(result, axis=-1, keepdims=True)
+    variance = jnp.mean(centered * centered, axis=-1, keepdims=True)
+    gain = over_rows(attend_ref)[:, :channel]
+    mixed = centered * lax.rsqrt(variance + group_eps) * gain + spare[:, :channel]
+    spare[:, :channel] = mixed
+    for pair in range(heads // 2):
+        left = spare[pl.ds(2 * pair, seqs, stride=heads), :]
+        right = spare[pl.ds(2 * pair + 1, seqs, stride=heads), :]
+        mixed_ref[:, pair * tile : (pair + 1) * tile] = jnp.where(
+            lower, left, pltpu.roll(right, channel, 1)
+        ).astype(bf16)
+    mixed_ref[:, heads * channel :] = tail_ref[...]
+    for c in range(chunks):
+        copy_out(c).wait()
+
+
+def output_kernel(room, members, chips, where_ref, *refs):
+    mixed_refs, own_ref, refs = refs[:GROUPS], refs[GROUPS], refs[GROUPS + 1 :]
+    others = chips - 1
+    near_refs, far_refs, refs = refs[:others], refs[others : 2 * others], refs[2 * others :]
+    part_refs, (pick_ref, tail_ref, mixed, result) = refs[:GROUPS], refs[GROUPS:]
     plane, place, core = where_ref[0], where_ref[1], where_ref[2]
     columns, depth = own_ref.shape
     half = depth // 2
@@ -183,11 +206,13 @@
         mixed[k * seqs : (k + 1) * seqs, :] = ref[...]
     near = mixed[:, pl.ds(pl.multiple_of(core * half, half), half)]
     far = mixed[:, pl.ds(pl.multiple_of((1 - core) * half, half), half)]
-    for kp in range(near_ref.shape[0] + 1):
+    for kp in range(chips):
         if kp == 0:
             block = turned_dot(mixed[:, :depth], own_ref[...])
         else:
-            block = turned_dot(near, near_ref[kp - 1]) + turned_dot(far, far_ref[kp - 1])
+            block = turned_dot(near, near_refs[kp - 1][...]) + turned_dot(
+                far, far_refs[kp - 1][...]
+            )
         at = pl.multiple_of((place ^ kp) * columns, columns)
         result[:, pl.ds(at, columns)] = block.astype(bf16)
 
@@ -313,7 +338,10 @@
     own_maps = [m.T for m in (query_map, lookup_map, content_map, result_map)]
     pair_maps = [swap(m, 1) for m in own_maps]
 
-    normed = rms_rows(line_rows[:seqs].astype(f32), earlier_rescale_gain)
+    late_rows, late_picks, late_shares, _ = lax.optimization_barrier(
+        (latest_embeddings, picked_specialists, specialist_picked_shares, line_rows)
+    )
+    normed = rms_rows(late_rows.astype(f32), earlier_rescale_gain)
     decay_low = jnp.tanh(
         jnp.dot(normed, forget_lower_map, preferred_element_type=f32)
     ).astype(bf16)
@@ -322,18 +350,17 @@
         * jax.nn.sigmoid(
             forget_shift + jnp.dot(decay_low, forget_upper_map, preferred_element_type=f32)
         )
-    ).reshape(seqs, heads, channel)
+    )
     rate_low = jnp.dot(normed, adapt_lower_map, preferred_element_type=f32).astype(bf16)
     rate = jax.nn.sigmoid(
         adapt_shift + jnp.dot(rate_low, adapt_upper_map, preferred_element_type=f32)
-    ).reshape(seqs, heads, channel)
-
-    top_count = picked_specialists.shape[1]
-    group = picked_specialists[:, 0] // members
+    )
+
+    group = late_picks[:, 0] // members
     share_at = (
-        picked_specialists[:, :, None] % members == jnp.arange(members, dtype=jnp.int32)
+        late_picks[:, :, None] % members == jnp.arange(members, dtype=jnp.int32)
     ).astype(f32)
-    shares = jnp.sum(share_at * specialist_picked_shares[:, :, None], axis=1)
+    shares = jnp.sum(share_at * late_shares[:, :, None], axis=1)
     share_high = shares.astype(bf16)
     share_low = (shares - share_high.astype(f32)).astype(bf16)
     tail_width = -(-(2 * members + 1) // 128) * 128
@@ -360,12 +387,6 @@
     arrived = lax.all_to_all(
         projected, "ep", split_axis=0, concat_axis=0, tiled=True, axis_index_groups=same_core
     )
-    signals = (
-        arrived.reshape(devices // 2, seqs, 3, heads * 2 // devices, channel)
-        .transpose(2, 1, 0, 3, 4)
-        .reshape(3, seqs, heads, channel)
-    )
-
     chip_map = jnp.where(
         core == 0,
         jnp.concatenate([own_maps[3], pair_maps[3]], axis=0),
@@ -373,51 +394,56 @@
     )
     half = lax.dynamic_slice_in_dim(chip_map, core * (width // 2), width // 2, axis=1)
     half, _ = lax.optimization_barrier((half, projected))
-    near = jnp.stack([swap(half, 2 * k) for k in range(1, chips)])
-    far = swap(near, 1)
+    near = [swap(half, 2 * k) for k in range(1, chips)]
 
     lanes = 1024
-    small = pl.BlockSpec((seqs, heads, channel), lambda i: (0, 0, 0))
-    gains = pl.BlockSpec((heads, channel), lambda i: (0, 0))
-    block = pl.BlockSpec((seqs, heads, lanes), lambda i: (0, 0, i))
-    tile = pltpu.VMEM((seqs * heads, 2 * channel), f32)
-    new_state, mixed = pl.pallas_call(
-        functools.partial(state_kernel, channel),
-        grid=(channel * channel // lanes,),
+    rows = seqs * heads
+
+    def twice(gains):
+        gains = gains.reshape(heads, channel)
+        return jnp.concatenate([gains, gains], axis=1)
+
+    hbm = pl.BlockSpec(memory_space=pltpu.HBM)
+    tile = pltpu.VMEM((rows, 2 * channel), f32)
+    sems = pltpu.SemaphoreType.DMA((channel * channel // lanes,))
+    new_state, mixed_rows = pl.pallas_call(
+        functools.partial(state_kernel, channel, lanes),
         out_shape=[
             jax.ShapeDtypeStruct(prior_memory_grids.shape, f32),
-            jax.ShapeDtypeStruct((seqs, heads, channel), bf16),
+            jax.ShapeDtypeStruct((seqs, width + tail_width), bf16),
         ],
-        in_specs=[small] * 5 + [gains] * 4 + [block],
-        out_specs=[block, small],
-        scratch_shapes=[tile] * 5 + [pltpu.VMEM((seqs * heads, channel), f32)],
-        compiler_params=limit(32),
+        in_specs=[vmem] * 8 + [hbm],
+        out_specs=[hbm, vmem],
+        scratch_shapes=[pltpu.VMEM(prior_memory_grids.shape, f32)]
+        + [tile] * 7
+        + [pltpu.VMEM((rows, channel), bf16), pltpu.VMEM((rows, channel), f32), sems, sems],
+        compiler_params=limit(57),
         name="state",
     )(
-        signals[1],
-        signals[0],
-        signals[2],
+        arrived,
         decay,
         rate,
-        erase_lookup_gains.reshape(heads, channel),
-        substitute_lookup_gains.reshape(heads, channel),
-        present_extra_gains.reshape(heads, channel),
-        attender_rescale_gain.reshape(heads, channel),
+        tail,
+        twice(erase_lookup_gains),
+        twice(substitute_lookup_gains),
+        twice(present_extra_gains),
+        twice(attender_rescale_gain),
         prior_memory_grids,
     )
 
-    mixed_rows = jnp.concatenate([mixed.reshape(seqs, width), tail], axis=1)
     mixed_line = [mixed_rows] + [swap(mixed_rows, members * k) for k in range(1, GROUPS)]
+    near, _ = lax.optimization_barrier((near, mixed_rows))
+    far = [swap(part, 1) for part in near]
     room = (seqs + 1) // 2
     count = GROUPS * room
     *parts, pick, chosen_tail = pl.pallas_call(
-        functools.partial(output_kernel, room, members),
+        functools.partial(output_kernel, room, members, chips),
         out_shape=[jax.ShapeDtypeStruct((count, width // GROUPS), bf16)] * GROUPS
         + [
             jax.ShapeDtypeStruct((count, GROUPS * seqs), bf16),
             jax.ShapeDtypeStruct((count, tail_width), bf16),
         ],
-        in_specs=[smem] + [vmem] * (GROUPS + 3),
+        in_specs=[smem] + [vmem] * (GROUPS + 1 + 2 * (chips - 1)),
         out_specs=[vmem] * (GROUPS + 2),
         scratch_shapes=[
             pltpu.VMEM((GROUPS * seqs, width + tail_width), bf16),
@@ -425,7 +451,7 @@
         ],
         compiler_params=limit(16),
         name="output",
-    )(where, *mixed_line, chip_map, near, far)
+    )(where, *mixed_line, chip_map, *near, *far)
     parts = [parts[0]] + [swap(parts[k], members * k) for k in range(1, GROUPS)]
     chosen_rows = jnp.dot(pick, line_rows, preferred_element_type=f32).astype(bf16)
     chosen, residual = pl.pallas_call(

time: 129 us -> 120 us (0.930)
  waiting for transfers between devices: 50.5 us -> 41.2 us
  local copies, waits for them, and re-layouts: 11.9 us -> 7.41 us
  Pallas kernels: 15.2 us -> 18.3 us
  starting transfers between devices: 41.8 us -> 39.8 us
  other arithmetic: 4.38 us -> 6.3 us
  matrix products: 3.98 us -> 5.3 us
    ppermute x34 -> x36, waiting for transfers between devices: 41.7 us -> 35.9 us  [swap(): return lax.ppermute(rows, 'ep', [(i, i ^ mask) for i in range(count)])]
    unnamed x38 -> x31, local copies, waits for them, and re-layouts: 7.57 us -> 2.47 us
    all_to_all x1, waiting for transfers between devices: 8.81 us -> 5.24 us  [layered(): lax.all_to_all(projected, 'ep', split_axis=0, concat_axis=0, tiled=True,...]
    pallas_call x2, Pallas kernels: 9.78 us -> 12.8 us  [the longest x1 10.8 us: layered(): pl.pallas_call(functools.partial(state_kernel, channel, lanes), out_shape...]
    ppermute x34 -> x36, starting transfers between devices: 35.9 us -> 33 us  [swap(): return lax.ppermute(rows, 'ep', [(i, i ^ mask) for i in range(count)])]
    slice x5 -> x0, local copies, waits for them, and re-layouts: 2.27 us -> none  [the longest x2 1.39 us: layered(): signals[2]]
    concatenate x0 -> x3, other arithmetic: none -> 2.05 us  [the longest x2 1.37 us: twice(): return jnp.concatenate([gains, gains], axis=1)]
    reshape x8 -> x4, local copies, waits for them, and re-layouts: 1.63 us -> 3.07 us  [twice(): gains = gains.reshape(heads, channel)]
  transfers between devices with their start and end apart: 35 -> 37, of which waited for: 19 -> 20; matrix products, arithmetic and copies ran while one was open for 10% -> 14% of each run, Pallas kernels for 6% -> 9%
where the time goes in v3:
time: 120 us; the launch traced here: 119 us
  waiting for transfers between devices  41.2 us (34%)
  starting transfers between devices  39.8 us (33%)
  Pallas kernels  18.3 us (15%)
  local copies, waits for them, and re-layouts  7.41 us (6%)
  other arithmetic  6.3 us (5%)
  matrix products  5.3 us (4%)
    ppermute x36, waiting for transfers between devices, swap(): return lax.ppermute(rows, 'ep', [(i, i ^ mask) for i in range(count)])  35.9 us
    ppermute x36, starting transfers between devices, swap(): return lax.ppermute(rows, 'ep', [(i, i ^ mask) for i in range(count)])  33 us
    pallas_call x1, Pallas kernels, layered(): pl.pallas_call(functools.partial(state_kernel, channel, lanes), out_shape...  10.8 us
    all_to_all x1, starting transfers between devices, layered(): lax.all_to_all(projected, 'ep', split_axis=0, concat_axis=0, tiled=True,...  6.82 us
    all_to_all x1, waiting for transfers between devices, layered(): lax.all_to_all(projected, 'ep', split_axis=0, concat_axis=0, tiled=True,...  5.24 us
    reshape x4, local copies, waits for them, and re-layouts, twice(): gains = gains.reshape(heads, channel)  3.07 us
    unnamed x31, local copies, waits for them, and re-layouts  2.47 us
    pallas_call x1, Pallas kernels, layered(): pl.pallas_call(functools.partial(expert_kernel, members), out_shape=[jax....  2.43 us
  transfers between devices with their start and end apart: 37, of which 20 were waited for; matrix products, arithmetic and copies ran while one was open for 14% of the time, Pallas kernels for 9%

profile of v3, /device:TPU:0, one launch (start us, length us, event | category | flops | bytes accessed | tf_op | source)
XLA Modules:
  0.0 119.3 jit_solution(5484003174619709869)
XLA Ops:
  0.7 5.1 %collective-permute-start.2 = (bf16[16,2048]{1,0:T(8,128)(2,1)}, bf16[16,2048]{1,0:T(8,128)(2,1)S(1)}, u32[]{:S(2)}, u32[]{:S(2)}) collective-permute-start(bf16[16,2048]{1,0:T(8,128)(2,1)} %param.23), channel_id=1, source_target_pairs={{0,24},{1,25},{2,26},{3,27},{4,28},{5,29},{6,30},{7,31},{8,16},{9,... | collective-permute-start | bytes 196616 | tf_op jit(solution)/shard_map/ppermute | solution.py:289
  15.3 2.6 %collective-permute-start.5 = (bf16[64,2048]{1,0:T(8,128)(2,1)S(1)}, bf16[64,2048]{1,0:T(8,128)(2,1)S(1)}, u32[]{:S(2)}, u32[]{:S(2)}) collective-permute-start(bf16[64,2048]{1,0:T(8,128)(2,1)S(1)} %constant_dynamic-update-slice_fusion.refs_0_), channel_id=1, source_target_pairs={{0,6},{1,7},{2,4},{3,5},{4,2},{5,3},{6,0},{7,1},{8,14},{9,15},{10,... | collective-permute-start | bytes 786440 | tf_op jit(solution)/shard_map/ppermute | solution.py:289
  17.9 1.0 fusion.11
  19.5 2.1 %fusion.3.rate_ref = f32[16,2048]{1,0:T(8,128)} fusion(bf16[64,2048]{1,0:T(8,128)(2,1)S(1)} %copy-done, bf16[2048,64]{0,1:T(8,128)(2,1)} %param.32, f32[2048]{0:T(1024)} %param.34, bf16[16,2048]{1,0:T(8,128)(2,1)} %param.23, f32[2048]{0:T(1024)} %param.25, f32[16]{0:T(128)S(1)} %add_rsqrt_fusion), kind=kOutput, calls=%fused_computation.5 | convolution fusion | flops 8651776 | bytes 737344 | tf_op jit(solution)/shard_map/dot_general | solution.py:356
  22.6 1.1 maximum_select_fusion.refs_4_
  24.6 5.4 %collective-permute-done.4.refs_2_ = bf16[64,2048]{1,0:T(8,128)(2,1)S(1)} collective-permute-done((bf16[64,2048]{1,0:T(8,128)(2,1)S(1)}, bf16[64,2048]{1,0:T(8,128)(2,1)S(1)}, u32[]{:S(2)}, u32[]{:S(2)}) %collective-permute-start.4) | collective-permute-done | bytes 262176 | tf_op jit(solution)/shard_map/ppermute | solution.py:289
  30.3 2.3 %project.1 = bf16[256,384]{1,0:T(8,128)(2,1)} custom-call(s32[4]{0:T(128)S(1)} %pad_add_fusion.where_ref, bf16[64,2048]{1,0:T(8,128)(2,1)S(1)} %constant_dynamic-update-slice_fusion.refs_0_, bf16[64,2048]{1,0:T(8,128)(2,1)S(1)} %collective-permute-done.3.refs_1_, bf16[64,2048]{1,0:T(8,128)(2,1)S(1)} %collective-permute-done.4.refs_2_, ...), custom_call_target="tpu_custom_call" | custom-call | tf_op jit(solution)/shard_map/project/pallas_call | solution.py:378
  32.6 2.4 %collective-permute-start.15 = (bf16[128,1024]{1,0:T(8,128)(2,1)}, bf16[128,1024]{1,0:T(8,128)(2,1)S(1)}, u32[]{:S(2)}, u32[]{:S(2)}) collective-permute-start(bf16[128,1024]{1,0:T(8,128)(2,1)} %constant_dynamic-slice_fusion), channel_id=1, source_target_pairs={{0,6},{1,7},{2,4},{3,5},{4,2},{5,3},{6,0},{7,1},{8,14},{9,15},{10,... | collective-permute-start | bytes 786440 | tf_op jit(solution)/shard_map/ppermute | solution.py:289
  36.1 6.8 %all-to-all-start = ((bf16[16,16,384]{2,1,0:T(8,128)(2,1)}), bf16[16,16,384]{2,1,0:T(8,128)(2,1)S(1)}, u32[]{:S(2)}, u32[]{:S(2)}) async-start(bf16[16,16,384]{2,1,0:T(8,128)(2,1)} %bitcast.9), calls=%async_computation | async-start | bytes 393216 | tf_op jit(solution)/shard_map/all_to_all | solution.py:387
  43.6 2.2 %fusion.9.decay_ref = f32[16,2048]{1,0:T(8,128)} fusion(bf16[64,2048]{1,0:T(8,128)(2,1)} %param.30, bf16[2048,64]{0,1:T(8,128)(2,1)} %param.29, f32[2048]{0:T(1024)S(1)} %copy-done.13, bf16[16,2048]{1,0:T(8,128)(2,1)S(1)} %copy-done.11, f32[2048]{0:T(1024)S(1)} %copy-done.8, f32[16]{0:T(128)S(1)} %add_rsqrt_fusion), kind=kOutput, calls=%fused_computation.12 | convolution fusion | flops 8684544 | bytes 737344 | tf_op jit(solution)/shard_map/dot_general | solution.py:351
  45.7 5.2 %all-to-all-done = bf16[16,16,384]{2,1,0:T(8,128)(2,1)S(1)} async-done(((bf16[16,16,384]{2,1,0:T(8,128)(2,1)}), bf16[16,16,384]{2,1,0:T(8,128)(2,1)S(1)}, u32[]{:S(2)}, u32[]{:S(2)}) %all-to-all-start) | async-done | bytes 196640 | tf_op jit(solution)/shard_map/all_to_all | solution.py:387
  51.6 10.8 %state.1 = (f32[16,32,4096]{2,1,0:T(8,128)}, bf16[16,2176]{1,0:T(8,128)(2,1)}) custom-call(bf16[256,384]{1,0:T(8,128)(2,1)} %bitcast.27, f32[16,2048]{1,0:T(8,128)} %fusion.9.decay_ref, f32[16,2048]{1,0:T(8,128)} %fusion.3.rate_ref, bf16[16,128]{1,0:T(8,128)(2,1)} %maximum_maximum_fusion.tail_ref, f32[32,128]{1,0:T(8,128)} %get-tuple-element.51.erase_ref, ...), custom_call_target="tpu_custom_call" | custom-call | tf_op jit(solution)/shard_map/state/pallas_call | solution.py:409
  63.1 2.3 %collective-permute-start.11 = (bf16[16,2176]{1,0:T(8,128)(2,1)}, bf16[16,2176]{1,0:T(8,128)(2,1)S(1)}, u32[]{:S(2)}, u32[]{:S(2)}) collective-permute-start(bf16[16,2176]{1,0:T(8,128)(2,1)} %get-tuple-element.24.refs_0_), channel_id=1, source_target_pairs={{0,24},{1,25},{2,26},{3,27},{4,28},{5,29},{6,30},{7,31},{8,16},{9,... | collective-permute-start | bytes 208904 | tf_op jit(solution)/shard_map/ppermute | solution.py:289
  65.4 4.8 %collective-permute-done.11.refs_3_ = bf16[16,2176]{1,0:T(8,128)(2,1)S(1)} collective-permute-done((bf16[16,2176]{1,0:T(8,128)(2,1)}, bf16[16,2176]{1,0:T(8,128)(2,1)S(1)}, u32[]{:S(2)}, u32[]{:S(2)}) %collective-permute-start.11) | collective-permute-done | bytes 69664 | tf_op jit(solution)/shard_map/ppermute | solution.py:289
  70.3 2.4 %collective-permute-done.10.refs_2_ = bf16[16,2176]{1,0:T(8,128)(2,1)S(1)} collective-permute-done((bf16[16,2176]{1,0:T(8,128)(2,1)}, bf16[16,2176]{1,0:T(8,128)(2,1)S(1)}, u32[]{:S(2)}, u32[]{:S(2)}) %collective-permute-start.10) | collective-permute-done | bytes 69664 | tf_op jit(solution)/shard_map/ppermute | solution.py:289
  72.7 2.1 %collective-permute-done.9.refs_1_ = bf16[16,2176]{1,0:T(8,128)(2,1)S(1)} collective-permute-done((bf16[16,2176]{1,0:T(8,128)(2,1)}, bf16[16,2176]{1,0:T(8,128)(2,1)S(1)}, u32[]{:S(2)}, u32[]{:S(2)}) %collective-permute-start.9) | collective-permute-done | bytes 69664 | tf_op jit(solution)/shard_map/ppermute | solution.py:289
  75.7 2.1 %output.1 = (bf16[32,512]{1,0:T(8,128)(2,1)S(1)}, bf16[32,512]{1,0:T(8,128)(2,1)S(1)}, bf16[32,512]{1,0:T(8,128)(2,1)S(1)}, bf16[32,512]{1,0:T(8,128)(2,1)S(1)},...) custom-call(s32[4]{0:T(128)S(1)} %pad_add_fusion.where_ref, bf16[16,2176]{1,0:T(8,128)(2,1)S(1)} %copy-done.7, ...), custom_call_target="tpu_custom_call" | custom-call | tf_op jit(solution)/shard_map/output/pallas_call | solution.py:439
  77.8 2.9 %collective-permute-start.20 = (bf16[32,512]{1,0:T(8,128)(2,1)S(1)}, bf16[32,512]{1,0:T(8,128)(2,1)S(1)}, u32[]{:S(2)}, u32[]{:S(2)}) collective-permute-start(bf16[32,512]{1,0:T(8,128)(2,1)S(1)} %get-tuple-element.31), channel_id=1, source_target_pairs={{0,16},{1,17},{2,18},{3,19},{4,20},{5,21},{6,22},{7,23},{8,24},{9,... | collective-permute-start | bytes 98312 | tf_op jit(solution)/shard_map/ppermute | solution.py:289
  80.7 1.5 %collective-permute-start.21 = (bf16[32,512]{1,0:T(8,128)(2,1)S(1)}, bf16[32,512]{1,0:T(8,128)(2,1)S(1)}, u32[]{:S(2)}, u32[]{:S(2)}) collective-permute-start(bf16[32,512]{1,0:T(8,128)(2,1)S(1)} %get-tuple-element.32), channel_id=1, source_target_pairs={{0,24},{1,25},{2,26},{3,27},{4,28},{5,29},{6,30},{7,31},{8,16},{9,... | collective-permute-start | bytes 98312 | tf_op jit(solution)/shard_map/ppermute | solution.py:289
  82.7 3.7 %collective-permute-done.21.refs_3_ = bf16[32,512]{1,0:T(8,128)(2,1)S(1)} collective-permute-done((bf16[32,512]{1,0:T(8,128)(2,1)S(1)}, bf16[32,512]{1,0:T(8,128)(2,1)S(1)}, u32[]{:S(2)}, u32[]{:S(2)}) %collective-permute-start.21) | collective-permute-done | bytes 32800 | tf_op jit(solution)/shard_map/ppermute | solution.py:289
  87.1 2.5 %collective-permute-start.24 = (bf16[32,2176]{1,0:T(8,128)(2,1)S(1)}, bf16[32,2176]{1,0:T(8,128)(2,1)S(1)}, u32[]{:S(2)}, u32[]{:S(2)}) collective-permute-start(bf16[32,2176]{1,0:T(8,128)(2,1)S(1)} %get-tuple-element.36.refs_0_), channel_id=1, source_target_pairs={{0,6},{1,7},{2,4},{3,5},{4,2},{5,3},{6,0},{7,1},{8,14},{9,15},{10,... | collective-permute-start | bytes 417800 | tf_op jit(solution)/shard_map/ppermute | solution.py:289
  90.7 2.5 %collective-permute-done.24.refs_3_ = bf16[32,2176]{1,0:T(8,128)(2,1)S(1)} collective-permute-done((bf16[32,2176]{1,0:T(8,128)(2,1)S(1)}, bf16[32,2176]{1,0:T(8,128)(2,1)S(1)}, u32[]{:S(2)}, u32[]{:S(2)}) %collective-permute-start.24) | collective-permute-done | bytes 139296 | tf_op jit(solution)/shard_map/ppermute | solution.py:289
  93.2 1.5 %collective-permute-done.23.refs_2_ = bf16[32,2176]{1,0:T(8,128)(2,1)S(1)} collective-permute-done((bf16[32,2176]{1,0:T(8,128)(2,1)S(1)}, bf16[32,2176]{1,0:T(8,128)(2,1)S(1)}, u32[]{:S(2)}, u32[]{:S(2)}) %collective-permute-start.23) | collective-permute-done | bytes 139296 | tf_op jit(solution)/shard_map/ppermute | solution.py:289
  96.5 2.4 %expert.1 = (bf16[128,2048]{1,0:T(8,128)(2,1)S(1)}, bf16[128,2048]{1,0:T(8,128)(2,1)S(1)}) custom-call(s32[4]{0:T(128)S(1)} %pad_add_fusion.where_ref, bf16[32,2176]{1,0:T(8,128)(2,1)S(1)} %get-tuple-element.36.refs_0_, bf16[32,2176]{1,0:T(8,128)(2,1)S(1)} %collective-permute-done.22.refs_1_, bf16[32,2176]{1,0:T(8,128)(2,1)S(1)} %collective-permute-done.23.refs_2_, ...), custom_call_target="tpu_custom_call" | custom-call | tf_op jit(solution)/shard_map/expert/pallas_call | solution.py:472
  99.2 1.8 %collective-permute-done.29 = bf16[128,2048]{1,0:T(8,128)(2,1)S(1)} collective-permute-done((bf16[128,2048]{1,0:T(8,128)(2,1)S(1)}, bf16[128,2048]{1,0:T(8,128)(2,1)S(1)}, u32[]{:S(2)}, u32[]{:S(2)}) %collective-permute-start.29) | collective-permute-done | bytes 524320 | tf_op jit(solution)/shard_map/ppermute | solution.py:289
  101.1 1.2 collective-permute-start.30
  102.3 1.9 %collective-permute-start.32 = (bf16[32,2048]{1,0:T(8,128)(2,1)S(1)}, bf16[32,2048]{1,0:T(8,128)(2,1)S(1)}, u32[]{:S(2)}, u32[]{:S(2)}) collective-permute-start(bf16[32,2048]{1,0:T(8,128)(2,1)S(1)} %get-tuple-element.43), channel_id=1, source_target_pairs={{0,6},{1,7},{2,4},{3,5},{4,2},{5,3},{6,0},{7,1},{8,14},{9,15},{10,... | collective-permute-start | bytes 393224 | tf_op jit(solution)/shard_map/ppermute | solution.py:289
  104.7 2.9 %collective-permute-done.30 = bf16[32,2048]{1,0:T(8,128)(2,1)S(1)} collective-permute-done((bf16[32,2048]{1,0:T(8,128)(2,1)S(1)}, bf16[32,2048]{1,0:T(8,128)(2,1)S(1)}, u32[]{:S(2)}, u32[]{:S(2)}) %collective-permute-start.30) | collective-permute-done | bytes 131104 | tf_op jit(solution)/shard_map/ppermute | solution.py:289
  107.6 3.0 %collective-permute-done.32 = bf16[32,2048]{1,0:T(8,128)(2,1)S(1)} collective-permute-done((bf16[32,2048]{1,0:T(8,128)(2,1)S(1)}, bf16[32,2048]{1,0:T(8,128)(2,1)S(1)}, u32[]{:S(2)}, u32[]{:S(2)}) %collective-permute-start.32) | collective-permute-done | bytes 131104 | tf_op jit(solution)/shard_map/ppermute | solution.py:289
  110.6 1.4 %collective-permute-done.31 = bf16[32,2048]{1,0:T(8,128)(2,1)S(1)} collective-permute-done((bf16[32,2048]{1,0:T(8,128)(2,1)S(1)}, bf16[32,2048]{1,0:T(8,128)(2,1)S(1)}, u32[]{:S(2)}, u32[]{:S(2)}) %collective-permute-start.31) | collective-permute-done | bytes 131104 | tf_op jit(solution)/shard_map/ppermute | solution.py:289
  112.7 3.8 %collective-permute-start.33 = (bf16[8,2048]{1,0:T(8,128)(2,1)S(1)}, bf16[8,2048]{1,0:T(8,128)(2,1)S(1)}, u32[]{:S(2)}, u32[]{:S(2)}) collective-permute-start(bf16[8,2048]{1,0:T(8,128)(2,1)S(1)} %get-tuple-element.48), channel_id=1, source_target_pairs={{0,8},{1,9},{2,10},{3,11},{4,12},{5,13},{6,14},{7,15},{8,0},{9,1},... | collective-permute-start | bytes 98312 | tf_op jit(solution)/shard_map/ppermute | solution.py:289
  116.5 1.4 %collective-permute-done.35 = bf16[8,2048]{1,0:T(8,128)(2,1)S(1)} collective-permute-done((bf16[8,2048]{1,0:T(8,128)(2,1)S(1)}, bf16[8,2048]{1,0:T(8,128)(2,1)S(1)}, u32[]{:S(2)}, u32[]{:S(2)}) %collective-permute-start.35) | collective-permute-done | bytes 32800 | tf_op jit(solution)/shard_map/ppermute | solution.py:289
  (113 shorter events, 23.3 us)
Async XLA Ops:
  0.7 12.4 %collective-permute-start.2 = (bf16[16,2048]{1,0:T(8,128)(2,1)}, bf16[16,2048]{1,0:T(8,128)(2,1)S(1)}, u32[]{:S(2)}, u32[]{:S(2)}) collective-permute-start(bf16[16,2048]{1,0:T(8,128)(2,1)} %param.23), channel_id=1, source_target_pairs={{0,24},{1,25},{2,26},{3,27},{4,28},{5,29},{6,30},{7,31},{8,16},{9,... | collective-permute-start | bytes 196616 | tf_op jit(solution)/shard_map/ppermute | solution.py:289
  5.8 6.6 %collective-permute-start.1 = (bf16[16,2048]{1,0:T(8,128)(2,1)}, bf16[16,2048]{1,0:T(8,128)(2,1)S(1)}, u32[]{:S(2)}, u32[]{:S(2)}) collective-permute-start(bf16[16,2048]{1,0:T(8,128)(2,1)} %param.23), channel_id=1, source_target_pairs={{0,16},{1,17},{2,18},{3,19},{4,20},{5,21},{6,22},{7,23},{8,24},{9,... | collective-permute-start | bytes 196616 | tf_op jit(solution)/shard_map/ppermute | solution.py:289
  5.8 6.6 %collective-permute-start = (bf16[16,2048]{1,0:T(8,128)(2,1)}, bf16[16,2048]{1,0:T(8,128)(2,1)S(1)}, u32[]{:S(2)}, u32[]{:S(2)}) collective-permute-start(bf16[16,2048]{1,0:T(8,128)(2,1)} %param.23), channel_id=1, source_target_pairs={{0,8},{1,9},{2,10},{3,11},{4,12},{5,13},{6,14},{7,15},{8,0},{9,1},... | collective-permute-start | bytes 196616 | tf_op jit(solution)/shard_map/ppermute | solution.py:289
  6.5 15.2 %collective-permute-start.6 = (bf16[64,2048]{1,0:T(8,128)(2,1)}, bf16[64,2048]{1,0:T(8,128)(2,1)S(1)}, u32[]{:S(2)}, u32[]{:S(2)}) collective-permute-start(bf16[64,2048]{1,0:T(8,128)(2,1)} %bitcast.19), channel_id=1, source_target_pairs={{0,1},{1,0},{2,3},{3,2},{4,5},{5,4},{6,7},{7,6},{8,9},{9,8},{10,11... | collective-permute-start | bytes 786440 | tf_op jit(solution)/shard_map/ppermute | solution.py:289
  6.5 18.0 %collective-permute-start.7 = (bf16[64,2048]{1,0:T(8,128)(2,1)}, bf16[64,2048]{1,0:T(8,128)(2,1)S(1)}, u32[]{:S(2)}, u32[]{:S(2)}) collective-permute-start(bf16[64,2048]{1,0:T(8,128)(2,1)} %bitcast.21), channel_id=1, source_target_pairs={{0,1},{1,0},{2,3},{3,2},{4,5},{5,4},{6,7},{7,6},{8,9},{9,8},{10,11... | collective-permute-start | bytes 786440 | tf_op jit(solution)/shard_map/ppermute | solution.py:289
  12.4 12.0 %collective-permute-start.8 = (bf16[64,2048]{1,0:T(8,128)(2,1)}, bf16[64,2048]{1,0:T(8,128)(2,1)S(1)}, u32[]{:S(2)}, u32[]{:S(2)}) collective-permute-start(bf16[64,2048]{1,0:T(8,128)(2,1)} %bitcast.23), channel_id=1, source_target_pairs={{0,1},{1,0},{2,3},{3,2},{4,5},{5,4},{6,7},{7,6},{8,9},{9,8},{10,11... | collective-permute-start | bytes 786440 | tf_op jit(solution)/shard_map/ppermute | solution.py:289
  12.5 9.7 %collective-permute-start.12 = (bf16[64,2048]{1,0:T(8,128)(2,1)}, bf16[64,2048]{1,0:T(8,128)(2,1)}, u32[]{:S(2)}, u32[]{:S(2)}) collective-permute-start(bf16[64,2048]{1,0:T(8,128)(2,1)} %bitcast.28), channel_id=1, source_target_pairs={{0,1},{1,0},{2,3},{3,2},{4,5},{5,4},{6,7},{7,6},{8,9},{9,8},{10,11... | collective-permute-start | bytes 786440 | tf_op jit(solution)/shard_map/ppermute | solution.py:289
  15.3 9.3 %collective-permute-start.5 = (bf16[64,2048]{1,0:T(8,128)(2,1)S(1)}, bf16[64,2048]{1,0:T(8,128)(2,1)S(1)}, u32[]{:S(2)}, u32[]{:S(2)}) collective-permute-start(bf16[64,2048]{1,0:T(8,128)(2,1)S(1)} %constant_dynamic-update-slice_fusion.refs_0_), channel_id=1, source_target_pairs={{0,6},{1,7},{2,4},{3,5},{4,2},{5,3},{6,0},{7,1},{8,14},{9,15},{10,... | collective-permute-start | bytes 786440 | tf_op jit(solution)/shard_map/ppermute | solution.py:289
  21.7 8.4 %collective-permute-start.4 = (bf16[64,2048]{1,0:T(8,128)(2,1)S(1)}, bf16[64,2048]{1,0:T(8,128)(2,1)S(1)}, u32[]{:S(2)}, u32[]{:S(2)}) collective-permute-start(bf16[64,2048]{1,0:T(8,128)(2,1)S(1)} %constant_dynamic-update-slice_fusion.refs_0_), channel_id=1, source_target_pairs={{0,4},{1,5},{2,6},{3,7},{4,0},{5,1},{6,2},{7,3},{8,12},{9,13},{10,... | collective-permute-start | bytes 786440 | tf_op jit(solution)/shard_map/ppermute | solution.py:289
  22.2 8.1 %collective-permute-start.3 = (bf16[64,2048]{1,0:T(8,128)(2,1)S(1)}, bf16[64,2048]{1,0:T(8,128)(2,1)S(1)}, u32[]{:S(2)}, u32[]{:S(2)}) collective-permute-start(bf16[64,2048]{1,0:T(8,128)(2,1)S(1)} %constant_dynamic-update-slice_fusion.refs_0_), channel_id=1, source_target_pairs={{0,2},{1,3},{2,0},{3,1},{4,6},{5,7},{6,4},{7,5},{8,10},{9,11},{10,... | collective-permute-start | bytes 786440 | tf_op jit(solution)/shard_map/ppermute | solution.py:289
  32.6 29.9 %collective-permute-start.15 = (bf16[128,1024]{1,0:T(8,128)(2,1)}, bf16[128,1024]{1,0:T(8,128)(2,1)S(1)}, u32[]{:S(2)}, u32[]{:S(2)}) collective-permute-start(bf16[128,1024]{1,0:T(8,128)(2,1)} %constant_dynamic-slice_fusion), channel_id=1, source_target_pairs={{0,6},{1,7},{2,4},{3,5},{4,2},{5,3},{6,0},{7,1},{8,14},{9,15},{10,... | collective-permute-start | bytes 786440 | tf_op jit(solution)/shard_map/ppermute | solution.py:289
  35.0 27.5 %collective-permute-start.14 = (bf16[128,1024]{1,0:T(8,128)(2,1)}, bf16[128,1024]{1,0:T(8,128)(2,1)}, u32[]{:S(2)}, u32[]{:S(2)}) collective-permute-start(bf16[128,1024]{1,0:T(8,128)(2,1)} %constant_dynamic-slice_fusion), channel_id=1, source_target_pairs={{0,4},{1,5},{2,6},{3,7},{4,0},{5,1},{6,2},{7,3},{8,12},{9,13},{10,... | collective-permute-start | bytes 786440 | tf_op jit(solution)/shard_map/ppermute | solution.py:289
  35.6 26.9 %collective-permute-start.13 = (bf16[128,1024]{1,0:T(8,128)(2,1)}, bf16[128,1024]{1,0:T(8,128)(2,1)}, u32[]{:S(2)}, u32[]{:S(2)}) collective-permute-start(bf16[128,1024]{1,0:T(8,128)(2,1)} %constant_dynamic-slice_fusion), channel_id=1, source_target_pairs={{0,2},{1,3},{2,0},{3,1},{4,6},{5,7},{6,4},{7,5},{8,10},{9,11},{10,... | collective-permute-start | bytes 786440 | tf_op jit(solution)/shard_map/ppermute | solution.py:289
  36.1 14.9 %all-to-all-start = ((bf16[16,16,384]{2,1,0:T(8,128)(2,1)}), bf16[16,16,384]{2,1,0:T(8,128)(2,1)S(1)}, u32[]{:S(2)}, u32[]{:S(2)}) async-start(bf16[16,16,384]{2,1,0:T(8,128)(2,1)} %bitcast.9), calls=%async_computation | async-start | bytes 393216 | tf_op jit(solution)/shard_map/all_to_all | solution.py:387
  62.5 12.3 %collective-permute-start.16 = (bf16[128,1024]{1,0:T(8,128)(2,1)}, bf16[128,1024]{1,0:T(8,128)(2,1)S(1)}, u32[]{:S(2)}, u32[]{:S(2)}) collective-permute-start(bf16[128,1024]{1,0:T(8,128)(2,1)} %collective-permute-done.13.refs_5_), channel_id=1, source_target_pairs={{0,1},{1,0},{2,3},{3,2},{4,5},{5,4},{6,7},{7,6},{8,9},{9,8},{10,11... | collective-permute-start | bytes 786440 | tf_op jit(solution)/shard_map/ppermute | solution.py:289
  62.6 12.3 %collective-permute-start.17 = (bf16[128,1024]{1,0:T(8,128)(2,1)}, bf16[128,1024]{1,0:T(8,128)(2,1)S(1)}, u32[]{:S(2)}, u32[]{:S(2)}) collective-permute-start(bf16[128,1024]{1,0:T(8,128)(2,1)} %collective-permute-done.14.refs_6_), channel_id=1, source_target_pairs={{0,1},{1,0},{2,3},{3,2},{4,5},{5,4},{6,7},{7,6},{8,9},{9,8},{10,11... | collective-permute-start | bytes 786440 | tf_op jit(solution)/shard_map/ppermute | solution.py:289
  63.1 11.8 %collective-permute-start.18 = (bf16[128,1024]{1,0:T(8,128)(2,1)S(1)}, bf16[128,1024]{1,0:T(8,128)(2,1)S(1)}, u32[]{:S(2)}, u32[]{:S(2)}) collective-permute-start(bf16[128,1024]{1,0:T(8,128)(2,1)S(1)} %collective-permute-done.15.refs_7_), channel_id=1, source_target_pairs={{0,1},{1,0},{2,3},{3,2},{4,5},{5,4},{6,7},{7,6},{8,9},{9,8},{10,11... | collective-permute-start | bytes 786440 | tf_op jit(solution)/shard_map/ppermute | solution.py:289
  63.1 7.2 %collective-permute-start.11 = (bf16[16,2176]{1,0:T(8,128)(2,1)}, bf16[16,2176]{1,0:T(8,128)(2,1)S(1)}, u32[]{:S(2)}, u32[]{:S(2)}) collective-permute-start(bf16[16,2176]{1,0:T(8,128)(2,1)} %get-tuple-element.24.refs_0_), channel_id=1, source_target_pairs={{0,24},{1,25},{2,26},{3,27},{4,28},{5,29},{6,30},{7,31},{8,16},{9,... | collective-permute-start | bytes 208904 | tf_op jit(solution)/shard_map/ppermute | solution.py:289
  65.4 7.3 %collective-permute-start.10 = (bf16[16,2176]{1,0:T(8,128)(2,1)}, bf16[16,2176]{1,0:T(8,128)(2,1)S(1)}, u32[]{:S(2)}, u32[]{:S(2)}) collective-permute-start(bf16[16,2176]{1,0:T(8,128)(2,1)} %get-tuple-element.24.refs_0_), channel_id=1, source_target_pairs={{0,16},{1,17},{2,18},{3,19},{4,20},{5,21},{6,22},{7,23},{8,24},{9,... | collective-permute-start | bytes 208904 | tf_op jit(solution)/shard_map/ppermute | solution.py:289
  70.3 4.5 %collective-permute-start.9 = (bf16[16,2176]{1,0:T(8,128)(2,1)}, bf16[16,2176]{1,0:T(8,128)(2,1)S(1)}, u32[]{:S(2)}, u32[]{:S(2)}) collective-permute-start(bf16[16,2176]{1,0:T(8,128)(2,1)} %get-tuple-element.24.refs_0_), channel_id=1, source_target_pairs={{0,8},{1,9},{2,10},{3,11},{4,12},{5,13},{6,14},{7,15},{8,0},{9,1},... | collective-permute-start | bytes 208904 | tf_op jit(solution)/shard_map/ppermute | solution.py:289
  77.8 4.6 %collective-permute-start.19 = (bf16[32,512]{1,0:T(8,128)(2,1)S(1)}, bf16[32,512]{1,0:T(8,128)(2,1)S(1)}, u32[]{:S(2)}, u32[]{:S(2)}) collective-permute-start(bf16[32,512]{1,0:T(8,128)(2,1)S(1)} %get-tuple-element.30), channel_id=1, source_target_pairs={{0,8},{1,9},{2,10},{3,11},{4,12},{5,13},{6,14},{7,15},{8,0},{9,1},... | collective-permute-start | bytes 98312 | tf_op jit(solution)/shard_map/ppermute | solution.py:289
  77.8 4.9 %collective-permute-start.20 = (bf16[32,512]{1,0:T(8,128)(2,1)S(1)}, bf16[32,512]{1,0:T(8,128)(2,1)S(1)}, u32[]{:S(2)}, u32[]{:S(2)}) collective-permute-start(bf16[32,512]{1,0:T(8,128)(2,1)S(1)} %get-tuple-element.31), channel_id=1, source_target_pairs={{0,16},{1,17},{2,18},{3,19},{4,20},{5,21},{6,22},{7,23},{8,24},{9,... | collective-permute-start | bytes 98312 | tf_op jit(solution)/shard_map/ppermute | solution.py:289
  80.7 5.7 %collective-permute-start.21 = (bf16[32,512]{1,0:T(8,128)(2,1)S(1)}, bf16[32,512]{1,0:T(8,128)(2,1)S(1)}, u32[]{:S(2)}, u32[]{:S(2)}) collective-permute-start(bf16[32,512]{1,0:T(8,128)(2,1)S(1)} %get-tuple-element.32), channel_id=1, source_target_pairs={{0,24},{1,25},{2,26},{3,27},{4,28},{5,29},{6,30},{7,31},{8,16},{9,... | collective-permute-start | bytes 98312 | tf_op jit(solution)/shard_map/ppermute | solution.py:289
  87.1 6.0 %collective-permute-start.24 = (bf16[32,2176]{1,0:T(8,128)(2,1)S(1)}, bf16[32,2176]{1,0:T(8,128)(2,1)S(1)}, u32[]{:S(2)}, u32[]{:S(2)}) collective-permute-start(bf16[32,2176]{1,0:T(8,128)(2,1)S(1)} %get-tuple-element.36.refs_0_), channel_id=1, source_target_pairs={{0,6},{1,7},{2,4},{3,5},{4,2},{5,3},{6,0},{7,1},{8,14},{9,15},{10,... | collective-permute-start | bytes 417800 | tf_op jit(solution)/shard_map/ppermute | solution.py:289
  89.6 5.1 %collective-permute-start.23 = (bf16[32,2176]{1,0:T(8,128)(2,1)S(1)}, bf16[32,2176]{1,0:T(8,128)(2,1)S(1)}, u32[]{:S(2)}, u32[]{:S(2)}) collective-permute-start(bf16[32,2176]{1,0:T(8,128)(2,1)S(1)} %get-tuple-element.36.refs_0_), channel_id=1, source_target_pairs={{0,4},{1,5},{2,6},{3,7},{4,0},{5,1},{6,2},{7,3},{8,12},{9,13},{10,... | collective-permute-start | bytes 417800 | tf_op jit(solution)/shard_map/ppermute | solution.py:289
  90.1 5.1 %collective-permute-start.22 = (bf16[32,2176]{1,0:T(8,128)(2,1)S(1)}, bf16[32,2176]{1,0:T(8,128)(2,1)S(1)}, u32[]{:S(2)}, u32[]{:S(2)}) collective-permute-start(bf16[32,2176]{1,0:T(8,128)(2,1)S(1)} %get-tuple-element.36.refs_0_), channel_id=1, source_target_pairs={{0,2},{1,3},{2,0},{3,1},{4,6},{5,7},{6,4},{7,5},{8,10},{9,11},{10,... | collective-permute-start | bytes 417800 | tf_op jit(solution)/shard_map/ppermute | solution.py:289
  101.1 6.4 %collective-permute-start.30 = (bf16[32,2048]{1,0:T(8,128)(2,1)S(1)}, bf16[32,2048]{1,0:T(8,128)(2,1)S(1)}, u32[]{:S(2)}, u32[]{:S(2)}) collective-permute-start(bf16[32,2048]{1,0:T(8,128)(2,1)S(1)} %get-tuple-element.42), channel_id=1, source_target_pairs={{0,2},{1,3},{2,0},{3,1},{4,6},{5,7},{6,4},{7,5},{8,10},{9,11},{10,... | collective-permute-start | bytes 393224 | tf_op jit(solution)/shard_map/ppermute | solution.py:289
  102.3 8.3 %collective-permute-start.32 = (bf16[32,2048]{1,0:T(8,128)(2,1)S(1)}, bf16[32,2048]{1,0:T(8,128)(2,1)S(1)}, u32[]{:S(2)}, u32[]{:S(2)}) collective-permute-start(bf16[32,2048]{1,0:T(8,128)(2,1)S(1)} %get-tuple-element.43), channel_id=1, source_target_pairs={{0,6},{1,7},{2,4},{3,5},{4,2},{5,3},{6,0},{7,1},{8,14},{9,15},{10,... | collective-permute-start | bytes 393224 | tf_op jit(solution)/shard_map/ppermute | solution.py:289
  104.2 7.8 %collective-permute-start.31 = (bf16[32,2048]{1,0:T(8,128)(2,1)S(1)}, bf16[32,2048]{1,0:T(8,128)(2,1)S(1)}, u32[]{:S(2)}, u32[]{:S(2)}) collective-permute-start(bf16[32,2048]{1,0:T(8,128)(2,1)S(1)} %get-tuple-element.44), channel_id=1, source_target_pairs={{0,4},{1,5},{2,6},{3,7},{4,0},{5,1},{6,2},{7,3},{8,12},{9,13},{10,... | collective-permute-start | bytes 393224 | tf_op jit(solution)/shard_map/ppermute | solution.py:289
  112.1 5.8 %collective-permute-start.35 = (bf16[8,2048]{1,0:T(8,128)(2,1)S(1)}, bf16[8,2048]{1,0:T(8,128)(2,1)S(1)}, u32[]{:S(2)}, u32[]{:S(2)}) collective-permute-start(bf16[8,2048]{1,0:T(8,128)(2,1)S(1)} %get-tuple-element.46), channel_id=1, source_target_pairs={{0,24},{1,25},{2,26},{3,27},{4,28},{5,29},{6,30},{7,31},{8,16},{9,... | collective-permute-start | bytes 98312 | tf_op jit(solution)/shard_map/ppermute | solution.py:289
  112.7 5.2 %collective-permute-start.34 = (bf16[8,2048]{1,0:T(8,128)(2,1)S(1)}, bf16[8,2048]{1,0:T(8,128)(2,1)S(1)}, u32[]{:S(2)}, u32[]{:S(2)}) collective-permute-start(bf16[8,2048]{1,0:T(8,128)(2,1)S(1)} %get-tuple-element.47), channel_id=1, source_target_pairs={{0,16},{1,17},{2,18},{3,19},{4,20},{5,21},{6,22},{7,23},{8,24},{9,... | collective-permute-start | bytes 98312 | tf_op jit(solution)/shard_map/ppermute | solution.py:289
  112.7 5.7 %collective-permute-start.33 = (bf16[8,2048]{1,0:T(8,128)(2,1)S(1)}, bf16[8,2048]{1,0:T(8,128)(2,1)S(1)}, u32[]{:S(2)}, u32[]{:S(2)}) collective-permute-start(bf16[8,2048]{1,0:T(8,128)(2,1)S(1)} %get-tuple-element.48), channel_id=1, source_target_pairs={{0,8},{1,9},{2,10},{3,11},{4,12},{5,13},{6,14},{7,15},{8,0},{9,1},... | collective-permute-start | bytes 98312 | tf_op jit(solution)/shard_map/ppermute | solution.py:289
  (19 other events, 370.3 us)
